TPU v7x, 32 devices: a whole 2x2x4 slice. The times are simulated.
32 devices in a mesh: ep: 8 (over z, core), tp: 4 (over y, x).
Axes of the slice: x: 2, y: 2, z: 4, core: 2. Of those that a mesh axis runs over, the one named last changes fastest.
Arguments:
- query_rows: bfloat16 [3072, 2048], P('ep', 'tp'), may hold values from -6 to 6
- key_rows: bfloat16 [3072, 2048], P('ep', 'tp'), may hold values from -6 to 6
- value_rows: bfloat16 [3072, 2048], P('ep', 'tp'), may hold values from -6 to 6
- second_scale: float32 [16], P('tp'), may hold values from 0.3 to 0.8
- head_gain: float32 [128], replicated, may hold values from 0.1 to 1.9
- out_weight: bfloat16 [2048, 4096], P(None, 'tp'), may hold values from -0.125 to 0.125
- routed_rows: bfloat16 [1024, 4096], P('ep', 'tp'), may hold values from -6 to 6
- norm_gain: float32 [4096], replicated, may hold values from 0.1 to 1.9
- route_ids: int32 [1024, 2], P('ep'), may hold values from 0 to 7, all different within a row; in each aligned block of 128 rows (0 to 127, 128 to 255, ...) at most 64 rows name the same one
- route_weight: float32 [1024, 2], P('ep'), may hold values from 0.1 to 0.9
- expert_gate: bfloat16 [8, 4096, 2048], P('ep', None, 'tp'), may hold values from -0.09375 to 0.09375
- expert_up: bfloat16 [8, 4096, 2048], P('ep', None, 'tp'), may hold values from -0.09375 to 0.09375
- expert_down: bfloat16 [8, 2048, 4096], P('ep', None, 'tp'), may hold values from -0.125 to 0.125
Outputs:
- mixer_out: bfloat16 [3072, 4096], P('ep', 'tp')
- expert_mix: bfloat16 [1024, 4096], P('ep', 'tp')
Inputs may be any that keep to these rules, and one draw needn't show every extreme that they name: `route_ids`: among the 128 tokens of one index of ep, no expert is named by more than 64 of them, a bound that some block reaches.
All inputs are finite; a program needn't handle non-finite values.
Results may differ from a plain program's by a relative error of at most 0.0085.
Values may be sent and summed in bfloat16 or wider, within the bound.
No kernel may reach another device: no remote copies, remote signals or barrier semaphores. Data moves between devices by JAX's collectives and lax.ppermute only.
A program may use at most 128 MiB of HBM per device.

v0:
```python
import functools

import jax
import jax.numpy as jnp
from jax import lax
from jax.experimental import pallas as pl
from jax.experimental.pallas import tpu as pltpu
from jax.sharding import PartitionSpec as P


eps = 1e-06
head_factor = 0.8
neg_big = -1e30
key_block_rows = 1024


def rms_rows(rows_in, gain):
    floats = rows_in.astype(jnp.float32)
    factor = lax.rsqrt(jnp.mean(floats * floats, axis=-1, keepdims=True) + eps)
    return (floats * factor * gain).astype(jnp.bfloat16)


def per_device(
    query_rows,
    key_rows,
    value_rows,
    second_scale,
    head_gain,
    out_weight,
    routed_rows,
    norm_gain,
    route_ids,
    route_weight,
    expert_gate,
    expert_up,
    expert_down,
):
    count_a = query_rows.shape[0]
    per_head = second_scale.shape[0]
    head_dim = query_rows.shape[1] // (2 * per_head)
    value_dim = head_gain.shape[0]
    query_four = query_rows.reshape(count_a, per_head, 2, head_dim)
    query_pos = lax.axis_index("ep") * count_a + jnp.arange(count_a, dtype=jnp.int32)

    def key_block(carry_state, key_part, value_part, block_start):
        key_count = key_part.shape[0]
        key_four = key_part.reshape(key_count, per_head, 2, head_dim)
        value_three = value_part.reshape(key_count, per_head, value_dim)
        scores = jnp.einsum(
            "ihcd,jhcd->ihcj", query_four, key_four, preferred_element_type=jnp.float32
        ) * head_dim ** (-0.5)
        allowed = (
            query_pos[:, None] >= block_start + jnp.arange(key_count, dtype=jnp.int32)[None, :]
        )[:, None, None, :]
        scores = jnp.where(allowed, scores, neg_big)
        old_max, old_sum, old_acc = carry_state
        new_max = jnp.maximum(old_max, jnp.max(scores, axis=-1))
        weights = jnp.where(allowed, jnp.exp(scores - new_max[..., None]), 0.0)
        shrink = jnp.exp(old_max - new_max)
        new_sum = old_sum * shrink + jnp.sum(weights, axis=-1)
        update = jnp.einsum(
            "ihcj,jhe->ihce",
            weights.astype(jnp.bfloat16),
            value_three,
            preferred_element_type=jnp.float32,
        )
        return (new_max, new_sum, old_acc * shrink[..., None] + update)

    start_state = (
        jnp.full((count_a, per_head, 2), neg_big, jnp.float32),
        jnp.zeros((count_a, per_head, 2), jnp.float32),
        jnp.zeros((count_a, per_head, 2, value_dim), jnp.float32),
    )
    key_part = lax.all_gather(key_rows, "ep", axis=0, tiled=True)
    value_part = lax.all_gather(value_rows, "ep", axis=0, tiled=True)
    key_count = key_part.shape[0]

    def step_block(block_num, inner_state):
        offset_rows = block_num * key_block_rows
        key_slice = lax.dynamic_slice_in_dim(key_part, offset_rows, key_block_rows, 0)
        value_slice = lax.dynamic_slice_in_dim(value_part, offset_rows, key_block_rows, 0)
        return key_block(inner_state, key_slice, value_slice, offset_rows)

    _, run_sum, run_acc = lax.fori_loop(0, key_count // key_block_rows, step_block, start_state)
    maps_both = run_acc / run_sum[..., None]
    mixed_maps = maps_both[:, :, 0] - second_scale[None, :, None] * maps_both[:, :, 1]
    mean_sq = jnp.mean(mixed_maps * mixed_maps, axis=-1, keepdims=True)
    head_out = (
        (mixed_maps * lax.rsqrt(mean_sq + eps) * head_gain * head_factor)
        .astype(jnp.bfloat16)
        .reshape(count_a, per_head * value_dim)
    )
    count_b = routed_rows.shape[0]
    route_count = route_ids.shape[1]
    experts_here = expert_gate.shape[0]
    ep_devices = lax.axis_size("ep")
    expert_total = experts_here * ep_devices
    capacity = 2 * count_b * route_count // expert_total
    flat_expert = route_ids.reshape(-1)
    chosen = (flat_expert[:, None] == jnp.arange(expert_total, dtype=jnp.int32)[None, :]).astype(
        jnp.int32
    )
    ranks = jnp.sum((jnp.cumsum(chosen, axis=0) - 1) * chosen, axis=1)
    slot_of = flat_expert * capacity + ranks
    token_of = jnp.arange(count_b * route_count, dtype=jnp.int32) // route_count
    slot_token = jnp.full((expert_total * capacity,), count_b, jnp.int32).at[slot_of].set(token_of)
    padded = jnp.concatenate(
        [routed_rows, jnp.zeros((1, routed_rows.shape[1]), jnp.bfloat16)], axis=0
    )
    outgoing = padded[slot_token].reshape(ep_devices, experts_here, capacity, routed_rows.shape[1])
    column_parts = lax.all_to_all(outgoing, "ep", split_axis=0, concat_axis=0, tiled=True)
    arrived = rms_rows(lax.all_gather(column_parts, "tp", axis=3, tiled=True), norm_gain)
    gate_val = jnp.einsum(
        "sxcd,xdf->sxcf", arrived, expert_gate, preferred_element_type=jnp.float32
    )
    up_val = jnp.einsum("sxcd,xdf->sxcf", arrived, expert_up, preferred_element_type=jnp.float32)
    hidden = (jax.nn.silu(gate_val) * up_val).astype(jnp.bfloat16)
    weight_rows = out_weight
    attn_total = jnp.dot(
        lax.all_gather(
            head_out.reshape(1, 1, count_a, head_out.shape[1]), "tp", axis=3, tiled=True
        )[0, 0],
        weight_rows,
        preferred_element_type=jnp.float32,
    )
    weight_rows = expert_down
    moe_total = jnp.einsum(
        "sxcf,xfd->sxcd",
        lax.all_gather(hidden, "tp", axis=3, tiled=True),
        weight_rows,
        preferred_element_type=jnp.float32,
    )
    mixer_out = attn_total.astype(jnp.bfloat16)
    returned = lax.all_to_all(
        moe_total.astype(jnp.bfloat16), "ep", split_axis=0, concat_axis=0, tiled=True
    )
    flat_back = returned.reshape(expert_total * capacity, returned.shape[3])
    picked = flat_back[slot_of].astype(jnp.float32).reshape(count_b, route_count, returned.shape[3])
    expert_mix = jnp.sum(picked * route_weight[:, :, None], axis=1).astype(jnp.bfloat16)
    return (mixer_out, expert_mix)


bf16 = jnp.bfloat16
f32 = jnp.float32
vmem = pl.BlockSpec(memory_space=pltpu.VMEM)
smem = pl.BlockSpec(memory_space=pltpu.SMEM)


def params(limit):
    return pltpu.CompilerParams(vmem_limit_bytes=limit * 1024 * 1024)


def near(value):
    return pltpu.with_memory_space_constraint(value, pltpu.VMEM)


def near_shapes(tree):
    return jax.tree.map(lambda leaf: pltpu.VMEM(leaf.shape, leaf.dtype), tree)


def sds(*shape):
    return jax.ShapeDtypeStruct(shape, bf16)


def pack_kernel(width, where_ref, q_ref, k_ref, v_ref, *outs):
    chip = where_ref[0]
    scale = (width // 2) ** (-0.5)
    for slot, out in enumerate(outs):
        at = pl.ds(pl.multiple_of((chip ^ slot) * width, width), width)
        out[:, 0:width] = (q_ref[:, at].astype(f32) * scale).astype(bf16)
        out[:, width : 2 * width] = k_ref[:, at]
        out[:, 2 * width : 3 * width] = v_ref[:, at]


def attention_kernel(chips, count, width, where_ref, scale_ref, gain_ref, *refs):
    own, other = refs[:chips], refs[chips : 2 * chips]
    outs = refs[2 * chips : 3 * chips]
    keys, values, queries, scores, acc, row_max, row_sum = refs[3 * chips :]
    chip, core = where_ref[0], where_ref[1]
    half = width // 2
    pair = 2 * count
    for slot in range(chips):
        at = chip ^ slot
        for parity, part in ((core, own[slot]), (1 - core, other[slot])):
            rows = pl.ds(pl.multiple_of(parity * count, count), count)
            keys[at, rows] = part[:, width : 2 * width]
            values[at, rows] = part[:, 2 * width : 3 * width]
    lane = lax.broadcasted_iota(jnp.int32, (count, width), 1)

    def widest(block):
        best = block[:, 0:width]
        for i in range(width, pair, width):
            best = jnp.maximum(best, block[:, i : i + width])
        return best

    def products(number):
        return lax.dot_general(
            queries[...], keys[number], (((1,), (1,)), ((), ())), preferred_element_type=f32
        )

    def weigh(number):
        top = row_max[...]
        block = [
            jnp.exp(scores[number, :, i : i + width] - top) for i in range(0, pair, width)
        ]
        total = functools.reduce(jnp.add, block)
        weights = jnp.concatenate([part.astype(bf16) for part in block], axis=1)
        return total, jnp.dot(weights, values[number], preferred_element_type=f32)

    for slot in range(chips):
        last = chip ^ slot
        rows = own[slot][:, 0:width]
        queries[0:count] = jnp.where(lane < half, rows, jnp.zeros_like(rows))
        queries[count:pair] = jnp.where(lane < half, jnp.zeros_like(rows), rows)
        allowed = lax.broadcasted_iota(jnp.int32, (pair, pair), 1) <= (
            lax.broadcasted_iota(jnp.int32, (pair, pair), 0) % count + core * count
        )
        masked = jnp.where(allowed, products(last), neg_big)
        scores[last] = masked
        row_max[...] = widest(masked)

        @pl.loop(0, last)
        def _(number):
            block = products(number)
            scores[number] = block
            row_max[...] = jnp.maximum(row_max[...], widest(block))

        row_max[...] = jnp.broadcast_to(
            jnp.max(row_max[...], axis=-1, keepdims=True), row_max.shape
        )
        row_sum[...], acc[...] = weigh(last)

        @pl.loop(0, last)
        def _(number):
            total, update = weigh(number)
            row_sum[...] += total
            acc[...] += update

        maps = acc[...] / jnp.sum(row_sum[...], axis=-1, keepdims=True)
        mixed = maps[0:count] - scale_ref[chip] * maps[count:pair]
        mean_sq = jnp.mean(mixed * mixed, axis=-1, keepdims=True)
        outs[slot][...] = (
            mixed * lax.rsqrt(mean_sq + eps) * gain_ref[...] * head_factor
        ).astype(bf16)


def project_kernel(parts, groups, width, where_ref, w_ref, *refs):
    pieces, (out, heads) = refs[: len(groups) * parts], refs[-2:]
    chip, tp = where_ref[0], where_ref[2]
    depth = heads.shape[1] // parts
    for part in range(parts):
        for number, slots in enumerate(groups):
            for i, slot in enumerate(slots):
                at = pl.multiple_of((tp ^ part) * depth + (chip ^ slot) * width, width)
                heads[:, pl.ds(at, width)] = pieces[number * parts + part][
                    :, i * width : (i + 1) * width
                ]
    out[...] = jnp.dot(heads[...], w_ref[...], preferred_element_type=f32).astype(bf16)


def rows_kernel(count, rows_ref, ids_ref, share_ref, out, ids, share, sems):
    copies = [
        pltpu.make_async_copy(rows_ref, out.at[0:count], sems.at[0]),
        pltpu.make_async_copy(ids_ref, ids, sems.at[1]),
        pltpu.make_async_copy(share_ref, share, sems.at[2]),
    ]
    for copy in copies:
        copy.start()
    out[count:] = jnp.zeros((out.shape[0] - count, out.shape[1]), bf16)
    copies[1].wait()
    copies[2].wait()
    table, rest = [ids[...].astype(f32)], share[...]
    for _ in range(3):
        table.append(rest.astype(bf16).astype(f32))
        rest = rest - table[-1]
    out[count:, 0:count] = jnp.concatenate(table, axis=0).astype(bf16)
    copies[0].wait()


def select_kernel(count, routes, capacity, groups, where_ref, *refs):
    slots = [slot for group in groups for slot in group]
    own, other, outs = refs[: len(slots)], refs[len(slots) : 2 * len(slots)], refs[2 * len(slots) :]
    expert = (2 * where_ref[0] + where_ref[1]).astype(f32)
    before = (
        lax.broadcasted_iota(jnp.int32, (count, count), 0)
        < lax.broadcasted_iota(jnp.int32, (count, count), 1)
    ).astype(f32).astype(bf16)
    row_of = lax.broadcasted_iota(jnp.int32, (capacity, count), 0).astype(f32)
    at = 0
    for out, group in zip(outs, groups):
        for i in range(len(group)):
            for side, part in ((0, own[at]), (1, other[at])):
                ids = part[count : count + 8, 0:count].astype(f32)
                chosen = jnp.zeros((1, count), f32)
                for k in range(routes):
                    chosen = jnp.where(ids[k : k + 1] == expert, 1.0, chosen)
                rank = jnp.dot(
                    jnp.broadcast_to(chosen, (8, count)).astype(bf16),
                    before,
                    preferred_element_type=f32,
                )[0:1]
                rank = jnp.where(chosen > 0, rank, -1.0)
                pick = jnp.where(row_of == rank, 1.0, 0.0).astype(bf16)
                first = (2 * i + side) * capacity
                out[first : first + capacity] = jnp.dot(
                    pick, part[0:count], preferred_element_type=f32
                ).astype(bf16)
            at += 1


def gate_up_kernel(parts, groups, where_ref, gain_ref, gate_ref, up_ref, *refs):
    pieces, (out, rows) = refs[: groups * parts], refs[-2:]
    tp = where_ref[2]
    width = rows.shape[1] // parts
    count = rows.shape[0] // groups
    factors = []
    for group in range(groups):
        square = jnp.zeros((count, 128), f32)
        for part in range(parts):
            floats = pieces[group * parts + part][...].astype(f32)
            for i in range(0, width, 128):
                square = square + floats[:, i : i + 128] * floats[:, i : i + 128]
            at = pl.ds(pl.multiple_of((tp ^ part) * width, width), width)
            rows[group * count : (group + 1) * count, at] = (
                floats * gain_ref[tp ^ part]
            ).astype(bf16)
        mean = jnp.sum(square, axis=-1, keepdims=True) * (1.0 / rows.shape[1])
        factors.append(lax.rsqrt(mean + eps))
    factor = jnp.concatenate(factors, axis=0)
    g = jnp.dot(rows[...], gate_ref[0], preferred_element_type=f32) * factor
    u = jnp.dot(rows[...], up_ref[0], preferred_element_type=f32) * factor
    out[...] = (g / (1.0 + jnp.exp(-g)) * u).astype(bf16)


def down_kernel(parts, capacity, where_ref, w_ref, *refs):
    pieces, (own_out, other_out, rows) = refs[:parts], refs[-3:]
    tp = where_ref[2]
    width = rows.shape[1] // parts
    for part in range(parts):
        rows[:, pl.ds(pl.multiple_of((tp ^ part) * width, width), width)] = pieces[part][...]
    total = jnp.dot(rows[...], w_ref[0], preferred_element_type=f32).astype(bf16)
    for i in range(total.shape[0] // capacity):
        at = i // 2 * capacity
        (own_out, other_out)[i % 2][at : at + capacity] = total[i * capacity : (i + 1) * capacity]


def combine_kernel(chips, count, capacity, routes, where_ref, *refs):
    ids_refs, mine_ref, theirs_ref = refs[:chips], refs[chips], refs[chips + 1]
    outs, rows = refs[chips + 2 : 2 * chips + 2], refs[-1]
    chip, core = where_ref[0], where_ref[1]
    before = (
        lax.broadcasted_iota(jnp.int32, (count, count), 0)
        < lax.broadcasted_iota(jnp.int32, (count, count), 1)
    ).astype(f32).astype(bf16)
    row_of = lax.broadcasted_iota(jnp.int32, (capacity, count), 0).astype(f32)
    for slot, out in enumerate(outs):
        part = ids_refs[slot][count : count + 8, 0:count].astype(f32)
        terms = [[], [], []]
        for side, results in ((0, mine_ref), (1, theirs_ref)):
            rows[side * capacity : (side + 1) * capacity] = results[
                slot * capacity : (slot + 1) * capacity
            ]
            expert = (2 * chip + (core ^ side)).astype(f32)
            chosen = jnp.zeros((1, count), f32)
            share = [jnp.zeros((1, count), f32)] * 3
            for k in range(routes):
                same = part[k : k + 1] == expert
                chosen = jnp.where(same, 1.0, chosen)
                for i in range(3):
                    at = routes * (1 + i) + k
                    share[i] = jnp.where(same, part[at : at + 1], share[i])
            rank = jnp.dot(
                jnp.broadcast_to(chosen, (8, count)).astype(bf16),
                before,
                preferred_element_type=f32,
            )[0:1]
            rank = jnp.where(chosen > 0, rank, -1.0)
            for i in range(3):
                terms[i].append(jnp.where(row_of == rank, share[i], 0.0).astype(bf16))
        total = jnp.zeros(out.shape, f32)
        for i in range(3):
            total = total + lax.dot_general(
                jnp.concatenate(terms[i], axis=0),
                rows[...],
                (((0,), (0,)), ((), ())),
                preferred_element_type=f32,
            )
        out[...] = total.astype(bf16)


def per_device_fast(
    query_rows,
    key_rows,
    value_rows,
    second_scale,
    head_gain,
    out_weight,
    routed_rows,
    norm_gain,
    route_ids,
    route_weight,
    expert_gate,
    expert_up,
    expert_down,
):
    ep_devices, tp_devices = lax.axis_size("ep"), lax.axis_size("tp")
    chips = ep_devices // 2
    count_a, count_b = query_rows.shape[0], routed_rows.shape[0]
    heads_here = second_scale.shape[0]
    width = query_rows.shape[1] // heads_here
    columns = routed_rows.shape[1]
    model = columns * tp_devices
    routes = route_ids.shape[1]
    capacity = 2 * count_b * routes // ep_devices
    units = expert_gate.shape[2]
    out_columns = out_weight.shape[1]
    ep_at = lax.axis_index("ep")
    where = jnp.stack([ep_at // 2, ep_at % 2, lax.axis_index("tp")]).astype(jnp.int32)

    def over_ep(value, slot, cross=0):
        pairs = [(i, (((i // 2) ^ slot) * 2 + (i % 2)) ^ cross) for i in range(ep_devices)]
        return lax.ppermute(value, "ep", pairs)

    def over_tp(value, offset):
        return lax.ppermute(value, "tp", [(i, i ^ offset) for i in range(tp_devices)])

    def spread(value, first):
        second = 3 ^ first
        one = over_tp(value, first)
        two = over_tp(value, second)
        pieces = {0: value, first: one, second: two, 3: over_tp(one, second)}
        return [pieces[offset] for offset in range(tp_devices)]

    def spread_direct(value):
        return [value] + [over_tp(value, offset) for offset in range(1, tp_devices)]

    def call(body, out_shape, *args, scratch=(), scalars=1, limit=8, last=False):
        return pl.pallas_call(
            body,
            out_shape=out_shape if last else near_shapes(out_shape),
            in_specs=[smem] * scalars + [vmem] * (len(args) - scalars),
            out_specs=jax.tree.map(lambda _: vmem, out_shape),
            scratch_shapes=list(scratch),
            compiler_params=params(limit),
        )(*args[:scalars], *[near(arg) for arg in args[scalars:]])

    far = [
        pltpu.with_memory_space_constraint(value, pltpu.HBM)
        for value in (routed_rows, route_ids.T, route_weight.T)
    ]
    packed = pl.pallas_call(
        functools.partial(rows_kernel, count_b),
        out_shape=pltpu.VMEM((count_b + 4 * routes, columns), bf16),
        in_specs=[pl.BlockSpec(memory_space=pltpu.HBM)] * 3,
        out_specs=vmem,
        scratch_shapes=[
            pltpu.VMEM((routes, count_b), jnp.int32),
            pltpu.VMEM((routes, count_b), f32),
            pltpu.SemaphoreType.DMA((3,)),
        ],
        compiler_params=params(8),
    )(*far)
    arrived = [packed] + [over_ep(packed, slot) for slot in range(1, chips)]
    swapped = [over_ep(part, 0, 1) for part in arrived]

    packs = call(
        functools.partial(pack_kernel, width),
        [sds(count_a, 3 * width)] * chips,
        where,
        query_rows,
        key_rows,
        value_rows,
    )
    mine = [packs[0]] + [over_ep(packs[slot], slot) for slot in range(1, chips)]
    theirs = [over_ep(part, 0, 1) for part in mine]

    gain_parts = norm_gain.reshape(tp_devices, 1, columns)
    mixes = {}
    for slots in row_groups:
        total = 2 * capacity * len(slots)
        pieces = []
        for slot in slots:
            picked = call(
        functools.partial(select_kernel, count_b, routes, capacity, [(slot,)]),
        sds(2 * capacity, columns),
        where,
        arrived[slot],
        swapped[slot],
            )
            pieces += spread(picked, 1 + slot % 2)
        hidden = call(
            functools.partial(gate_up_kernel, tp_devices, len(slots)),
            sds(total, units),
            where,
            gain_parts,
            expert_gate,
            expert_up,
            *pieces,
            scratch=[pltpu.VMEM((total, model), bf16)],
            limit=16,
        )
        own_side, other_side = call(
            functools.partial(down_kernel, tp_devices, capacity),
            [sds(capacity * len(slots), columns)] * 2,
            where,
            expert_down,
            *spread_direct(hidden),
            scratch=[pltpu.VMEM((total, units * tp_devices), bf16)],
            limit=12,
        )
        mixed = call(
        functools.partial(combine_kernel, len(slots), count_b, capacity, routes),
        [sds(count_b, columns)] * len(slots),
        where,
        *[arrived[slot] for slot in slots],
        own_side,
        over_ep(other_side, 0, 1),
        scratch=[pltpu.VMEM((2 * capacity, columns), bf16)],
        )
        for slot, part in zip(slots, mixed):
            mixes[slot] = over_ep(part, slot) if slot else part

    head_outs = call(
        functools.partial(attention_kernel, chips, count_a, width),
        [sds(count_a, width)] * chips,
        where,
        second_scale,
        head_gain.reshape(1, width),
        *mine,
        *theirs,
        scalars=2,
        limit=24,
        scratch=[
            pltpu.VMEM((chips, 2 * count_a, width), bf16),
            pltpu.VMEM((chips, 2 * count_a, width), bf16),
            pltpu.VMEM((2 * count_a, width), bf16),
            pltpu.VMEM((chips, 2 * count_a, 2 * count_a), f32),
            pltpu.VMEM((2 * count_a, width), f32),
            pltpu.VMEM((2 * count_a, width), f32),
            pltpu.VMEM((2 * count_a, width), f32),
        ],
    )
    back = [head_outs[0]] + [over_ep(head_outs[slot], slot) for slot in range(1, chips)]
    pieces = []
    for number, group in enumerate(head_groups):
        value = jnp.concatenate([back[slot] for slot in group], axis=1)
        pieces += spread(value, 1 + number)
    mixer_out = call(
        functools.partial(project_kernel, tp_devices, head_groups, width),
        sds(count_a, out_columns),
        where,
        out_weight,
        *pieces,
        scratch=[pltpu.VMEM((count_a, out_weight.shape[0]), bf16)],
        limit=12,
        last=True,
    )
    expert_mix = functools.reduce(
        jnp.add, [mixes[slot].astype(f32) for slot in range(chips)]
    ).astype(bf16)
    return (mixer_out, expert_mix)


row_groups = [(0, 1), (2, 3)]
head_groups = [(0, 1), (2, 3)]


def fast_fits(mesh):
    return mesh.shape["tp"] == 4 and mesh.shape["ep"] == 8


def solution(mesh):
    placed = (
        P("ep", "tp"),
        P("ep", "tp"),
        P("ep", "tp"),
        P("tp"),
        P(),
        P(None, "tp"),
        P("ep", "tp"),
        P(),
        P("ep", None),
        P("ep", None),
        P("ep", None, "tp"),
        P("ep", None, "tp"),
        P("ep", None, "tp"),
    )
    fast = fast_fits(mesh)

    def body(*args):
        if not fast:
            return per_device(*args)
        return per_device_fast(*args)

    return jax.shard_map(
        body,
        mesh=mesh,
        in_specs=placed,
        out_specs=(P("ep", "tp"), P("ep", "tp")),
        check_vma=False,
    )
```

profile of v0, /device:TPU:0, one launch (start us, length us, event | category | flops | bytes accessed | tf_op | source)
XLA Modules:
  0.0 156.7 jit_solution(5212109570756706798)
XLA Ops:
  0.6 1.0 shard_map.143.refs_0_
  1.6 5.1 %collective-permute-start.31 = (bf16[136,1024]{1,0:T(8,128)(2,1)S(1)}, bf16[136,1024]{1,0:T(8,128)(2,1)S(1)}, u32[]{:S(2)}, u32[]{:S(2)}) collective-permute-start(bf16[136,1024]{1,0:T(8,128)(2,1)S(1)} %shard_map.143.refs_0_), channel_id=1, source_target_pairs={{0,24},{4,28},{8,16},{12,20},{16,8},{20,12},{24,0},{28,4},{1,25},{... | collective-permute-start | bytes 835592 | tf_op jit(solution)/shard_map/ppermute | solution.py:422
  6.8 0.6 collective-permute-start.16
  7.5 1.1 copy-done.4
  8.6 1.1 copy-done.5
  9.8 1.0 copy-done.6
  10.8 0.8 shard_map.140
  11.6 1.5 collective-permute-start
  13.0 1.4 collective-permute-done.31.refs_0_.refs_1_
  14.4 12.8 %collective-permute-start.1 = (bf16[384,384]{1,0:T(8,128)(2,1)S(1)}, bf16[384,384]{1,0:T(8,128)(2,1)S(1)}, u32[]{:S(2)}, u32[]{:S(2)}) collective-permute-start(bf16[384,384]{1,0:T(8,128)(2,1)S(1)} %get-tuple-element.20), channel_id=1, source_target_pairs={{0,16},{4,20},{8,24},{12,28},{16,0},{20,4},{24,8},{28,12},{1,17},{... | collective-permute-start | bytes 884744 | tf_op jit(solution)/shard_map/ppermute | solution.py:422
  27.2 4.8 %collective-permute-done.30.refs_0_ = bf16[136,1024]{1,0:T(8,128)(2,1)S(1)} collective-permute-done((bf16[136,1024]{1,0:T(8,128)(2,1)S(1)}, bf16[136,1024]{1,0:T(8,128)(2,1)S(1)}, u32[]{:S(2)}, u32[]{:S(2)}) %collective-permute-start.30) | collective-permute-done | bytes 278560 | tf_op jit(solution)/shard_map/ppermute | solution.py:422
  32.0 2.2 %collective-permute-start.2 = (bf16[384,384]{1,0:T(8,128)(2,1)S(1)}, bf16[384,384]{1,0:T(8,128)(2,1)S(1)}, u32[]{:S(2)}, u32[]{:S(2)}) collective-permute-start(bf16[384,384]{1,0:T(8,128)(2,1)S(1)} %get-tuple-element.21), channel_id=1, source_target_pairs={{0,24},{4,28},{8,16},{12,20},{16,8},{20,12},{24,0},{28,4},{1,25},{... | collective-permute-start | bytes 884744 | tf_op jit(solution)/shard_map/ppermute | solution.py:422
  34.8 1.0 shard_map.144.refs_0_
  35.8 14.6 %collective-permute-done.1.refs_2_ = bf16[384,384]{1,0:T(8,128)(2,1)S(1)} collective-permute-done((bf16[384,384]{1,0:T(8,128)(2,1)S(1)}, bf16[384,384]{1,0:T(8,128)(2,1)S(1)}, u32[]{:S(2)}, u32[]{:S(2)}) %collective-permute-start.1) | collective-permute-done | bytes 294944 | tf_op jit(solution)/shard_map/ppermute | solution.py:422
  50.4 1.5 collective-permute-start.19
  52.0 1.5 collective-permute-start.18
  54.0 1.0 shard_map.150.refs_4_
  55.0 1.0 shard_map.149.refs_0_
  56.0 0.6 collective-permute-start.38
  56.9 1.5 collective-permute-start.33
  58.4 1.8 %collective-permute-start.37 = (bf16[128,1024]{1,0:T(8,128)(2,1)S(1)}, bf16[128,1024]{1,0:T(8,128)(2,1)S(1)}, u32[]{:S(2)}, u32[]{:S(2)}) collective-permute-start(bf16[128,1024]{1,0:T(8,128)(2,1)S(1)} %shard_map.150.refs_4_), channel_id=1, source_target_pairs={{0,1},{1,0},{2,3},{3,2},{4,5},{5,4},{6,7},{7,6},{8,9},{9,8},{10,11... | collective-permute-start | bytes 786440 | tf_op jit(solution)/shard_map/ppermute | solution.py:425
  60.4 1.0 shard_map.145.refs_4_
  61.4 1.8 %collective-permute-start.23 = (bf16[128,1024]{1,0:T(8,128)(2,1)S(1)}, bf16[128,1024]{1,0:T(8,128)(2,1)S(1)}, u32[]{:S(2)}, u32[]{:S(2)}) collective-permute-start(bf16[128,1024]{1,0:T(8,128)(2,1)S(1)} %shard_map.145.refs_4_), channel_id=1, source_target_pairs={{0,2},{1,3},{2,0},{3,1},{4,6},{5,7},{6,4},{7,5},{8,10},{9,11},{10,... | collective-permute-start | bytes 786440 | tf_op jit(solution)/shard_map/ppermute | solution.py:425
  63.3 2.0 %collective-permute-done.38.refs_6_ = bf16[128,1024]{1,0:T(8,128)(2,1)S(1)} collective-permute-done((bf16[128,1024]{1,0:T(8,128)(2,1)S(1)}, bf16[128,1024]{1,0:T(8,128)(2,1)S(1)}, u32[]{:S(2)}, u32[]{:S(2)}) %collective-permute-start.38) | collective-permute-done | bytes 262176 | tf_op jit(solution)/shard_map/ppermute | solution.py:425
  66.1 1.5 collective-permute-start.35
  67.6 4.1 %collective-permute-done.37.refs_5_ = bf16[128,1024]{1,0:T(8,128)(2,1)S(1)} collective-permute-done((bf16[128,1024]{1,0:T(8,128)(2,1)S(1)}, bf16[128,1024]{1,0:T(8,128)(2,1)S(1)}, u32[]{:S(2)}, u32[]{:S(2)}) %collective-permute-start.37) | collective-permute-done | bytes 262176 | tf_op jit(solution)/shard_map/ppermute | solution.py:425
  71.7 1.5 collective-permute-start.20
  73.2 1.6 %collective-permute-start.22 = (bf16[128,1024]{1,0:T(8,128)(2,1)S(1)}, bf16[128,1024]{1,0:T(8,128)(2,1)S(1)}, u32[]{:S(2)}, u32[]{:S(2)}) collective-permute-start(bf16[128,1024]{1,0:T(8,128)(2,1)S(1)} %shard_map.145.refs_4_), channel_id=1, source_target_pairs={{0,1},{1,0},{2,3},{3,2},{4,5},{5,4},{6,7},{7,6},{8,9},{9,8},{10,11... | collective-permute-start | bytes 786440 | tf_op jit(solution)/shard_map/ppermute | solution.py:425
  74.8 1.7 %collective-permute-done.23.refs_6_ = bf16[128,1024]{1,0:T(8,128)(2,1)S(1)} collective-permute-done((bf16[128,1024]{1,0:T(8,128)(2,1)S(1)}, bf16[128,1024]{1,0:T(8,128)(2,1)S(1)}, u32[]{:S(2)}, u32[]{:S(2)}) %collective-permute-start.23) | collective-permute-done | bytes 262176 | tf_op jit(solution)/shard_map/ppermute | solution.py:425
  77.3 4.8 %collective-permute-done.35.refs_3_ = bf16[128,1024]{1,0:T(8,128)(2,1)S(1)} collective-permute-done((bf16[128,1024]{1,0:T(8,128)(2,1)S(1)}, bf16[128,1024]{1,0:T(8,128)(2,1)S(1)}, u32[]{:S(2)}, u32[]{:S(2)}) %collective-permute-start.35) | collective-permute-done | bytes 262176 | tf_op jit(solution)/shard_map/ppermute | solution.py:425
  82.1 2.2 %copy-done.1 = bf16[1,4096,512]{2,1,0:T(8,128)(2,1)S(1)} copy-done((bf16[1,4096,512]{2,1,0:T(8,128)(2,1)S(1)}, bf16[1,4096,512]{2,1,0:T(8,128)(2,1)}, u32[]{:S(2)}) %copy-start.1) | copy-done | bytes 4194328
  84.3 3.8 %shard_map.151.refs_0_ = bf16[256,512]{1,0:T(8,128)(2,1)S(1)} custom-call(s32[3]{0:T(128)S(1)} %pad_add_fusion.where_ref, f32[4,1,1024]{2,1,0:T(1,128)S(1)} %bitcast.7, bf16[1,4096,512]{2,1,0:T(8,128)(2,1)S(1)} %copy-done, bf16[1,4096,512]{2,1,0:T(8,128)(2,1)S(1)} %copy-done.1, bf16[128,1024]{1,0:T(8,128)(2,1)S(1)} %shard_map.149.refs_0_, ...), custom_call_target="tpu_custom_call" | custom-call | tf_op jit(solution)/shard_map/pallas_call | solution.py:438
  88.2 0.5 collective-permute-start.42
  88.7 1.5 collective-permute-start.41
  90.2 1.5 collective-permute-start.40
  91.7 3.8 %shard_map.146.refs_0_ = bf16[256,512]{1,0:T(8,128)(2,1)S(1)} custom-call(s32[3]{0:T(128)S(1)} %pad_add_fusion.where_ref, f32[4,1,1024]{2,1,0:T(1,128)S(1)} %bitcast.8, bf16[1,4096,512]{2,1,0:T(8,128)(2,1)S(1)} %copy-done, bf16[1,4096,512]{2,1,0:T(8,128)(2,1)S(1)} %copy-done.1, bf16[128,1024]{1,0:T(8,128)(2,1)S(1)} %shard_map.144.refs_0_, ...), custom_call_target="tpu_custom_call" | custom-call | tf_op jit(solution)/shard_map/pallas_call | solution.py:438
  95.6 0.5 collective-permute-start.27
  96.1 1.5 collective-permute-start.26
  97.6 0.7 collective-permute-done.42.refs_3_
  98.4 0.8 collective-permute-start.25
  99.1 11.9 %shard_map.141 = (bf16[384,128]{1,0:T(8,128)(2,1)S(1)}, bf16[384,128]{1,0:T(8,128)(2,1)S(1)}, bf16[384,128]{1,0:T(8,128)(2,1)S(1)}, bf16[384,128]{1,0:T(8,128)(2,1)S(1)}) custom-call(s32[3]{0:T(128)S(1)} %pad_add_fusion.where_ref, f32[4]{0:T(128)S(1)} %copy-done.8, f32[1,128]{1,0:T(1,128)S(1)} %bitcast.9, bf16[384,384]{1,0:T(8,128)(2,1)S(1)} %get-tuple-element.18.refs_0_, ...), custom_call_target="tpu_custom_call" | custom-call | tf_op jit(solution)/shard_map/pallas_call | solution.py:438
  111.1 5.5 %collective-permute-start.11 = (bf16[384,128]{1,0:T(8,128)(2,1)S(1)}, bf16[384,128]{1,0:T(8,128)(2,1)S(1)}, u32[]{:S(2)}, u32[]{:S(2)}) collective-permute-start(bf16[384,128]{1,0:T(8,128)(2,1)S(1)} %get-tuple-element.24), channel_id=1, source_target_pairs={{0,16},{4,20},{8,24},{12,28},{16,0},{20,4},{24,8},{28,12},{1,17},{... | collective-permute-start | bytes 294920 | tf_op jit(solution)/shard_map/ppermute | solution.py:422
  116.6 1.5 collective-permute-start.12
  118.1 1.9 %shard_map.152 = (bf16[128,1024]{1,0:T(8,128)(2,1)S(1)}, bf16[128,1024]{1,0:T(8,128)(2,1)S(1)}) custom-call(s32[3]{0:T(128)S(1)} %pad_add_fusion.where_ref, bf16[1,2048,1024]{2,1,0:T(8,128)(2,1)S(1)} %copy-done.2, bf16[256,512]{1,0:T(8,128)(2,1)S(1)} %shard_map.151.refs_0_, bf16[256,512]{1,0:T(8,128)(2,1)S(1)} %collective-permute-done.40.refs_1_, ...), custom_call_target="tpu_custom_call" | custom-call | tf_op jit(solution)/shard_map/pallas_call | solution.py:438
  119.9 3.7 %collective-permute-done.11 = bf16[384,128]{1,0:T(8,128)(2,1)S(1)} collective-permute-done((bf16[384,128]{1,0:T(8,128)(2,1)S(1)}, bf16[384,128]{1,0:T(8,128)(2,1)S(1)}, u32[]{:S(2)}, u32[]{:S(2)}) %collective-permute-start.11) | collective-permute-done | bytes 98336 | tf_op jit(solution)/shard_map/ppermute | solution.py:422
  123.7 1.9 %shard_map.147 = (bf16[128,1024]{1,0:T(8,128)(2,1)S(1)}, bf16[128,1024]{1,0:T(8,128)(2,1)S(1)}) custom-call(s32[3]{0:T(128)S(1)} %pad_add_fusion.where_ref, bf16[1,2048,1024]{2,1,0:T(8,128)(2,1)S(1)} %copy-done.2, bf16[256,512]{1,0:T(8,128)(2,1)S(1)} %shard_map.146.refs_0_, bf16[256,512]{1,0:T(8,128)(2,1)S(1)} %collective-permute-done.25.refs_1_, ...), custom_call_target="tpu_custom_call" | custom-call | tf_op jit(solution)/shard_map/pallas_call | solution.py:438
  125.6 0.6 collective-permute-start.28
  126.2 1.7 %collective-permute-start.14 = (bf16[384,256]{1,0:T(8,128)(2,1)S(1)}, bf16[384,256]{1,0:T(8,128)(2,1)S(1)}, u32[]{:S(2)}, u32[]{:S(2)}) collective-permute-start(bf16[384,256]{1,0:T(8,128)(2,1)S(1)} %constant_dynamic-update-slice_fusion.2.refs_4_), channel_id=1, source_target_pairs={{0,2},{1,3},{2,0},{3,1},{4,6},{5,7},{6,4},{7,5},{8,10},{9,11},{10,... | collective-permute-start | bytes 589832 | tf_op jit(solution)/shard_map/ppermute | solution.py:425
  127.9 1.4 collective-permute-start.13
  129.3 1.3 collective-permute-start.9
  130.6 1.4 collective-permute-start.8
  132.0 1.5 shard_map.153
  133.5 0.6 collective-permute-start.44
  134.1 1.5 shard_map.148
  135.6 2.2 %collective-permute-start.45 = (bf16[128,1024]{1,0:T(8,128)(2,1)S(1)}, bf16[128,1024]{1,0:T(8,128)(2,1)S(1)}, u32[]{:S(2)}, u32[]{:S(2)}) collective-permute-start(bf16[128,1024]{1,0:T(8,128)(2,1)S(1)} %get-tuple-element.33), channel_id=1, source_target_pairs={{0,24},{4,28},{8,16},{12,20},{16,8},{20,12},{24,0},{28,4},{1,25},{... | collective-permute-start | bytes 786440 | tf_op jit(solution)/shard_map/ppermute | solution.py:422
  137.7 0.8 collective-permute-start.29
  138.6 0.7 collective-permute-start.15
  139.2 1.4 collective-permute-start.10
  140.6 3.6 %collective-permute-done.15.refs_7_ = bf16[384,256]{1,0:T(8,128)(2,1)S(1)} collective-permute-done((bf16[384,256]{1,0:T(8,128)(2,1)S(1)}, bf16[384,256]{1,0:T(8,128)(2,1)S(1)}, u32[]{:S(2)}, u32[]{:S(2)}) %collective-permute-start.15) | collective-permute-done | bytes 196640 | tf_op jit(solution)/shard_map/ppermute | solution.py:425
  144.2 0.7 collective-permute-done.10.refs_3_
  144.9 3.7 %shard_map.142 = bf16[384,1024]{1,0:T(8,128)(2,1)} custom-call(s32[3]{0:T(128)S(1)} %pad_add_fusion.where_ref, bf16[2048,1024]{1,0:T(8,128)(2,1)S(1)} %copy-done.3, bf16[384,256]{1,0:T(8,128)(2,1)S(1)} %constant_dynamic-update-slice_fusion.refs_0_, bf16[384,256]{1,0:T(8,128)(2,1)S(1)} %collective-permute-done.8.refs_1_, ...), custom_call_target="tpu_custom_call" | custom-call | tf_op jit(solution)/shard_map/pallas_call | solution.py:438
  148.6 4.5 %collective-permute-done.44 = bf16[128,1024]{1,0:T(8,128)(2,1)S(1)} collective-permute-done((bf16[128,1024]{1,0:T(8,128)(2,1)S(1)}, bf16[128,1024]{1,0:T(8,128)(2,1)S(1)}, u32[]{:S(2)}, u32[]{:S(2)}) %collective-permute-start.44) | collective-permute-done | bytes 262176 | tf_op jit(solution)/shard_map/ppermute | solution.py:422
  153.1 2.8 %collective-permute-done.29 = bf16[128,1024]{1,0:T(8,128)(2,1)S(1)} collective-permute-done((bf16[128,1024]{1,0:T(8,128)(2,1)S(1)}, bf16[128,1024]{1,0:T(8,128)(2,1)S(1)}, u32[]{:S(2)}, u32[]{:S(2)}) %collective-permute-start.29) | collective-permute-done | bytes 262176 | tf_op jit(solution)/shard_map/ppermute | solution.py:422
  155.9 0.9 add_convert_fusion
  (68 shorter events, 3.6 us)
Async XLA Ops:
  0.6 81.5 %copy-start.7 = (f32[4096]{0:T(1024)S(1)}, f32[4096]{0:T(1024)}, u32[]{:S(2)}) copy-start(f32[4096]{0:T(1024)} %param.20) | copy-start | bytes 49156
  1.6 12.8 %collective-permute-start.31 = (bf16[136,1024]{1,0:T(8,128)(2,1)S(1)}, bf16[136,1024]{1,0:T(8,128)(2,1)S(1)}, u32[]{:S(2)}, u32[]{:S(2)}) collective-permute-start(bf16[136,1024]{1,0:T(8,128)(2,1)S(1)} %shard_map.143.refs_0_), channel_id=1, source_target_pairs={{0,24},{4,28},{8,16},{12,20},{16,8},{20,12},{24,0},{28,4},{1,25},{... | collective-permute-start | bytes 835592 | tf_op jit(solution)/shard_map/ppermute | solution.py:422
  6.8 25.2 %collective-permute-start.30 = (bf16[136,1024]{1,0:T(8,128)(2,1)S(1)}, bf16[136,1024]{1,0:T(8,128)(2,1)S(1)}, u32[]{:S(2)}, u32[]{:S(2)}) collective-permute-start(bf16[136,1024]{1,0:T(8,128)(2,1)S(1)} %shard_map.143.refs_0_), channel_id=1, source_target_pairs={{0,16},{4,20},{8,24},{12,28},{16,0},{20,4},{24,8},{28,12},{1,17},{... | collective-permute-start | bytes 835592 | tf_op jit(solution)/shard_map/ppermute | solution.py:422
  6.8 27.4 %collective-permute-start.17 = (bf16[136,1024]{1,0:T(8,128)(2,1)S(1)}, bf16[136,1024]{1,0:T(8,128)(2,1)S(1)}, u32[]{:S(2)}, u32[]{:S(2)}) collective-permute-start(bf16[136,1024]{1,0:T(8,128)(2,1)S(1)} %shard_map.143.refs_0_), channel_id=1, source_target_pairs={{0,4},{4,0},{8,12},{12,8},{16,20},{20,16},{24,28},{28,24},{1,5},{5... | collective-permute-start | bytes 835592 | tf_op jit(solution)/shard_map/ppermute | solution.py:422
  6.8 27.4 %collective-permute-start.16 = (bf16[136,1024]{1,0:T(8,128)(2,1)S(1)}, bf16[136,1024]{1,0:T(8,128)(2,1)S(1)}, u32[]{:S(2)}, u32[]{:S(2)}) collective-permute-start(bf16[136,1024]{1,0:T(8,128)(2,1)S(1)} %shard_map.143.refs_0_), channel_id=1, source_target_pairs={{0,8},{4,12},{8,0},{12,4},{16,24},{20,28},{24,16},{28,20},{1,9},{5... | collective-permute-start | bytes 835592 | tf_op jit(solution)/shard_map/ppermute | solution.py:422
  7.4 74.7 %copy-start = (bf16[1,4096,512]{2,1,0:T(8,128)(2,1)S(1)}, bf16[1,4096,512]{2,1,0:T(8,128)(2,1)}, u32[]{:S(2)}) copy-start(bf16[1,4096,512]{2,1,0:T(8,128)(2,1)} %gate_ref.3) | copy-start | bytes 12582916
  7.5 1.1 copy-start.4
  8.6 1.1 copy-start.5
  9.8 1.0 copy-start.6
  11.6 23.2 %collective-permute-start = (bf16[384,384]{1,0:T(8,128)(2,1)S(1)}, bf16[384,384]{1,0:T(8,128)(2,1)S(1)}, u32[]{:S(2)}, u32[]{:S(2)}) collective-permute-start(bf16[384,384]{1,0:T(8,128)(2,1)S(1)} %get-tuple-element.19), channel_id=1, source_target_pairs={{0,8},{4,12},{8,0},{12,4},{16,24},{20,28},{24,16},{28,20},{1,9},{5... | collective-permute-start | bytes 884744 | tf_op jit(solution)/shard_map/ppermute | solution.py:422
  14.4 36.0 %collective-permute-start.1 = (bf16[384,384]{1,0:T(8,128)(2,1)S(1)}, bf16[384,384]{1,0:T(8,128)(2,1)S(1)}, u32[]{:S(2)}, u32[]{:S(2)}) collective-permute-start(bf16[384,384]{1,0:T(8,128)(2,1)S(1)} %get-tuple-element.20), channel_id=1, source_target_pairs={{0,16},{4,20},{8,24},{12,28},{16,0},{20,4},{24,8},{28,12},{1,17},{... | collective-permute-start | bytes 884744 | tf_op jit(solution)/shard_map/ppermute | solution.py:422
  32.0 19.9 %collective-permute-start.2 = (bf16[384,384]{1,0:T(8,128)(2,1)S(1)}, bf16[384,384]{1,0:T(8,128)(2,1)S(1)}, u32[]{:S(2)}, u32[]{:S(2)}) collective-permute-start(bf16[384,384]{1,0:T(8,128)(2,1)S(1)} %get-tuple-element.21), channel_id=1, source_target_pairs={{0,24},{4,28},{8,16},{12,20},{16,8},{20,12},{24,0},{28,4},{1,25},{... | collective-permute-start | bytes 884744 | tf_op jit(solution)/shard_map/ppermute | solution.py:422
  34.2 19.3 %collective-permute-start.36 = (bf16[136,1024]{1,0:T(8,128)(2,1)S(1)}, bf16[136,1024]{1,0:T(8,128)(2,1)S(1)}, u32[]{:S(2)}, u32[]{:S(2)}) collective-permute-start(bf16[136,1024]{1,0:T(8,128)(2,1)S(1)} %collective-permute-done.31.refs_0_.refs_1_), channel_id=1, source_target_pairs={{0,4},{4,0},{8,12},{12,8},{16,20},{20,16},{24,28},{28,24},{1,5},{5... | collective-permute-start | bytes 835592 | tf_op jit(solution)/shard_map/ppermute | solution.py:422
  34.2 19.3 %collective-permute-start.32 = (bf16[136,1024]{1,0:T(8,128)(2,1)S(1)}, bf16[136,1024]{1,0:T(8,128)(2,1)S(1)}, u32[]{:S(2)}, u32[]{:S(2)}) collective-permute-start(bf16[136,1024]{1,0:T(8,128)(2,1)S(1)} %collective-permute-done.30.refs_0_), channel_id=1, source_target_pairs={{0,4},{4,0},{8,12},{12,8},{16,20},{20,16},{24,28},{28,24},{1,5},{5... | collective-permute-start | bytes 835592 | tf_op jit(solution)/shard_map/ppermute | solution.py:422
  34.7 21.3 %collective-permute-start.3 = (bf16[384,384]{1,0:T(8,128)(2,1)S(1)}, bf16[384,384]{1,0:T(8,128)(2,1)S(1)}, u32[]{:S(2)}, u32[]{:S(2)}) collective-permute-start(bf16[384,384]{1,0:T(8,128)(2,1)S(1)} %get-tuple-element.18.refs_0_), channel_id=1, source_target_pairs={{0,4},{4,0},{8,12},{12,8},{16,20},{20,16},{24,28},{28,24},{1,5},{5... | collective-permute-start | bytes 884744 | tf_op jit(solution)/shard_map/ppermute | solution.py:422
  50.4 6.4 %collective-permute-start.19 = (bf16[128,1024]{1,0:T(8,128)(2,1)S(1)}, bf16[128,1024]{1,0:T(8,128)(2,1)S(1)}, u32[]{:S(2)}, u32[]{:S(2)}) collective-permute-start(bf16[128,1024]{1,0:T(8,128)(2,1)S(1)} %shard_map.144.refs_0_), channel_id=1, source_target_pairs={{0,2},{1,3},{2,0},{3,1},{4,6},{5,7},{6,4},{7,5},{8,10},{9,11},{10,... | collective-permute-start | bytes 786440 | tf_op jit(solution)/shard_map/ppermute | solution.py:425
  52.0 6.4 %collective-permute-start.18 = (bf16[128,1024]{1,0:T(8,128)(2,1)S(1)}, bf16[128,1024]{1,0:T(8,128)(2,1)S(1)}, u32[]{:S(2)}, u32[]{:S(2)}) collective-permute-start(bf16[128,1024]{1,0:T(8,128)(2,1)S(1)} %shard_map.144.refs_0_), channel_id=1, source_target_pairs={{0,1},{1,0},{2,3},{3,2},{4,5},{5,4},{6,7},{7,6},{8,9},{9,8},{10,11... | collective-permute-start | bytes 786440 | tf_op jit(solution)/shard_map/ppermute | solution.py:425
  53.5 6.7 %collective-permute-start.21 = (bf16[136,1024]{1,0:T(8,128)(2,1)S(1)}, bf16[136,1024]{1,0:T(8,128)(2,1)S(1)}, u32[]{:S(2)}, u32[]{:S(2)}) collective-permute-start(bf16[136,1024]{1,0:T(8,128)(2,1)S(1)} %collective-permute-done.16.refs_0_.refs_1_), channel_id=1, source_target_pairs={{0,4},{4,0},{8,12},{12,8},{16,20},{20,16},{24,28},{28,24},{1,5},{5... | collective-permute-start | bytes 835592 | tf_op jit(solution)/shard_map/ppermute | solution.py:422
  53.5 8.0 %collective-permute-start.4 = (bf16[384,384]{1,0:T(8,128)(2,1)S(1)}, bf16[384,384]{1,0:T(8,128)(2,1)S(1)}, u32[]{:S(2)}, u32[]{:S(2)}) collective-permute-start(bf16[384,384]{1,0:T(8,128)(2,1)S(1)} %collective-permute-done.refs_1_), channel_id=1, source_target_pairs={{0,4},{4,0},{8,12},{12,8},{16,20},{20,16},{24,28},{28,24},{1,5},{5... | collective-permute-start | bytes 884744 | tf_op jit(solution)/shard_map/ppermute | solution.py:422
  56.0 9.2 %collective-permute-start.38 = (bf16[128,1024]{1,0:T(8,128)(2,1)S(1)}, bf16[128,1024]{1,0:T(8,128)(2,1)S(1)}, u32[]{:S(2)}, u32[]{:S(2)}) collective-permute-start(bf16[128,1024]{1,0:T(8,128)(2,1)S(1)} %shard_map.150.refs_4_), channel_id=1, source_target_pairs={{0,2},{1,3},{2,0},{3,1},{4,6},{5,7},{6,4},{7,5},{8,10},{9,11},{10,... | collective-permute-start | bytes 786440 | tf_op jit(solution)/shard_map/ppermute | solution.py:425
  56.9 9.2 %collective-permute-start.33 = (bf16[128,1024]{1,0:T(8,128)(2,1)S(1)}, bf16[128,1024]{1,0:T(8,128)(2,1)S(1)}, u32[]{:S(2)}, u32[]{:S(2)}) collective-permute-start(bf16[128,1024]{1,0:T(8,128)(2,1)S(1)} %shard_map.149.refs_0_), channel_id=1, source_target_pairs={{0,1},{1,0},{2,3},{3,2},{4,5},{5,4},{6,7},{7,6},{8,9},{9,8},{10,11... | collective-permute-start | bytes 786440 | tf_op jit(solution)/shard_map/ppermute | solution.py:425
  58.4 13.3 %collective-permute-start.37 = (bf16[128,1024]{1,0:T(8,128)(2,1)S(1)}, bf16[128,1024]{1,0:T(8,128)(2,1)S(1)}, u32[]{:S(2)}, u32[]{:S(2)}) collective-permute-start(bf16[128,1024]{1,0:T(8,128)(2,1)S(1)} %shard_map.150.refs_4_), channel_id=1, source_target_pairs={{0,1},{1,0},{2,3},{3,2},{4,5},{5,4},{6,7},{7,6},{8,9},{9,8},{10,11... | collective-permute-start | bytes 786440 | tf_op jit(solution)/shard_map/ppermute | solution.py:425
  60.2 13.0 %collective-permute-start.34 = (bf16[128,1024]{1,0:T(8,128)(2,1)S(1)}, bf16[128,1024]{1,0:T(8,128)(2,1)S(1)}, u32[]{:S(2)}, u32[]{:S(2)}) collective-permute-start(bf16[128,1024]{1,0:T(8,128)(2,1)S(1)} %shard_map.149.refs_0_), channel_id=1, source_target_pairs={{0,2},{1,3},{2,0},{3,1},{4,6},{5,7},{6,4},{7,5},{8,10},{9,11},{10,... | collective-permute-start | bytes 786440 | tf_op jit(solution)/shard_map/ppermute | solution.py:425
  61.4 15.0 %collective-permute-start.23 = (bf16[128,1024]{1,0:T(8,128)(2,1)S(1)}, bf16[128,1024]{1,0:T(8,128)(2,1)S(1)}, u32[]{:S(2)}, u32[]{:S(2)}) collective-permute-start(bf16[128,1024]{1,0:T(8,128)(2,1)S(1)} %shard_map.145.refs_4_), channel_id=1, source_target_pairs={{0,2},{1,3},{2,0},{3,1},{4,6},{5,7},{6,4},{7,5},{8,10},{9,11},{10,... | collective-permute-start | bytes 786440 | tf_op jit(solution)/shard_map/ppermute | solution.py:425
  65.2 12.0 %collective-permute-start.39 = (bf16[128,1024]{1,0:T(8,128)(2,1)S(1)}, bf16[128,1024]{1,0:T(8,128)(2,1)S(1)}, u32[]{:S(2)}, u32[]{:S(2)}) collective-permute-start(bf16[128,1024]{1,0:T(8,128)(2,1)S(1)} %collective-permute-done.38.refs_6_), channel_id=1, source_target_pairs={{0,1},{1,0},{2,3},{3,2},{4,5},{5,4},{6,7},{7,6},{8,9},{9,8},{10,11... | collective-permute-start | bytes 786440 | tf_op jit(solution)/shard_map/ppermute | solution.py:425
  66.1 16.0 %collective-permute-start.35 = (bf16[128,1024]{1,0:T(8,128)(2,1)S(1)}, bf16[128,1024]{1,0:T(8,128)(2,1)S(1)}, u32[]{:S(2)}, u32[]{:S(2)}) collective-permute-start(bf16[128,1024]{1,0:T(8,128)(2,1)S(1)} %collective-permute-done.33.refs_1_), channel_id=1, source_target_pairs={{0,2},{1,3},{2,0},{3,1},{4,6},{5,7},{6,4},{7,5},{8,10},{9,11},{10,... | collective-permute-start | bytes 786440 | tf_op jit(solution)/shard_map/ppermute | solution.py:425
  71.7 16.5 %collective-permute-start.20 = (bf16[128,1024]{1,0:T(8,128)(2,1)S(1)}, bf16[128,1024]{1,0:T(8,128)(2,1)S(1)}, u32[]{:S(2)}, u32[]{:S(2)}) collective-permute-start(bf16[128,1024]{1,0:T(8,128)(2,1)S(1)} %collective-permute-done.18.refs_1_), channel_id=1, source_target_pairs={{0,2},{1,3},{2,0},{3,1},{4,6},{5,7},{6,4},{7,5},{8,10},{9,11},{10,... | collective-permute-start | bytes 786440 | tf_op jit(solution)/shard_map/ppermute | solution.py:425
  73.2 15.5 %collective-permute-start.22 = (bf16[128,1024]{1,0:T(8,128)(2,1)S(1)}, bf16[128,1024]{1,0:T(8,128)(2,1)S(1)}, u32[]{:S(2)}, u32[]{:S(2)}) collective-permute-start(bf16[128,1024]{1,0:T(8,128)(2,1)S(1)} %shard_map.145.refs_4_), channel_id=1, source_target_pairs={{0,1},{1,0},{2,3},{3,2},{4,5},{5,4},{6,7},{7,6},{8,9},{9,8},{10,11... | collective-permute-start | bytes 786440 | tf_op jit(solution)/shard_map/ppermute | solution.py:425
  76.5 13.8 %collective-permute-start.24 = (bf16[128,1024]{1,0:T(8,128)(2,1)S(1)}, bf16[128,1024]{1,0:T(8,128)(2,1)S(1)}, u32[]{:S(2)}, u32[]{:S(2)}) collective-permute-start(bf16[128,1024]{1,0:T(8,128)(2,1)S(1)} %collective-permute-done.23.refs_6_), channel_id=1, source_target_pairs={{0,1},{1,0},{2,3},{3,2},{4,5},{5,4},{6,7},{7,6},{8,9},{9,8},{10,11... | collective-permute-start | bytes 786440 | tf_op jit(solution)/shard_map/ppermute | solution.py:425
  77.3 18.3 %collective-permute-start.5 = (bf16[384,384]{1,0:T(8,128)(2,1)S(1)}, bf16[384,384]{1,0:T(8,128)(2,1)S(1)}, u32[]{:S(2)}, u32[]{:S(2)}) collective-permute-start(bf16[384,384]{1,0:T(8,128)(2,1)S(1)} %collective-permute-done.1.refs_2_), channel_id=1, source_target_pairs={{0,4},{4,0},{8,12},{12,8},{16,20},{20,16},{24,28},{28,24},{1,5},{5... | collective-permute-start | bytes 884744 | tf_op jit(solution)/shard_map/ppermute | solution.py:422
  82.1 14.0 %collective-permute-start.6 = (bf16[384,384]{1,0:T(8,128)(2,1)S(1)}, bf16[384,384]{1,0:T(8,128)(2,1)S(1)}, u32[]{:S(2)}, u32[]{:S(2)}) collective-permute-start(bf16[384,384]{1,0:T(8,128)(2,1)S(1)} %collective-permute-done.2.refs_3_), channel_id=1, source_target_pairs={{0,4},{4,0},{8,12},{12,8},{16,20},{20,16},{24,28},{28,24},{1,5},{5... | collective-permute-start | bytes 884744 | tf_op jit(solution)/shard_map/ppermute | solution.py:422
  82.1 2.2 %copy-start.1 = (bf16[1,4096,512]{2,1,0:T(8,128)(2,1)S(1)}, bf16[1,4096,512]{2,1,0:T(8,128)(2,1)}, u32[]{:S(2)}) copy-start(bf16[1,4096,512]{2,1,0:T(8,128)(2,1)} %up_ref.3) | copy-start | bytes 12582916
  88.1 11.0 %copy-start.8 = (f32[4]{0:T(128)S(1)}, f32[4]{0:T(128)}, u32[]{:S(2)}) copy-start(f32[4]{0:T(128)} %scale_ref.1) | copy-start | bytes 52
  88.1 11.0 %copy-start.9 = (f32[128]{0:T(128)S(1)}, f32[128]{0:T(128)}, u32[]{:S(2)}) copy-start(f32[128]{0:T(128)} %param.17) | copy-start | bytes 1540
  88.1 29.9 %copy-start.2 = (bf16[1,2048,1024]{2,1,0:T(8,128)(2,1)S(1)}, bf16[1,2048,1024]{2,1,0:T(8,128)(2,1)}, u32[]{:S(2)}) copy-start(bf16[1,2048,1024]{2,1,0:T(8,128)(2,1)} %w_ref.5) | copy-start | bytes 12582916
  88.2 10.2 %collective-permute-start.42 = (bf16[256,512]{1,0:T(8,128)(2,1)S(1)}, bf16[256,512]{1,0:T(8,128)(2,1)S(1)}, u32[]{:S(2)}, u32[]{:S(2)}) collective-permute-start(bf16[256,512]{1,0:T(8,128)(2,1)S(1)} %shard_map.151.refs_0_), channel_id=1, source_target_pairs={{0,3},{1,2},{2,1},{3,0},{4,7},{5,6},{6,5},{7,4},{8,11},{9,10},{10,... | collective-permute-start | bytes 786440 | tf_op jit(solution)/shard_map/ppermute | solution.py:425
  88.7 22.3 %collective-permute-start.41 = (bf16[256,512]{1,0:T(8,128)(2,1)S(1)}, bf16[256,512]{1,0:T(8,128)(2,1)S(1)}, u32[]{:S(2)}, u32[]{:S(2)}) collective-permute-start(bf16[256,512]{1,0:T(8,128)(2,1)S(1)} %shard_map.151.refs_0_), channel_id=1, source_target_pairs={{0,2},{1,3},{2,0},{3,1},{4,6},{5,7},{6,4},{7,5},{8,10},{9,11},{10,... | collective-permute-start | bytes 786440 | tf_op jit(solution)/shard_map/ppermute | solution.py:425
  90.2 26.3 %collective-permute-start.40 = (bf16[256,512]{1,0:T(8,128)(2,1)S(1)}, bf16[256,512]{1,0:T(8,128)(2,1)S(1)}, u32[]{:S(2)}, u32[]{:S(2)}) collective-permute-start(bf16[256,512]{1,0:T(8,128)(2,1)S(1)} %shard_map.151.refs_0_), channel_id=1, source_target_pairs={{0,1},{1,0},{2,3},{3,2},{4,5},{5,4},{6,7},{7,6},{8,9},{9,8},{10,11... | collective-permute-start | bytes 786440 | tf_op jit(solution)/shard_map/ppermute | solution.py:425
  95.6 28.1 %collective-permute-start.27 = (bf16[256,512]{1,0:T(8,128)(2,1)S(1)}, bf16[256,512]{1,0:T(8,128)(2,1)S(1)}, u32[]{:S(2)}, u32[]{:S(2)}) collective-permute-start(bf16[256,512]{1,0:T(8,128)(2,1)S(1)} %shard_map.146.refs_0_), channel_id=1, source_target_pairs={{0,3},{1,2},{2,1},{3,0},{4,7},{5,6},{6,5},{7,4},{8,11},{9,10},{10,... | collective-permute-start | bytes 786440 | tf_op jit(solution)/shard_map/ppermute | solution.py:425
  96.1 27.6 %collective-permute-start.26 = (bf16[256,512]{1,0:T(8,128)(2,1)S(1)}, bf16[256,512]{1,0:T(8,128)(2,1)S(1)}, u32[]{:S(2)}, u32[]{:S(2)}) collective-permute-start(bf16[256,512]{1,0:T(8,128)(2,1)S(1)} %shard_map.146.refs_0_), channel_id=1, source_target_pairs={{0,2},{1,3},{2,0},{3,1},{4,6},{5,7},{6,4},{7,5},{8,10},{9,11},{10,... | collective-permute-start | bytes 786440 | tf_op jit(solution)/shard_map/ppermute | solution.py:425
  98.4 25.4 %collective-permute-start.25 = (bf16[256,512]{1,0:T(8,128)(2,1)S(1)}, bf16[256,512]{1,0:T(8,128)(2,1)S(1)}, u32[]{:S(2)}, u32[]{:S(2)}) collective-permute-start(bf16[256,512]{1,0:T(8,128)(2,1)S(1)} %shard_map.146.refs_0_), channel_id=1, source_target_pairs={{0,1},{1,0},{2,3},{3,2},{4,5},{5,4},{6,7},{7,6},{8,9},{9,8},{10,11... | collective-permute-start | bytes 786440 | tf_op jit(solution)/shard_map/ppermute | solution.py:425
  111.1 12.6 %collective-permute-start.11 = (bf16[384,128]{1,0:T(8,128)(2,1)S(1)}, bf16[384,128]{1,0:T(8,128)(2,1)S(1)}, u32[]{:S(2)}, u32[]{:S(2)}) collective-permute-start(bf16[384,128]{1,0:T(8,128)(2,1)S(1)} %get-tuple-element.24), channel_id=1, source_target_pairs={{0,16},{4,20},{8,24},{12,28},{16,0},{20,4},{24,8},{28,12},{1,17},{... | collective-permute-start | bytes 294920 | tf_op jit(solution)/shard_map/ppermute | solution.py:422
  116.6 9.6 %collective-permute-start.12 = (bf16[384,128]{1,0:T(8,128)(2,1)S(1)}, bf16[384,128]{1,0:T(8,128)(2,1)S(1)}, u32[]{:S(2)}, u32[]{:S(2)}) collective-permute-start(bf16[384,128]{1,0:T(8,128)(2,1)S(1)} %get-tuple-element.25), channel_id=1, source_target_pairs={{0,24},{4,28},{8,16},{12,20},{16,8},{20,12},{24,0},{28,4},{1,25},{... | collective-permute-start | bytes 294920 | tf_op jit(solution)/shard_map/ppermute | solution.py:422
  119.9 25.0 %copy-start.3 = (bf16[2048,1024]{1,0:T(8,128)(2,1)S(1)}, bf16[2048,1024]{1,0:T(8,128)(2,1)}, u32[]{:S(2)}) copy-start(bf16[2048,1024]{1,0:T(8,128)(2,1)} %w_ref.3) | copy-start | bytes 12582916
  123.6 7.0 %collective-permute-start.43 = (bf16[128,1024]{1,0:T(8,128)(2,1)S(1)}, bf16[128,1024]{1,0:T(8,128)(2,1)S(1)}, u32[]{:S(2)}, u32[]{:S(2)}) collective-permute-start(bf16[128,1024]{1,0:T(8,128)(2,1)S(1)} %get-tuple-element.31), channel_id=1, source_target_pairs={{0,4},{4,0},{8,12},{12,8},{16,20},{20,16},{24,28},{28,24},{1,5},{5... | collective-permute-start | bytes 786440 | tf_op jit(solution)/shard_map/ppermute | solution.py:422
  123.6 5.6 %collective-permute-start.7 = (bf16[384,128]{1,0:T(8,128)(2,1)S(1)}, bf16[384,128]{1,0:T(8,128)(2,1)S(1)}, u32[]{:S(2)}, u32[]{:S(2)}) collective-permute-start(bf16[384,128]{1,0:T(8,128)(2,1)S(1)} %get-tuple-element.23), channel_id=1, source_target_pairs={{0,8},{4,12},{8,0},{12,4},{16,24},{20,28},{24,16},{28,20},{1,9},{5... | collective-permute-start | bytes 294920 | tf_op jit(solution)/shard_map/ppermute | solution.py:422
  125.6 7.8 %collective-permute-start.28 = (bf16[128,1024]{1,0:T(8,128)(2,1)S(1)}, bf16[128,1024]{1,0:T(8,128)(2,1)S(1)}, u32[]{:S(2)}, u32[]{:S(2)}) collective-permute-start(bf16[128,1024]{1,0:T(8,128)(2,1)S(1)} %get-tuple-element.27), channel_id=1, source_target_pairs={{0,4},{4,0},{8,12},{12,8},{16,20},{20,16},{24,28},{28,24},{1,5},{5... | collective-permute-start | bytes 786440 | tf_op jit(solution)/shard_map/ppermute | solution.py:422
  126.2 9.3 %collective-permute-start.14 = (bf16[384,256]{1,0:T(8,128)(2,1)S(1)}, bf16[384,256]{1,0:T(8,128)(2,1)S(1)}, u32[]{:S(2)}, u32[]{:S(2)}) collective-permute-start(bf16[384,256]{1,0:T(8,128)(2,1)S(1)} %constant_dynamic-update-slice_fusion.2.refs_4_), channel_id=1, source_target_pairs={{0,2},{1,3},{2,0},{3,1},{4,6},{5,7},{6,4},{7,5},{8,10},{9,11},{10,... | collective-permute-start | bytes 589832 | tf_op jit(solution)/shard_map/ppermute | solution.py:425
  127.9 9.8 %collective-permute-start.13 = (bf16[384,256]{1,0:T(8,128)(2,1)S(1)}, bf16[384,256]{1,0:T(8,128)(2,1)S(1)}, u32[]{:S(2)}, u32[]{:S(2)}) collective-permute-start(bf16[384,256]{1,0:T(8,128)(2,1)S(1)} %constant_dynamic-update-slice_fusion.2.refs_4_), channel_id=1, source_target_pairs={{0,1},{1,0},{2,3},{3,2},{4,5},{5,4},{6,7},{7,6},{8,9},{9,8},{10,11... | collective-permute-start | bytes 589832 | tf_op jit(solution)/shard_map/ppermute | solution.py:425
  129.3 9.3 %collective-permute-start.9 = (bf16[384,256]{1,0:T(8,128)(2,1)S(1)}, bf16[384,256]{1,0:T(8,128)(2,1)S(1)}, u32[]{:S(2)}, u32[]{:S(2)}) collective-permute-start(bf16[384,256]{1,0:T(8,128)(2,1)S(1)} %constant_dynamic-update-slice_fusion.refs_0_), channel_id=1, source_target_pairs={{0,2},{1,3},{2,0},{3,1},{4,6},{5,7},{6,4},{7,5},{8,10},{9,11},{10,... | collective-permute-start | bytes 589832 | tf_op jit(solution)/shard_map/ppermute | solution.py:425
  130.6 8.6 %collective-permute-start.8 = (bf16[384,256]{1,0:T(8,128)(2,1)S(1)}, bf16[384,256]{1,0:T(8,128)(2,1)S(1)}, u32[]{:S(2)}, u32[]{:S(2)}) collective-permute-start(bf16[384,256]{1,0:T(8,128)(2,1)S(1)} %constant_dynamic-update-slice_fusion.refs_0_), channel_id=1, source_target_pairs={{0,1},{1,0},{2,3},{3,2},{4,5},{5,4},{6,7},{7,6},{8,9},{9,8},{10,11... | collective-permute-start | bytes 589832 | tf_op jit(solution)/shard_map/ppermute | solution.py:425
  133.5 19.6 %collective-permute-start.44 = (bf16[128,1024]{1,0:T(8,128)(2,1)S(1)}, bf16[128,1024]{1,0:T(8,128)(2,1)S(1)}, u32[]{:S(2)}, u32[]{:S(2)}) collective-permute-start(bf16[128,1024]{1,0:T(8,128)(2,1)S(1)} %get-tuple-element.32), channel_id=1, source_target_pairs={{0,16},{4,20},{8,24},{12,28},{16,0},{20,4},{24,8},{28,12},{1,17},{... | collective-permute-start | bytes 786440 | tf_op jit(solution)/shard_map/ppermute | solution.py:422
  135.6 17.6 %collective-permute-start.45 = (bf16[128,1024]{1,0:T(8,128)(2,1)S(1)}, bf16[128,1024]{1,0:T(8,128)(2,1)S(1)}, u32[]{:S(2)}, u32[]{:S(2)}) collective-permute-start(bf16[128,1024]{1,0:T(8,128)(2,1)S(1)} %get-tuple-element.33), channel_id=1, source_target_pairs={{0,24},{4,28},{8,16},{12,20},{16,8},{20,12},{24,0},{28,4},{1,25},{... | collective-permute-start | bytes 786440 | tf_op jit(solution)/shard_map/ppermute | solution.py:422
  137.7 18.2 %collective-permute-start.29 = (bf16[128,1024]{1,0:T(8,128)(2,1)S(1)}, bf16[128,1024]{1,0:T(8,128)(2,1)S(1)}, u32[]{:S(2)}, u32[]{:S(2)}) collective-permute-start(bf16[128,1024]{1,0:T(8,128)(2,1)S(1)} %get-tuple-element.29), channel_id=1, source_target_pairs={{0,8},{4,12},{8,0},{12,4},{16,24},{20,28},{24,16},{28,20},{1,9},{5... | collective-permute-start | bytes 786440 | tf_op jit(solution)/shard_map/ppermute | solution.py:422
  138.6 5.7 %collective-permute-start.15 = (bf16[384,256]{1,0:T(8,128)(2,1)S(1)}, bf16[384,256]{1,0:T(8,128)(2,1)S(1)}, u32[]{:S(2)}, u32[]{:S(2)}) collective-permute-start(bf16[384,256]{1,0:T(8,128)(2,1)S(1)} %collective-permute-done.14.refs_6_), channel_id=1, source_target_pairs={{0,1},{1,0},{2,3},{3,2},{4,5},{5,4},{6,7},{7,6},{8,9},{9,8},{10,11... | collective-permute-start | bytes 589832 | tf_op jit(solution)/shard_map/ppermute | solution.py:425
  139.2 5.7 %collective-permute-start.10 = (bf16[384,256]{1,0:T(8,128)(2,1)S(1)}, bf16[384,256]{1,0:T(8,128)(2,1)S(1)}, u32[]{:S(2)}, u32[]{:S(2)}) collective-permute-start(bf16[384,256]{1,0:T(8,128)(2,1)S(1)} %collective-permute-done.8.refs_1_), channel_id=1, source_target_pairs={{0,2},{1,3},{2,0},{3,1},{4,6},{5,7},{6,4},{7,5},{8,10},{9,11},{10,... | collective-permute-start | bytes 589832 | tf_op jit(solution)/shard_map/ppermute | solution.py:425
where the time goes:
time: 157 us
  starting transfers between devices  63.4 us (40%)
  waiting for transfers between devices  50.3 us (32%)
  Pallas kernels  35.6 us (23%)
  local copies, waits for them, and re-layouts  5.59 us (4%)
    pallas_call x13, Pallas kernels, call(): pl.pallas_call(body, out_shape=out_shape if last else near_shapes(out_sha...  34.6 us
    ppermute x22, starting transfers between devices, over_ep(): return lax.ppermute(value, 'ep', pairs)  34.5 us
    ppermute x22, waiting for transfers between devices, over_ep(): return lax.ppermute(value, 'ep', pairs)  31.8 us
    ppermute x24, starting transfers between devices, over_tp(): lax.ppermute(value, 'tp', [(i, i ^ offset) for i in range(tp_devices)])  28.9 us
    ppermute x24, waiting for transfers between devices, over_tp(): lax.ppermute(value, 'tp', [(i, i ^ offset) for i in range(tp_devices)])  18.4 us
    unnamed x22, local copies, waits for them, and re-layouts  5.54 us
  transfers between devices with their start and end apart: 46, of which 16 were waited for; matrix products, arithmetic and copies ran while one was open for 0% of the time, Pallas kernels for 22%

commit v1 on v0

--- a/solution.py
+++ b/solution.py
@@ -150,10 +150,6 @@
     return pltpu.CompilerParams(vmem_limit_bytes=limit * 1024 * 1024)
 
 
-def near(value):
-    return pltpu.with_memory_space_constraint(value, pltpu.VMEM)
-
-
 def near_shapes(tree):
     return jax.tree.map(lambda leaf: pltpu.VMEM(leaf.shape, leaf.dtype), tree)
 
@@ -162,14 +158,24 @@
     return jax.ShapeDtypeStruct(shape, bf16)
 
 
-def pack_kernel(width, where_ref, q_ref, k_ref, v_ref, *outs):
+def pack_kernel(width, where_ref, q_ref, k_ref, v_ref, _, *refs):
+    outs, (queries, sems) = refs[:-2], refs[-2:]
     chip = where_ref[0]
     scale = (width // 2) ** (-0.5)
+    heads = [pl.ds(pl.multiple_of((chip ^ slot) * width, width), width) for slot in range(len(outs))]
+    copies = [pltpu.make_async_copy(q_ref, queries, sems.at[0])]
     for slot, out in enumerate(outs):
-        at = pl.ds(pl.multiple_of((chip ^ slot) * width, width), width)
-        out[:, 0:width] = (q_ref[:, at].astype(f32) * scale).astype(bf16)
-        out[:, width : 2 * width] = k_ref[:, at]
-        out[:, 2 * width : 3 * width] = v_ref[:, at]
+        for i, ref in ((1, k_ref), (2, v_ref)):
+            at = out.at[:, i * width : (i + 1) * width]
+            sem = sems.at[2 * slot + i]
+            copies.append(pltpu.make_async_copy(ref.at[:, heads[slot]], at, sem))
+    for copy in copies:
+        copy.start()
+    copies[0].wait()
+    for slot, out in enumerate(outs):
+        out[:, 0:width] = (queries[:, heads[slot]].astype(f32) * scale).astype(bf16)
+    for copy in copies[1:]:
+        copy.wait()
 
 
 def attention_kernel(chips, count, width, where_ref, scale_ref, gain_ref, *refs):
@@ -242,6 +248,10 @@
         outs[slot][...] = (
             mixed * lax.rsqrt(mean_sq + eps) * gain_ref[...] * head_factor
         ).astype(bf16)
+
+
+def fetch_kernel(value_ref, out):
+    out[...] = value_ref[0, 0:8, 0:128]
 
 
 def project_kernel(parts, groups, width, where_ref, w_ref, *refs):
@@ -434,15 +444,21 @@
     def spread_direct(value):
         return [value] + [over_tp(value, offset) for offset in range(1, tp_devices)]
 
-    def call(body, out_shape, *args, scratch=(), scalars=1, limit=8, last=False):
+    def call(body, out_shape, *args, scratch=(), scalars=1, limit=8, last=False, far=()):
+        far_spec = pl.BlockSpec(memory_space=pltpu.HBM)
+        specs = [vmem if i not in far else far_spec for i in range(len(args) - scalars)]
+        placed = [
+            pltpu.with_memory_space_constraint(value, pltpu.HBM if i in far else pltpu.VMEM)
+            for i, value in enumerate(args[scalars:])
+        ]
         return pl.pallas_call(
             body,
             out_shape=out_shape if last else near_shapes(out_shape),
-            in_specs=[smem] * scalars + [vmem] * (len(args) - scalars),
+            in_specs=[smem] * scalars + specs,
             out_specs=jax.tree.map(lambda _: vmem, out_shape),
             scratch_shapes=list(scratch),
             compiler_params=params(limit),
-        )(*args[:scalars], *[near(arg) for arg in args[scalars:]])
+        )(*args[:scalars], *placed)
 
     far = [
         pltpu.with_memory_space_constraint(value, pltpu.HBM)
@@ -463,13 +479,28 @@
     arrived = [packed] + [over_ep(packed, slot) for slot in range(1, chips)]
     swapped = [over_ep(part, 0, 1) for part in arrived]
 
-    packs = call(
+    fetched = [
+        call(fetch_kernel, sds(8, 128), value, scalars=0)
+        for value in (expert_gate, expert_up)
+    ]
+
+    packs = pl.pallas_call(
         functools.partial(pack_kernel, width),
-        [sds(count_a, 3 * width)] * chips,
+        out_shape=[pltpu.VMEM((count_a, 3 * width), bf16)] * chips,
+        in_specs=[smem] + [pl.BlockSpec(memory_space=pltpu.HBM)] * 3 + [vmem],
+        out_specs=[vmem] * chips,
+        scratch_shapes=[
+            pltpu.VMEM(query_rows.shape, bf16),
+            pltpu.SemaphoreType.DMA((2 * chips + 1,)),
+        ],
+        compiler_params=params(8),
+    )(
         where,
-        query_rows,
-        key_rows,
-        value_rows,
+        *[
+            pltpu.with_memory_space_constraint(value, pltpu.HBM)
+            for value in (query_rows, key_rows, value_rows)
+        ],
+        fetched[0],
     )
     mine = [packs[0]] + [over_ep(packs[slot], slot) for slot in range(1, chips)]
     theirs = [over_ep(part, 0, 1) for part in mine]
@@ -496,6 +527,7 @@
             expert_gate,
             expert_up,
             *pieces,
+            fetched[1],
             scratch=[pltpu.VMEM((total, model), bf16)],
             limit=16,
         )

time: 157 us -> 156 us (level)
  waiting for transfers between devices: 50.3 us -> 61.6 us
  starting transfers between devices: 63.4 us -> 52.2 us
  local copies, waits for them, and re-layouts: 5.59 us -> 2.31 us
    ppermute x22, starting transfers between devices: 34.5 us -> 22.2 us  [over_ep(): return lax.ppermute(value, 'ep', pairs)]
    ppermute x22, waiting for transfers between devices: 31.8 us -> 44.1 us  [over_ep(): return lax.ppermute(value, 'ep', pairs)]
    unnamed x22 -> x18, local copies, waits for them, and re-layouts: 5.54 us -> 2.26 us
    pallas_call x0 -> x1, Pallas kernels: none -> 2.2 us  [per_device_fast(): pl.pallas_call(functools.partial(pack_kernel, width), out_shape=[pltpu.VM...]
    pallas_call x13 -> x14, Pallas kernels: 34.6 us -> 33.6 us  [call(): pl.pallas_call(body, out_shape=out_shape if last else near_shapes(out_sha...]
  transfers between devices with their start and end apart: 46 -> 46, of which waited for: 16 -> 13; matrix products, arithmetic and copies ran while one was open for 0% -> 0% of each run, Pallas kernels for 22% -> 23%
where the time goes in v1:
time: 156 us; the launch traced here: 155 us
  waiting for transfers between devices  61.6 us (39%)
  starting transfers between devices  52.2 us (33%)
  Pallas kernels  36.8 us (24%)
  local copies, waits for them, and re-layouts  2.31 us (1%)
    ppermute x22, waiting for transfers between devices, over_ep(): return lax.ppermute(value, 'ep', pairs)  44.1 us
    pallas_call x14, Pallas kernels, call(): pl.pallas_call(body, out_shape=out_shape if last else near_shapes(out_sha...  33.6 us
    ppermute x24, starting transfers between devices, over_tp(): lax.ppermute(value, 'tp', [(i, i ^ offset) for i in range(tp_devices)])  30 us
    ppermute x22, starting transfers between devices, over_ep(): return lax.ppermute(value, 'ep', pairs)  22.2 us
    ppermute x24, waiting for transfers between devices, over_tp(): lax.ppermute(value, 'tp', [(i, i ^ offset) for i in range(tp_devices)])  17.5 us
  transfers between devices with their start and end apart: 46, of which 13 were waited for; matrix products, arithmetic and copies ran while one was open for 0% of the time, Pallas kernels for 23%

profile of v1, /device:TPU:0, one launch (start us, length us, event | category | flops | bytes accessed | tf_op | source)
XLA Modules:
  0.0 154.8 jit_solution(8102822385319732077)
XLA Ops:
  0.6 1.0 shard_map.144.refs_0_
  1.6 3.1 %collective-permute-start.16 = (bf16[136,1024]{1,0:T(8,128)(2,1)S(1)}, bf16[136,1024]{1,0:T(8,128)(2,1)S(1)}, u32[]{:S(2)}, u32[]{:S(2)}) collective-permute-start(bf16[136,1024]{1,0:T(8,128)(2,1)S(1)} %shard_map.144.refs_0_), channel_id=1, source_target_pairs={{0,8},{4,12},{8,0},{12,4},{16,24},{20,28},{24,16},{28,20},{1,9},{5... | collective-permute-start | bytes 835592 | tf_op jit(solution)/shard_map/ppermute | solution.py:432
  4.7 2.6 %collective-permute-start.30 = (bf16[136,1024]{1,0:T(8,128)(2,1)S(1)}, bf16[136,1024]{1,0:T(8,128)(2,1)S(1)}, u32[]{:S(2)}, u32[]{:S(2)}) collective-permute-start(bf16[136,1024]{1,0:T(8,128)(2,1)S(1)} %shard_map.144.refs_0_), channel_id=1, source_target_pairs={{0,16},{4,20},{8,24},{12,28},{16,0},{20,4},{24,8},{28,12},{1,17},{... | collective-permute-start | bytes 835592 | tf_op jit(solution)/shard_map/ppermute | solution.py:432
  7.3 2.2 %copy-done = bf16[1,4096,512]{2,1,0:T(8,128)(2,1)S(1)} copy-done((bf16[1,4096,512]{2,1,0:T(8,128)(2,1)S(1)}, bf16[1,4096,512]{2,1,0:T(8,128)(2,1)}, u32[]{:S(2)}) %copy-start) | copy-done | bytes 4194328
  9.6 2.2 %shard_map.141 = (bf16[384,384]{1,0:T(8,128)(2,1)S(1)}, bf16[384,384]{1,0:T(8,128)(2,1)S(1)}, bf16[384,384]{1,0:T(8,128)(2,1)S(1)}, bf16[384,384]{1,0:T(8,128)(2,1)S(1)}) custom-call(s32[3]{0:T(128)S(1)} %pad_add_fusion.where_ref, bf16[384,512]{1,0:T(8,128)(2,1)} %q_ref.1, bf16[384,512]{1,0:T(8,128)(2,1)} %k_ref.1, bf16[384,512]{1,0:T(8,128)(2,1)} %v_ref.1, ...), custom_call_target="tpu_custom_call" | custom-call | tf_op jit(solution)/shard_map/pallas_call | solution.py:487
  11.8 1.0 collective-permute-start
  12.8 4.4 %collective-permute-done.16.refs_0_.refs_1_ = bf16[136,1024]{1,0:T(8,128)(2,1)S(1)} collective-permute-done((bf16[136,1024]{1,0:T(8,128)(2,1)S(1)}, bf16[136,1024]{1,0:T(8,128)(2,1)S(1)}, u32[]{:S(2)}, u32[]{:S(2)}) %collective-permute-start.16) | collective-permute-done | bytes 278560 | tf_op jit(solution)/shard_map/ppermute | solution.py:432
  17.1 0.6 collective-permute-start.1
  17.7 1.9 %collective-permute-start.2 = (bf16[384,384]{1,0:T(8,128)(2,1)S(1)}, bf16[384,384]{1,0:T(8,128)(2,1)S(1)}, u32[]{:S(2)}, u32[]{:S(2)}) collective-permute-start(bf16[384,384]{1,0:T(8,128)(2,1)S(1)} %get-tuple-element.21), channel_id=1, source_target_pairs={{0,24},{4,28},{8,16},{12,20},{16,8},{20,12},{24,0},{28,4},{1,25},{... | collective-permute-start | bytes 884744 | tf_op jit(solution)/shard_map/ppermute | solution.py:432
  19.6 7.6 %collective-permute-done.30.refs_0_ = bf16[136,1024]{1,0:T(8,128)(2,1)S(1)} collective-permute-done((bf16[136,1024]{1,0:T(8,128)(2,1)S(1)}, bf16[136,1024]{1,0:T(8,128)(2,1)S(1)}, u32[]{:S(2)}, u32[]{:S(2)}) %collective-permute-start.30) | collective-permute-done | bytes 278560 | tf_op jit(solution)/shard_map/ppermute | solution.py:432
  27.2 0.5 collective-permute-start.21
  27.7 1.0 shard_map.145.refs_0_
  28.7 1.4 collective-permute-done.refs_1_
  30.1 1.5 collective-permute-start.18
  31.6 20.5 %collective-permute-done.1.refs_2_ = bf16[384,384]{1,0:T(8,128)(2,1)S(1)} collective-permute-done((bf16[384,384]{1,0:T(8,128)(2,1)S(1)}, bf16[384,384]{1,0:T(8,128)(2,1)S(1)}, u32[]{:S(2)}, u32[]{:S(2)}) %collective-permute-start.1) | collective-permute-done | bytes 294944 | tf_op jit(solution)/shard_map/ppermute | solution.py:432
  52.1 1.5 collective-permute-start.19
  54.2 1.0 shard_map.146.refs_4_
  55.2 0.6 collective-permute-start.20
  55.8 4.9 %collective-permute-done.19.refs_2_ = bf16[128,1024]{1,0:T(8,128)(2,1)S(1)} collective-permute-done((bf16[128,1024]{1,0:T(8,128)(2,1)S(1)}, bf16[128,1024]{1,0:T(8,128)(2,1)S(1)}, u32[]{:S(2)}, u32[]{:S(2)}) %collective-permute-start.19) | collective-permute-done | bytes 262176 | tf_op jit(solution)/shard_map/ppermute | solution.py:435
  60.7 2.1 %collective-permute-start.23 = (bf16[128,1024]{1,0:T(8,128)(2,1)S(1)}, bf16[128,1024]{1,0:T(8,128)(2,1)S(1)}, u32[]{:S(2)}, u32[]{:S(2)}) collective-permute-start(bf16[128,1024]{1,0:T(8,128)(2,1)S(1)} %shard_map.146.refs_4_), channel_id=1, source_target_pairs={{0,2},{1,3},{2,0},{3,1},{4,6},{5,7},{6,4},{7,5},{8,10},{9,11},{10,... | collective-permute-start | bytes 786440 | tf_op jit(solution)/shard_map/ppermute | solution.py:435
  62.8 1.5 collective-permute-start.22
  64.3 1.0 shard_map.151.refs_0_
  65.3 0.6 collective-permute-start.33
  65.9 1.0 shard_map.152.refs_4_
  67.0 2.0 %collective-permute-start.34 = (bf16[128,1024]{1,0:T(8,128)(2,1)S(1)}, bf16[128,1024]{1,0:T(8,128)(2,1)S(1)}, u32[]{:S(2)}, u32[]{:S(2)}) collective-permute-start(bf16[128,1024]{1,0:T(8,128)(2,1)S(1)} %shard_map.151.refs_0_), channel_id=1, source_target_pairs={{0,2},{1,3},{2,0},{3,1},{4,6},{5,7},{6,4},{7,5},{8,10},{9,11},{10,... | collective-permute-start | bytes 786440 | tf_op jit(solution)/shard_map/ppermute | solution.py:435
  69.0 2.9 %collective-permute-done.23.refs_6_ = bf16[128,1024]{1,0:T(8,128)(2,1)S(1)} collective-permute-done((bf16[128,1024]{1,0:T(8,128)(2,1)S(1)}, bf16[128,1024]{1,0:T(8,128)(2,1)S(1)}, u32[]{:S(2)}, u32[]{:S(2)}) %collective-permute-start.23) | collective-permute-done | bytes 262176 | tf_op jit(solution)/shard_map/ppermute | solution.py:435
  71.9 1.5 collective-permute-start.24
  73.4 0.5 collective-permute-start.37
  74.0 2.1 %collective-permute-start.35 = (bf16[128,1024]{1,0:T(8,128)(2,1)S(1)}, bf16[128,1024]{1,0:T(8,128)(2,1)S(1)}, u32[]{:S(2)}, u32[]{:S(2)}) collective-permute-start(bf16[128,1024]{1,0:T(8,128)(2,1)S(1)} %collective-permute-done.33.refs_1_), channel_id=1, source_target_pairs={{0,2},{1,3},{2,0},{3,1},{4,6},{5,7},{6,4},{7,5},{8,10},{9,11},{10,... | collective-permute-start | bytes 786440 | tf_op jit(solution)/shard_map/ppermute | solution.py:435
  76.1 1.5 collective-permute-done.38.refs_6_
  77.5 1.5 collective-permute-start.39
  79.0 4.1 %collective-permute-done.34.refs_2_ = bf16[128,1024]{1,0:T(8,128)(2,1)S(1)} collective-permute-done((bf16[128,1024]{1,0:T(8,128)(2,1)S(1)}, bf16[128,1024]{1,0:T(8,128)(2,1)S(1)}, u32[]{:S(2)}, u32[]{:S(2)}) %collective-permute-start.34) | collective-permute-done | bytes 262176 | tf_op jit(solution)/shard_map/ppermute | solution.py:435
  83.2 0.5 collective-permute-start.6
  83.7 3.7 %shard_map.148.refs_0_ = bf16[256,512]{1,0:T(8,128)(2,1)S(1)} custom-call(s32[3]{0:T(128)S(1)} %pad_add_fusion.where_ref, f32[4,1,1024]{2,1,0:T(1,128)S(1)} %bitcast.7, bf16[1,4096,512]{2,1,0:T(8,128)(2,1)S(1)} %copy-done.1, bf16[1,4096,512]{2,1,0:T(8,128)(2,1)S(1)} %copy-done.2, bf16[128,1024]{1,0:T(8,128)(2,1)S(1)} %shard_map.145.refs_0_, ...), custom_call_target="tpu_custom_call" | custom-call | tf_op jit(solution)/shard_map/pallas_call | solution.py:454
  87.4 1.6 %collective-permute-start.25 = (bf16[256,512]{1,0:T(8,128)(2,1)S(1)}, bf16[256,512]{1,0:T(8,128)(2,1)S(1)}, u32[]{:S(2)}, u32[]{:S(2)}) collective-permute-start(bf16[256,512]{1,0:T(8,128)(2,1)S(1)} %shard_map.148.refs_0_), channel_id=1, source_target_pairs={{0,1},{1,0},{2,3},{3,2},{4,5},{5,4},{6,7},{7,6},{8,9},{9,8},{10,11... | collective-permute-start | bytes 786440 | tf_op jit(solution)/shard_map/ppermute | solution.py:435
  89.0 2.1 %collective-permute-start.26 = (bf16[256,512]{1,0:T(8,128)(2,1)S(1)}, bf16[256,512]{1,0:T(8,128)(2,1)S(1)}, u32[]{:S(2)}, u32[]{:S(2)}) collective-permute-start(bf16[256,512]{1,0:T(8,128)(2,1)S(1)} %shard_map.148.refs_0_), channel_id=1, source_target_pairs={{0,2},{1,3},{2,0},{3,1},{4,6},{5,7},{6,4},{7,5},{8,10},{9,11},{10,... | collective-permute-start | bytes 786440 | tf_op jit(solution)/shard_map/ppermute | solution.py:435
  91.2 3.7 %shard_map.153.refs_0_ = bf16[256,512]{1,0:T(8,128)(2,1)S(1)} custom-call(s32[3]{0:T(128)S(1)} %pad_add_fusion.where_ref, f32[4,1,1024]{2,1,0:T(1,128)S(1)} %bitcast.8, bf16[1,4096,512]{2,1,0:T(8,128)(2,1)S(1)} %copy-done.1, bf16[1,4096,512]{2,1,0:T(8,128)(2,1)S(1)} %copy-done.2, bf16[128,1024]{1,0:T(8,128)(2,1)S(1)} %shard_map.151.refs_0_, ...), custom_call_target="tpu_custom_call" | custom-call | tf_op jit(solution)/shard_map/pallas_call | solution.py:454
  94.9 1.5 collective-permute-start.40
  96.4 2.0 %collective-permute-start.41 = (bf16[256,512]{1,0:T(8,128)(2,1)S(1)}, bf16[256,512]{1,0:T(8,128)(2,1)S(1)}, u32[]{:S(2)}, u32[]{:S(2)}) collective-permute-start(bf16[256,512]{1,0:T(8,128)(2,1)S(1)} %shard_map.153.refs_0_), channel_id=1, source_target_pairs={{0,2},{1,3},{2,0},{3,1},{4,6},{5,7},{6,4},{7,5},{8,10},{9,11},{10,... | collective-permute-start | bytes 786440 | tf_op jit(solution)/shard_map/ppermute | solution.py:435
  98.4 1.4 collective-permute-start.42
  99.7 11.9 %shard_map.142 = (bf16[384,128]{1,0:T(8,128)(2,1)S(1)}, bf16[384,128]{1,0:T(8,128)(2,1)S(1)}, bf16[384,128]{1,0:T(8,128)(2,1)S(1)}, bf16[384,128]{1,0:T(8,128)(2,1)S(1)}) custom-call(s32[3]{0:T(128)S(1)} %pad_add_fusion.where_ref, f32[4]{0:T(128)S(1)} %copy-done.6, f32[1,128]{1,0:T(1,128)S(1)} %bitcast.9, bf16[384,384]{1,0:T(8,128)(2,1)S(1)} %get-tuple-element.18.refs_0_, ...), custom_call_target="tpu_custom_call" | custom-call | tf_op jit(solution)/shard_map/pallas_call | solution.py:454
  111.7 4.9 %collective-permute-start.11 = (bf16[384,128]{1,0:T(8,128)(2,1)S(1)}, bf16[384,128]{1,0:T(8,128)(2,1)S(1)}, u32[]{:S(2)}, u32[]{:S(2)}) collective-permute-start(bf16[384,128]{1,0:T(8,128)(2,1)S(1)} %get-tuple-element.24), channel_id=1, source_target_pairs={{0,16},{4,20},{8,24},{12,28},{16,0},{20,4},{24,8},{28,12},{1,17},{... | collective-permute-start | bytes 294920 | tf_op jit(solution)/shard_map/ppermute | solution.py:432
  116.6 1.4 collective-permute-start.12
  118.0 1.9 %shard_map.149 = (bf16[128,1024]{1,0:T(8,128)(2,1)S(1)}, bf16[128,1024]{1,0:T(8,128)(2,1)S(1)}) custom-call(s32[3]{0:T(128)S(1)} %pad_add_fusion.where_ref, bf16[1,2048,1024]{2,1,0:T(8,128)(2,1)S(1)} %copy-done.3, bf16[256,512]{1,0:T(8,128)(2,1)S(1)} %shard_map.148.refs_0_, bf16[256,512]{1,0:T(8,128)(2,1)S(1)} %collective-permute-done.25.refs_1_, ...), custom_call_target="tpu_custom_call" | custom-call | tf_op jit(solution)/shard_map/pallas_call | solution.py:454
  119.9 1.3 collective-permute-done.11
  121.3 1.9 %shard_map.154 = (bf16[128,1024]{1,0:T(8,128)(2,1)S(1)}, bf16[128,1024]{1,0:T(8,128)(2,1)S(1)}) custom-call(s32[3]{0:T(128)S(1)} %pad_add_fusion.where_ref, bf16[1,2048,1024]{2,1,0:T(8,128)(2,1)S(1)} %copy-done.3, bf16[256,512]{1,0:T(8,128)(2,1)S(1)} %shard_map.153.refs_0_, bf16[256,512]{1,0:T(8,128)(2,1)S(1)} %collective-permute-done.40.refs_1_, ...), custom_call_target="tpu_custom_call" | custom-call | tf_op jit(solution)/shard_map/pallas_call | solution.py:454
  123.2 0.6 collective-permute-start.43
  123.8 0.6 collective-permute-start.14
  124.4 1.2 collective-permute-start.13
  125.5 0.9 collective-permute-done.7
  126.5 0.6 collective-permute-start.8
  127.1 1.2 collective-permute-start.9
  128.3 1.5 shard_map.150
  129.7 1.5 collective-permute-start.29
  131.3 1.5 shard_map.155
  132.7 1.9 %collective-permute-start.44 = (bf16[128,1024]{1,0:T(8,128)(2,1)S(1)}, bf16[128,1024]{1,0:T(8,128)(2,1)S(1)}, u32[]{:S(2)}, u32[]{:S(2)}) collective-permute-start(bf16[128,1024]{1,0:T(8,128)(2,1)S(1)} %get-tuple-element.32), channel_id=1, source_target_pairs={{0,16},{4,20},{8,24},{12,28},{16,0},{20,4},{24,8},{28,12},{1,17},{... | collective-permute-start | bytes 786440 | tf_op jit(solution)/shard_map/ppermute | solution.py:432
  134.7 1.1 collective-permute-start.45
  135.8 0.8 collective-permute-start.15
  136.6 1.5 collective-permute-start.10
  138.1 3.3 %collective-permute-done.15.refs_7_ = bf16[384,256]{1,0:T(8,128)(2,1)S(1)} collective-permute-done((bf16[384,256]{1,0:T(8,128)(2,1)S(1)}, bf16[384,256]{1,0:T(8,128)(2,1)S(1)}, u32[]{:S(2)}, u32[]{:S(2)}) %collective-permute-start.15) | collective-permute-done | bytes 196640 | tf_op jit(solution)/shard_map/ppermute | solution.py:435
  141.4 0.8 collective-permute-done.10.refs_3_
  142.3 3.7 %shard_map.143 = bf16[384,1024]{1,0:T(8,128)(2,1)} custom-call(s32[3]{0:T(128)S(1)} %pad_add_fusion.where_ref, bf16[2048,1024]{1,0:T(8,128)(2,1)S(1)} %copy-done.4, bf16[384,256]{1,0:T(8,128)(2,1)S(1)} %constant_dynamic-update-slice_fusion.refs_0_, bf16[384,256]{1,0:T(8,128)(2,1)S(1)} %collective-permute-done.8.refs_1_, ...), custom_call_target="tpu_custom_call" | custom-call | tf_op jit(solution)/shard_map/pallas_call | solution.py:454
  146.0 7.9 %collective-permute-done.44 = bf16[128,1024]{1,0:T(8,128)(2,1)S(1)} collective-permute-done((bf16[128,1024]{1,0:T(8,128)(2,1)S(1)}, bf16[128,1024]{1,0:T(8,128)(2,1)S(1)}, u32[]{:S(2)}, u32[]{:S(2)}) %collective-permute-start.44) | collective-permute-done | bytes 262176 | tf_op jit(solution)/shard_map/ppermute | solution.py:432
  153.9 0.9 add_convert_fusion
  (66 shorter events, 1.1 us)
Async XLA Ops:
  1.6 15.5 %collective-permute-start.16 = (bf16[136,1024]{1,0:T(8,128)(2,1)S(1)}, bf16[136,1024]{1,0:T(8,128)(2,1)S(1)}, u32[]{:S(2)}, u32[]{:S(2)}) collective-permute-start(bf16[136,1024]{1,0:T(8,128)(2,1)S(1)} %shard_map.144.refs_0_), channel_id=1, source_target_pairs={{0,8},{4,12},{8,0},{12,4},{16,24},{20,28},{24,16},{28,20},{1,9},{5... | collective-permute-start | bytes 835592 | tf_op jit(solution)/shard_map/ppermute | solution.py:432
  4.7 13.0 %collective-permute-start.17 = (bf16[136,1024]{1,0:T(8,128)(2,1)S(1)}, bf16[136,1024]{1,0:T(8,128)(2,1)S(1)}, u32[]{:S(2)}, u32[]{:S(2)}) collective-permute-start(bf16[136,1024]{1,0:T(8,128)(2,1)S(1)} %shard_map.144.refs_0_), channel_id=1, source_target_pairs={{0,4},{4,0},{8,12},{12,8},{16,20},{20,16},{24,28},{28,24},{1,5},{5... | collective-permute-start | bytes 835592 | tf_op jit(solution)/shard_map/ppermute | solution.py:432
  4.7 22.5 %collective-permute-start.30 = (bf16[136,1024]{1,0:T(8,128)(2,1)S(1)}, bf16[136,1024]{1,0:T(8,128)(2,1)S(1)}, u32[]{:S(2)}, u32[]{:S(2)}) collective-permute-start(bf16[136,1024]{1,0:T(8,128)(2,1)S(1)} %shard_map.144.refs_0_), channel_id=1, source_target_pairs={{0,16},{4,20},{8,24},{12,28},{16,0},{20,4},{24,8},{28,12},{1,17},{... | collective-permute-start | bytes 835592 | tf_op jit(solution)/shard_map/ppermute | solution.py:432
  7.3 19.9 %collective-permute-start.31 = (bf16[136,1024]{1,0:T(8,128)(2,1)S(1)}, bf16[136,1024]{1,0:T(8,128)(2,1)S(1)}, u32[]{:S(2)}, u32[]{:S(2)}) collective-permute-start(bf16[136,1024]{1,0:T(8,128)(2,1)S(1)} %shard_map.144.refs_0_), channel_id=1, source_target_pairs={{0,24},{4,28},{8,16},{12,20},{16,8},{20,12},{24,0},{28,4},{1,25},{... | collective-permute-start | bytes 835592 | tf_op jit(solution)/shard_map/ppermute | solution.py:432
  7.3 2.2 %copy-start = (bf16[1,4096,512]{2,1,0:T(8,128)(2,1)S(1)}, bf16[1,4096,512]{2,1,0:T(8,128)(2,1)}, u32[]{:S(2)}) copy-start(bf16[1,4096,512]{2,1,0:T(8,128)(2,1)} %gate_ref.3) | copy-start | bytes 12582916
  9.5 74.2 %copy-start.2 = (bf16[1,4096,512]{2,1,0:T(8,128)(2,1)S(1)}, bf16[1,4096,512]{2,1,0:T(8,128)(2,1)}, u32[]{:S(2)}) copy-start(bf16[1,4096,512]{2,1,0:T(8,128)(2,1)} %up_ref.3) | copy-start | bytes 12582916
  9.6 74.1 %copy-start.1 = (bf16[1,4096,512]{2,1,0:T(8,128)(2,1)S(1)}, bf16[1,4096,512]{2,1,0:T(8,128)(2,1)}, u32[]{:S(2)}) copy-start(bf16[1,4096,512]{2,1,0:T(8,128)(2,1)} %gate_ref.3) | copy-start | bytes 12582916
  9.6 74.1 %copy-start.5 = (f32[4096]{0:T(1024)S(1)}, f32[4096]{0:T(1024)}, u32[]{:S(2)}) copy-start(f32[4096]{0:T(1024)} %param.20) | copy-start | bytes 49156
  11.8 18.3 %collective-permute-start = (bf16[384,384]{1,0:T(8,128)(2,1)S(1)}, bf16[384,384]{1,0:T(8,128)(2,1)S(1)}, u32[]{:S(2)}, u32[]{:S(2)}) collective-permute-start(bf16[384,384]{1,0:T(8,128)(2,1)S(1)} %get-tuple-element.19), channel_id=1, source_target_pairs={{0,8},{4,12},{8,0},{12,4},{16,24},{20,28},{24,16},{28,20},{1,9},{5... | collective-permute-start | bytes 884744 | tf_op jit(solution)/shard_map/ppermute | solution.py:432
  17.1 35.0 %collective-permute-start.1 = (bf16[384,384]{1,0:T(8,128)(2,1)S(1)}, bf16[384,384]{1,0:T(8,128)(2,1)S(1)}, u32[]{:S(2)}, u32[]{:S(2)}) collective-permute-start(bf16[384,384]{1,0:T(8,128)(2,1)S(1)} %get-tuple-element.20), channel_id=1, source_target_pairs={{0,16},{4,20},{8,24},{12,28},{16,0},{20,4},{24,8},{28,12},{1,17},{... | collective-permute-start | bytes 884744 | tf_op jit(solution)/shard_map/ppermute | solution.py:432
  17.7 35.9 %collective-permute-start.2 = (bf16[384,384]{1,0:T(8,128)(2,1)S(1)}, bf16[384,384]{1,0:T(8,128)(2,1)S(1)}, u32[]{:S(2)}, u32[]{:S(2)}) collective-permute-start(bf16[384,384]{1,0:T(8,128)(2,1)S(1)} %get-tuple-element.21), channel_id=1, source_target_pairs={{0,24},{4,28},{8,16},{12,20},{16,8},{20,12},{24,0},{28,4},{1,25},{... | collective-permute-start | bytes 884744 | tf_op jit(solution)/shard_map/ppermute | solution.py:432
  27.2 26.5 %collective-permute-start.3 = (bf16[384,384]{1,0:T(8,128)(2,1)S(1)}, bf16[384,384]{1,0:T(8,128)(2,1)S(1)}, u32[]{:S(2)}, u32[]{:S(2)}) collective-permute-start(bf16[384,384]{1,0:T(8,128)(2,1)S(1)} %get-tuple-element.18.refs_0_), channel_id=1, source_target_pairs={{0,4},{4,0},{8,12},{12,8},{16,20},{20,16},{24,28},{28,24},{1,5},{5... | collective-permute-start | bytes 884744 | tf_op jit(solution)/shard_map/ppermute | solution.py:432
  27.2 27.0 %collective-permute-start.21 = (bf16[136,1024]{1,0:T(8,128)(2,1)S(1)}, bf16[136,1024]{1,0:T(8,128)(2,1)S(1)}, u32[]{:S(2)}, u32[]{:S(2)}) collective-permute-start(bf16[136,1024]{1,0:T(8,128)(2,1)S(1)} %collective-permute-done.16.refs_0_.refs_1_), channel_id=1, source_target_pairs={{0,4},{4,0},{8,12},{12,8},{16,20},{20,16},{24,28},{28,24},{1,5},{5... | collective-permute-start | bytes 835592 | tf_op jit(solution)/shard_map/ppermute | solution.py:432
  30.1 25.1 %collective-permute-start.18 = (bf16[128,1024]{1,0:T(8,128)(2,1)S(1)}, bf16[128,1024]{1,0:T(8,128)(2,1)S(1)}, u32[]{:S(2)}, u32[]{:S(2)}) collective-permute-start(bf16[128,1024]{1,0:T(8,128)(2,1)S(1)} %shard_map.145.refs_0_), channel_id=1, source_target_pairs={{0,1},{1,0},{2,3},{3,2},{4,5},{5,4},{6,7},{7,6},{8,9},{9,8},{10,11... | collective-permute-start | bytes 786440 | tf_op jit(solution)/shard_map/ppermute | solution.py:435
  52.1 8.6 %collective-permute-start.19 = (bf16[128,1024]{1,0:T(8,128)(2,1)S(1)}, bf16[128,1024]{1,0:T(8,128)(2,1)S(1)}, u32[]{:S(2)}, u32[]{:S(2)}) collective-permute-start(bf16[128,1024]{1,0:T(8,128)(2,1)S(1)} %shard_map.145.refs_0_), channel_id=1, source_target_pairs={{0,2},{1,3},{2,0},{3,1},{4,6},{5,7},{6,4},{7,5},{8,10},{9,11},{10,... | collective-permute-start | bytes 786440 | tf_op jit(solution)/shard_map/ppermute | solution.py:435
  53.6 9.2 %collective-permute-start.32 = (bf16[136,1024]{1,0:T(8,128)(2,1)S(1)}, bf16[136,1024]{1,0:T(8,128)(2,1)S(1)}, u32[]{:S(2)}, u32[]{:S(2)}) collective-permute-start(bf16[136,1024]{1,0:T(8,128)(2,1)S(1)} %collective-permute-done.30.refs_0_), channel_id=1, source_target_pairs={{0,4},{4,0},{8,12},{12,8},{16,20},{20,16},{24,28},{28,24},{1,5},{5... | collective-permute-start | bytes 835592 | tf_op jit(solution)/shard_map/ppermute | solution.py:432
  53.7 11.7 %collective-permute-start.36 = (bf16[136,1024]{1,0:T(8,128)(2,1)S(1)}, bf16[136,1024]{1,0:T(8,128)(2,1)S(1)}, u32[]{:S(2)}, u32[]{:S(2)}) collective-permute-start(bf16[136,1024]{1,0:T(8,128)(2,1)S(1)} %collective-permute-done.31.refs_0_.refs_1_), channel_id=1, source_target_pairs={{0,4},{4,0},{8,12},{12,8},{16,20},{20,16},{24,28},{28,24},{1,5},{5... | collective-permute-start | bytes 835592 | tf_op jit(solution)/shard_map/ppermute | solution.py:432
  54.2 12.8 %collective-permute-start.4 = (bf16[384,384]{1,0:T(8,128)(2,1)S(1)}, bf16[384,384]{1,0:T(8,128)(2,1)S(1)}, u32[]{:S(2)}, u32[]{:S(2)}) collective-permute-start(bf16[384,384]{1,0:T(8,128)(2,1)S(1)} %collective-permute-done.refs_1_), channel_id=1, source_target_pairs={{0,4},{4,0},{8,12},{12,8},{16,20},{20,16},{24,28},{28,24},{1,5},{5... | collective-permute-start | bytes 884744 | tf_op jit(solution)/shard_map/ppermute | solution.py:432
  55.2 11.8 %collective-permute-start.20 = (bf16[128,1024]{1,0:T(8,128)(2,1)S(1)}, bf16[128,1024]{1,0:T(8,128)(2,1)S(1)}, u32[]{:S(2)}, u32[]{:S(2)}) collective-permute-start(bf16[128,1024]{1,0:T(8,128)(2,1)S(1)} %collective-permute-done.18.refs_1_), channel_id=1, source_target_pairs={{0,2},{1,3},{2,0},{3,1},{4,6},{5,7},{6,4},{7,5},{8,10},{9,11},{10,... | collective-permute-start | bytes 786440 | tf_op jit(solution)/shard_map/ppermute | solution.py:435
  60.7 11.2 %collective-permute-start.23 = (bf16[128,1024]{1,0:T(8,128)(2,1)S(1)}, bf16[128,1024]{1,0:T(8,128)(2,1)S(1)}, u32[]{:S(2)}, u32[]{:S(2)}) collective-permute-start(bf16[128,1024]{1,0:T(8,128)(2,1)S(1)} %shard_map.146.refs_4_), channel_id=1, source_target_pairs={{0,2},{1,3},{2,0},{3,1},{4,6},{5,7},{6,4},{7,5},{8,10},{9,11},{10,... | collective-permute-start | bytes 786440 | tf_op jit(solution)/shard_map/ppermute | solution.py:435
  62.8 10.6 %collective-permute-start.22 = (bf16[128,1024]{1,0:T(8,128)(2,1)S(1)}, bf16[128,1024]{1,0:T(8,128)(2,1)S(1)}, u32[]{:S(2)}, u32[]{:S(2)}) collective-permute-start(bf16[128,1024]{1,0:T(8,128)(2,1)S(1)} %shard_map.146.refs_4_), channel_id=1, source_target_pairs={{0,1},{1,0},{2,3},{3,2},{4,5},{5,4},{6,7},{7,6},{8,9},{9,8},{10,11... | collective-permute-start | bytes 786440 | tf_op jit(solution)/shard_map/ppermute | solution.py:435
  65.3 8.6 %collective-permute-start.33 = (bf16[128,1024]{1,0:T(8,128)(2,1)S(1)}, bf16[128,1024]{1,0:T(8,128)(2,1)S(1)}, u32[]{:S(2)}, u32[]{:S(2)}) collective-permute-start(bf16[128,1024]{1,0:T(8,128)(2,1)S(1)} %shard_map.151.refs_0_), channel_id=1, source_target_pairs={{0,1},{1,0},{2,3},{3,2},{4,5},{5,4},{6,7},{7,6},{8,9},{9,8},{10,11... | collective-permute-start | bytes 786440 | tf_op jit(solution)/shard_map/ppermute | solution.py:435
  66.9 10.6 %collective-permute-start.38 = (bf16[128,1024]{1,0:T(8,128)(2,1)S(1)}, bf16[128,1024]{1,0:T(8,128)(2,1)S(1)}, u32[]{:S(2)}, u32[]{:S(2)}) collective-permute-start(bf16[128,1024]{1,0:T(8,128)(2,1)S(1)} %shard_map.152.refs_4_), channel_id=1, source_target_pairs={{0,2},{1,3},{2,0},{3,1},{4,6},{5,7},{6,4},{7,5},{8,10},{9,11},{10,... | collective-permute-start | bytes 786440 | tf_op jit(solution)/shard_map/ppermute | solution.py:435
  67.0 16.1 %collective-permute-start.34 = (bf16[128,1024]{1,0:T(8,128)(2,1)S(1)}, bf16[128,1024]{1,0:T(8,128)(2,1)S(1)}, u32[]{:S(2)}, u32[]{:S(2)}) collective-permute-start(bf16[128,1024]{1,0:T(8,128)(2,1)S(1)} %shard_map.151.refs_0_), channel_id=1, source_target_pairs={{0,2},{1,3},{2,0},{3,1},{4,6},{5,7},{6,4},{7,5},{8,10},{9,11},{10,... | collective-permute-start | bytes 786440 | tf_op jit(solution)/shard_map/ppermute | solution.py:435
  71.9 11.2 %collective-permute-start.24 = (bf16[128,1024]{1,0:T(8,128)(2,1)S(1)}, bf16[128,1024]{1,0:T(8,128)(2,1)S(1)}, u32[]{:S(2)}, u32[]{:S(2)}) collective-permute-start(bf16[128,1024]{1,0:T(8,128)(2,1)S(1)} %collective-permute-done.23.refs_6_), channel_id=1, source_target_pairs={{0,1},{1,0},{2,3},{3,2},{4,5},{5,4},{6,7},{7,6},{8,9},{9,8},{10,11... | collective-permute-start | bytes 786440 | tf_op jit(solution)/shard_map/ppermute | solution.py:435
  73.4 14.0 %collective-permute-start.37 = (bf16[128,1024]{1,0:T(8,128)(2,1)S(1)}, bf16[128,1024]{1,0:T(8,128)(2,1)S(1)}, u32[]{:S(2)}, u32[]{:S(2)}) collective-permute-start(bf16[128,1024]{1,0:T(8,128)(2,1)S(1)} %shard_map.152.refs_4_), channel_id=1, source_target_pairs={{0,1},{1,0},{2,3},{3,2},{4,5},{5,4},{6,7},{7,6},{8,9},{9,8},{10,11... | collective-permute-start | bytes 786440 | tf_op jit(solution)/shard_map/ppermute | solution.py:435
  74.0 15.0 %collective-permute-start.35 = (bf16[128,1024]{1,0:T(8,128)(2,1)S(1)}, bf16[128,1024]{1,0:T(8,128)(2,1)S(1)}, u32[]{:S(2)}, u32[]{:S(2)}) collective-permute-start(bf16[128,1024]{1,0:T(8,128)(2,1)S(1)} %collective-permute-done.33.refs_1_), channel_id=1, source_target_pairs={{0,2},{1,3},{2,0},{3,1},{4,6},{5,7},{6,4},{7,5},{8,10},{9,11},{10,... | collective-permute-start | bytes 786440 | tf_op jit(solution)/shard_map/ppermute | solution.py:435
  77.5 13.6 %collective-permute-start.39 = (bf16[128,1024]{1,0:T(8,128)(2,1)S(1)}, bf16[128,1024]{1,0:T(8,128)(2,1)S(1)}, u32[]{:S(2)}, u32[]{:S(2)}) collective-permute-start(bf16[128,1024]{1,0:T(8,128)(2,1)S(1)} %collective-permute-done.38.refs_6_), channel_id=1, source_target_pairs={{0,1},{1,0},{2,3},{3,2},{4,5},{5,4},{6,7},{7,6},{8,9},{9,8},{10,11... | collective-permute-start | bytes 786440 | tf_op jit(solution)/shard_map/ppermute | solution.py:435
  83.2 11.7 %collective-permute-start.5 = (bf16[384,384]{1,0:T(8,128)(2,1)S(1)}, bf16[384,384]{1,0:T(8,128)(2,1)S(1)}, u32[]{:S(2)}, u32[]{:S(2)}) collective-permute-start(bf16[384,384]{1,0:T(8,128)(2,1)S(1)} %collective-permute-done.1.refs_2_), channel_id=1, source_target_pairs={{0,4},{4,0},{8,12},{12,8},{16,20},{20,16},{24,28},{28,24},{1,5},{5... | collective-permute-start | bytes 884744 | tf_op jit(solution)/shard_map/ppermute | solution.py:432
  83.2 13.2 %collective-permute-start.6 = (bf16[384,384]{1,0:T(8,128)(2,1)S(1)}, bf16[384,384]{1,0:T(8,128)(2,1)S(1)}, u32[]{:S(2)}, u32[]{:S(2)}) collective-permute-start(bf16[384,384]{1,0:T(8,128)(2,1)S(1)} %collective-permute-done.2.refs_3_), channel_id=1, source_target_pairs={{0,4},{4,0},{8,12},{12,8},{16,20},{20,16},{24,28},{28,24},{1,5},{5... | collective-permute-start | bytes 884744 | tf_op jit(solution)/shard_map/ppermute | solution.py:432
  87.4 12.3 %copy-start.6 = (f32[4]{0:T(128)S(1)}, f32[4]{0:T(128)}, u32[]{:S(2)}) copy-start(f32[4]{0:T(128)} %scale_ref.1) | copy-start | bytes 52
  87.4 12.3 %copy-start.7 = (f32[128]{0:T(128)S(1)}, f32[128]{0:T(128)}, u32[]{:S(2)}) copy-start(f32[128]{0:T(128)} %param.17) | copy-start | bytes 1540
  87.4 30.6 %copy-start.3 = (bf16[1,2048,1024]{2,1,0:T(8,128)(2,1)S(1)}, bf16[1,2048,1024]{2,1,0:T(8,128)(2,1)}, u32[]{:S(2)}) copy-start(bf16[1,2048,1024]{2,1,0:T(8,128)(2,1)} %w_ref.5) | copy-start | bytes 12582916
  87.4 10.9 %collective-permute-start.25 = (bf16[256,512]{1,0:T(8,128)(2,1)S(1)}, bf16[256,512]{1,0:T(8,128)(2,1)S(1)}, u32[]{:S(2)}, u32[]{:S(2)}) collective-permute-start(bf16[256,512]{1,0:T(8,128)(2,1)S(1)} %shard_map.148.refs_0_), channel_id=1, source_target_pairs={{0,1},{1,0},{2,3},{3,2},{4,5},{5,4},{6,7},{7,6},{8,9},{9,8},{10,11... | collective-permute-start | bytes 786440 | tf_op jit(solution)/shard_map/ppermute | solution.py:435
  89.0 22.7 %collective-permute-start.26 = (bf16[256,512]{1,0:T(8,128)(2,1)S(1)}, bf16[256,512]{1,0:T(8,128)(2,1)S(1)}, u32[]{:S(2)}, u32[]{:S(2)}) collective-permute-start(bf16[256,512]{1,0:T(8,128)(2,1)S(1)} %shard_map.148.refs_0_), channel_id=1, source_target_pairs={{0,2},{1,3},{2,0},{3,1},{4,6},{5,7},{6,4},{7,5},{8,10},{9,11},{10,... | collective-permute-start | bytes 786440 | tf_op jit(solution)/shard_map/ppermute | solution.py:435
  91.1 25.5 %collective-permute-start.27 = (bf16[256,512]{1,0:T(8,128)(2,1)S(1)}, bf16[256,512]{1,0:T(8,128)(2,1)S(1)}, u32[]{:S(2)}, u32[]{:S(2)}) collective-permute-start(bf16[256,512]{1,0:T(8,128)(2,1)S(1)} %shard_map.148.refs_0_), channel_id=1, source_target_pairs={{0,3},{1,2},{2,1},{3,0},{4,7},{5,6},{6,5},{7,4},{8,11},{9,10},{10,... | collective-permute-start | bytes 786440 | tf_op jit(solution)/shard_map/ppermute | solution.py:435
  94.9 26.3 %collective-permute-start.40 = (bf16[256,512]{1,0:T(8,128)(2,1)S(1)}, bf16[256,512]{1,0:T(8,128)(2,1)S(1)}, u32[]{:S(2)}, u32[]{:S(2)}) collective-permute-start(bf16[256,512]{1,0:T(8,128)(2,1)S(1)} %shard_map.153.refs_0_), channel_id=1, source_target_pairs={{0,1},{1,0},{2,3},{3,2},{4,5},{5,4},{6,7},{7,6},{8,9},{9,8},{10,11... | collective-permute-start | bytes 786440 | tf_op jit(solution)/shard_map/ppermute | solution.py:435
  96.4 24.9 %collective-permute-start.41 = (bf16[256,512]{1,0:T(8,128)(2,1)S(1)}, bf16[256,512]{1,0:T(8,128)(2,1)S(1)}, u32[]{:S(2)}, u32[]{:S(2)}) collective-permute-start(bf16[256,512]{1,0:T(8,128)(2,1)S(1)} %shard_map.153.refs_0_), channel_id=1, source_target_pairs={{0,2},{1,3},{2,0},{3,1},{4,6},{5,7},{6,4},{7,5},{8,10},{9,11},{10,... | collective-permute-start | bytes 786440 | tf_op jit(solution)/shard_map/ppermute | solution.py:435
  98.4 22.9 %collective-permute-start.42 = (bf16[256,512]{1,0:T(8,128)(2,1)S(1)}, bf16[256,512]{1,0:T(8,128)(2,1)S(1)}, u32[]{:S(2)}, u32[]{:S(2)}) collective-permute-start(bf16[256,512]{1,0:T(8,128)(2,1)S(1)} %shard_map.153.refs_0_), channel_id=1, source_target_pairs={{0,3},{1,2},{2,1},{3,0},{4,7},{5,6},{6,5},{7,4},{8,11},{9,10},{10,... | collective-permute-start | bytes 786440 | tf_op jit(solution)/shard_map/ppermute | solution.py:435
  111.7 9.5 %collective-permute-start.11 = (bf16[384,128]{1,0:T(8,128)(2,1)S(1)}, bf16[384,128]{1,0:T(8,128)(2,1)S(1)}, u32[]{:S(2)}, u32[]{:S(2)}) collective-permute-start(bf16[384,128]{1,0:T(8,128)(2,1)S(1)} %get-tuple-element.24), channel_id=1, source_target_pairs={{0,16},{4,20},{8,24},{12,28},{16,0},{20,4},{24,8},{28,12},{1,17},{... | collective-permute-start | bytes 294920 | tf_op jit(solution)/shard_map/ppermute | solution.py:432
  116.6 7.2 %collective-permute-start.12 = (bf16[384,128]{1,0:T(8,128)(2,1)S(1)}, bf16[384,128]{1,0:T(8,128)(2,1)S(1)}, u32[]{:S(2)}, u32[]{:S(2)}) collective-permute-start(bf16[384,128]{1,0:T(8,128)(2,1)S(1)} %get-tuple-element.25), channel_id=1, source_target_pairs={{0,24},{4,28},{8,16},{12,20},{16,8},{20,12},{24,0},{28,4},{1,25},{... | collective-permute-start | bytes 294920 | tf_op jit(solution)/shard_map/ppermute | solution.py:432
  119.9 22.4 %copy-start.4 = (bf16[2048,1024]{1,0:T(8,128)(2,1)S(1)}, bf16[2048,1024]{1,0:T(8,128)(2,1)}, u32[]{:S(2)}) copy-start(bf16[2048,1024]{1,0:T(8,128)(2,1)} %w_ref.3) | copy-start | bytes 12582916
  121.2 5.9 %collective-permute-start.28 = (bf16[128,1024]{1,0:T(8,128)(2,1)S(1)}, bf16[128,1024]{1,0:T(8,128)(2,1)S(1)}, u32[]{:S(2)}, u32[]{:S(2)}) collective-permute-start(bf16[128,1024]{1,0:T(8,128)(2,1)S(1)} %get-tuple-element.27), channel_id=1, source_target_pairs={{0,4},{4,0},{8,12},{12,8},{16,20},{20,16},{24,28},{28,24},{1,5},{5... | collective-permute-start | bytes 786440 | tf_op jit(solution)/shard_map/ppermute | solution.py:432
  121.2 5.3 %collective-permute-start.7 = (bf16[384,128]{1,0:T(8,128)(2,1)S(1)}, bf16[384,128]{1,0:T(8,128)(2,1)S(1)}, u32[]{:S(2)}, u32[]{:S(2)}) collective-permute-start(bf16[384,128]{1,0:T(8,128)(2,1)S(1)} %get-tuple-element.23), channel_id=1, source_target_pairs={{0,8},{4,12},{8,0},{12,4},{16,24},{20,28},{24,16},{28,20},{1,9},{5... | collective-permute-start | bytes 294920 | tf_op jit(solution)/shard_map/ppermute | solution.py:432
  123.2 6.6 %collective-permute-start.43 = (bf16[128,1024]{1,0:T(8,128)(2,1)S(1)}, bf16[128,1024]{1,0:T(8,128)(2,1)S(1)}, u32[]{:S(2)}, u32[]{:S(2)}) collective-permute-start(bf16[128,1024]{1,0:T(8,128)(2,1)S(1)} %get-tuple-element.31), channel_id=1, source_target_pairs={{0,4},{4,0},{8,12},{12,8},{16,20},{20,16},{24,28},{28,24},{1,5},{5... | collective-permute-start | bytes 786440 | tf_op jit(solution)/shard_map/ppermute | solution.py:432
  123.8 8.9 %collective-permute-start.14 = (bf16[384,256]{1,0:T(8,128)(2,1)S(1)}, bf16[384,256]{1,0:T(8,128)(2,1)S(1)}, u32[]{:S(2)}, u32[]{:S(2)}) collective-permute-start(bf16[384,256]{1,0:T(8,128)(2,1)S(1)} %constant_dynamic-update-slice_fusion.2.refs_4_), channel_id=1, source_target_pairs={{0,2},{1,3},{2,0},{3,1},{4,6},{5,7},{6,4},{7,5},{8,10},{9,11},{10,... | collective-permute-start | bytes 589832 | tf_op jit(solution)/shard_map/ppermute | solution.py:435
  124.4 10.3 %collective-permute-start.13 = (bf16[384,256]{1,0:T(8,128)(2,1)S(1)}, bf16[384,256]{1,0:T(8,128)(2,1)S(1)}, u32[]{:S(2)}, u32[]{:S(2)}) collective-permute-start(bf16[384,256]{1,0:T(8,128)(2,1)S(1)} %constant_dynamic-update-slice_fusion.2.refs_4_), channel_id=1, source_target_pairs={{0,1},{1,0},{2,3},{3,2},{4,5},{5,4},{6,7},{7,6},{8,9},{9,8},{10,11... | collective-permute-start | bytes 589832 | tf_op jit(solution)/shard_map/ppermute | solution.py:435
  126.5 9.2 %collective-permute-start.8 = (bf16[384,256]{1,0:T(8,128)(2,1)S(1)}, bf16[384,256]{1,0:T(8,128)(2,1)S(1)}, u32[]{:S(2)}, u32[]{:S(2)}) collective-permute-start(bf16[384,256]{1,0:T(8,128)(2,1)S(1)} %constant_dynamic-update-slice_fusion.refs_0_), channel_id=1, source_target_pairs={{0,1},{1,0},{2,3},{3,2},{4,5},{5,4},{6,7},{7,6},{8,9},{9,8},{10,11... | collective-permute-start | bytes 589832 | tf_op jit(solution)/shard_map/ppermute | solution.py:435
  127.1 9.5 %collective-permute-start.9 = (bf16[384,256]{1,0:T(8,128)(2,1)S(1)}, bf16[384,256]{1,0:T(8,128)(2,1)S(1)}, u32[]{:S(2)}, u32[]{:S(2)}) collective-permute-start(bf16[384,256]{1,0:T(8,128)(2,1)S(1)} %constant_dynamic-update-slice_fusion.refs_0_), channel_id=1, source_target_pairs={{0,2},{1,3},{2,0},{3,1},{4,6},{5,7},{6,4},{7,5},{8,10},{9,11},{10,... | collective-permute-start | bytes 589832 | tf_op jit(solution)/shard_map/ppermute | solution.py:435
  129.7 16.2 %collective-permute-start.29 = (bf16[128,1024]{1,0:T(8,128)(2,1)S(1)}, bf16[128,1024]{1,0:T(8,128)(2,1)S(1)}, u32[]{:S(2)}, u32[]{:S(2)}) collective-permute-start(bf16[128,1024]{1,0:T(8,128)(2,1)S(1)} %get-tuple-element.29), channel_id=1, source_target_pairs={{0,8},{4,12},{8,0},{12,4},{16,24},{20,28},{24,16},{28,20},{1,9},{5... | collective-permute-start | bytes 786440 | tf_op jit(solution)/shard_map/ppermute | solution.py:432
  132.7 21.1 %collective-permute-start.44 = (bf16[128,1024]{1,0:T(8,128)(2,1)S(1)}, bf16[128,1024]{1,0:T(8,128)(2,1)S(1)}, u32[]{:S(2)}, u32[]{:S(2)}) collective-permute-start(bf16[128,1024]{1,0:T(8,128)(2,1)S(1)} %get-tuple-element.32), channel_id=1, source_target_pairs={{0,16},{4,20},{8,24},{12,28},{16,0},{20,4},{24,8},{28,12},{1,17},{... | collective-permute-start | bytes 786440 | tf_op jit(solution)/shard_map/ppermute | solution.py:432
  134.7 19.2 %collective-permute-start.45 = (bf16[128,1024]{1,0:T(8,128)(2,1)S(1)}, bf16[128,1024]{1,0:T(8,128)(2,1)S(1)}, u32[]{:S(2)}, u32[]{:S(2)}) collective-permute-start(bf16[128,1024]{1,0:T(8,128)(2,1)S(1)} %get-tuple-element.33), channel_id=1, source_target_pairs={{0,24},{4,28},{8,16},{12,20},{16,8},{20,12},{24,0},{28,4},{1,25},{... | collective-permute-start | bytes 786440 | tf_op jit(solution)/shard_map/ppermute | solution.py:432
  135.8 5.7 %collective-permute-start.15 = (bf16[384,256]{1,0:T(8,128)(2,1)S(1)}, bf16[384,256]{1,0:T(8,128)(2,1)S(1)}, u32[]{:S(2)}, u32[]{:S(2)}) collective-permute-start(bf16[384,256]{1,0:T(8,128)(2,1)S(1)} %collective-permute-done.14.refs_6_), channel_id=1, source_target_pairs={{0,1},{1,0},{2,3},{3,2},{4,5},{5,4},{6,7},{7,6},{8,9},{9,8},{10,11... | collective-permute-start | bytes 589832 | tf_op jit(solution)/shard_map/ppermute | solution.py:435
  136.6 5.7 %collective-permute-start.10 = (bf16[384,256]{1,0:T(8,128)(2,1)S(1)}, bf16[384,256]{1,0:T(8,128)(2,1)S(1)}, u32[]{:S(2)}, u32[]{:S(2)}) collective-permute-start(bf16[384,256]{1,0:T(8,128)(2,1)S(1)} %collective-permute-done.8.refs_1_), channel_id=1, source_target_pairs={{0,2},{1,3},{2,0},{3,1},{4,6},{5,7},{6,4},{7,5},{8,10},{9,11},{10,... | collective-permute-start | bytes 589832 | tf_op jit(solution)/shard_map/ppermute | solution.py:435

commit v2 on v1

--- a/solution.py
+++ b/solution.py
@@ -178,20 +178,22 @@
         copy.wait()
 
 
-def attention_kernel(chips, count, width, where_ref, scale_ref, gain_ref, *refs):
-    own, other = refs[:chips], refs[chips : 2 * chips]
-    outs = refs[2 * chips : 3 * chips]
-    keys, values, queries, scores, acc, row_max, row_sum = refs[3 * chips :]
-    chip, core = where_ref[0], where_ref[1]
-    half = width // 2
-    pair = 2 * count
-    for slot in range(chips):
-        at = chip ^ slot
+def fill_keys(chip, core, base, count, width, own, other, keys, values):
+    for slot in range(len(own)):
+        at = (chip ^ slot) - base
         for parity, part in ((core, own[slot]), (1 - core, other[slot])):
             rows = pl.ds(pl.multiple_of(parity * count, count), count)
             keys[at, rows] = part[:, width : 2 * width]
             values[at, rows] = part[:, 2 * width : 3 * width]
+
+
+def softmax_rows(rows, keys, values, queries, scores, state, upto, core, start=None):
+    acc, row_max, row_sum = state
+    count, width = rows.shape
+    half, pair = width // 2, 2 * count
     lane = lax.broadcasted_iota(jnp.int32, (count, width), 1)
+    queries[0:count] = jnp.where(lane < half, rows, jnp.zeros_like(rows))
+    queries[count:pair] = jnp.where(lane < half, jnp.zeros_like(rows), rows)
 
     def widest(block):
         best = block[:, 0:width]
@@ -206,42 +208,71 @@
 
     def weigh(number):
         top = row_max[...]
-        block = [
-            jnp.exp(scores[number, :, i : i + width] - top) for i in range(0, pair, width)
-        ]
+        block = [jnp.exp(scores[number, :, i : i + width] - top) for i in range(0, pair, width)]
         total = functools.reduce(jnp.add, block)
         weights = jnp.concatenate([part.astype(bf16) for part in block], axis=1)
         return total, jnp.dot(weights, values[number], preferred_element_type=f32)
 
-    for slot in range(chips):
-        last = chip ^ slot
-        rows = own[slot][:, 0:width]
-        queries[0:count] = jnp.where(lane < half, rows, jnp.zeros_like(rows))
-        queries[count:pair] = jnp.where(lane < half, jnp.zeros_like(rows), rows)
+    if start is None:
         allowed = lax.broadcasted_iota(jnp.int32, (pair, pair), 1) <= (
             lax.broadcasted_iota(jnp.int32, (pair, pair), 0) % count + core * count
         )
-        masked = jnp.where(allowed, products(last), neg_big)
-        scores[last] = masked
+        masked = jnp.where(allowed, products(upto), neg_big)
+        scores[upto] = masked
         row_max[...] = widest(masked)
-
-        @pl.loop(0, last)
-        def _(number):
-            block = products(number)
-            scores[number] = block
-            row_max[...] = jnp.maximum(row_max[...], widest(block))
-
-        row_max[...] = jnp.broadcast_to(
-            jnp.max(row_max[...], axis=-1, keepdims=True), row_max.shape
-        )
-        row_sum[...], acc[...] = weigh(last)
-
-        @pl.loop(0, last)
-        def _(number):
-            total, update = weigh(number)
-            row_sum[...] += total
-            acc[...] += update
-
+    else:
+        row_max[...] = start[1][...]
+
+    @pl.loop(0, upto)
+    def _(number):
+        block = products(number)
+        scores[number] = block
+        row_max[...] = jnp.maximum(row_max[...], widest(block))
+
+    row_max[...] = jnp.broadcast_to(
+        jnp.max(row_max[...], axis=-1, keepdims=True), row_max.shape
+    )
+    if start is None:
+        row_sum[...], acc[...] = weigh(upto)
+    else:
+        shrink = jnp.exp(start[1][...] - row_max[...])
+        acc[...] = start[0][...] * shrink
+        row_sum[...] = start[2][...] * shrink
+
+    @pl.loop(0, upto)
+    def _(number):
+        total, update = weigh(number)
+        row_sum[...] += total
+        acc[...] += update
+
+
+def near_attention_kernel(count, width, where_ref, *refs):
+    own, other, outs = refs[0:2], refs[2:4], refs[4:10]
+    keys, values, queries, scores = refs[10:]
+    chip, core = where_ref[0], where_ref[1]
+    base = chip // 2 * 2
+    fill_keys(chip, core, base, count, width, own, other, keys, values)
+    for slot in range(2):
+        state = outs[3 * slot : 3 * slot + 3]
+        last = (chip ^ slot) - base
+        rows = own[slot][:, 0:width]
+        softmax_rows(rows, keys, values, queries, scores, state, last, core)
+
+
+def attention_kernel(chips, count, width, where_ref, scale_ref, gain_ref, *refs):
+    own, other = refs[:chips], refs[chips : 2 * chips]
+    starts = refs[2 * chips : 2 * chips + 6]
+    outs = refs[2 * chips + 6 : 3 * chips + 6]
+    keys, values, queries, scores, acc, row_max, row_sum = refs[3 * chips + 6 :]
+    chip, core = where_ref[0], where_ref[1]
+    pair = 2 * count
+    fill_keys(chip, core, 0, count, width, own, other, keys, values)
+    for slot in range(chips):
+        start = starts[3 * slot : 3 * slot + 3] if slot < 2 else None
+        upto = chip // 2 * 2 if slot < 2 else chip ^ slot
+        rows = own[slot][:, 0:width]
+        state = (acc, row_max, row_sum)
+        softmax_rows(rows, keys, values, queries, scores, state, upto, core, start)
         maps = acc[...] / jnp.sum(row_sum[...], axis=-1, keepdims=True)
         mixed = maps[0:count] - scale_ref[chip] * maps[count:pair]
         mean_sq = jnp.mean(mixed * mixed, axis=-1, keepdims=True)
@@ -552,6 +583,21 @@
         for slot, part in zip(slots, mixed):
             mixes[slot] = over_ep(part, slot) if slot else part
 
+    pair_shape = (2 * count_a, width)
+    starts = call(
+        functools.partial(near_attention_kernel, count_a, width),
+        [jax.ShapeDtypeStruct(pair_shape, f32)] * 6,
+        where,
+        *mine[:2],
+        *theirs[:2],
+        limit=14,
+        scratch=[
+            pltpu.VMEM((2, *pair_shape), bf16),
+            pltpu.VMEM((2, *pair_shape), bf16),
+            pltpu.VMEM(pair_shape, bf16),
+            pltpu.VMEM((2, 2 * count_a, 2 * count_a), f32),
+        ],
+    )
     head_outs = call(
         functools.partial(attention_kernel, chips, count_a, width),
         [sds(count_a, width)] * chips,
@@ -560,16 +606,15 @@
         head_gain.reshape(1, width),
         *mine,
         *theirs,
+        *starts,
         scalars=2,
         limit=24,
         scratch=[
-            pltpu.VMEM((chips, 2 * count_a, width), bf16),
-            pltpu.VMEM((chips, 2 * count_a, width), bf16),
-            pltpu.VMEM((2 * count_a, width), bf16),
+            pltpu.VMEM((chips, *pair_shape), bf16),
+            pltpu.VMEM((chips, *pair_shape), bf16),
+            pltpu.VMEM(pair_shape, bf16),
             pltpu.VMEM((chips, 2 * count_a, 2 * count_a), f32),
-            pltpu.VMEM((2 * count_a, width), f32),
-            pltpu.VMEM((2 * count_a, width), f32),
-            pltpu.VMEM((2 * count_a, width), f32),
+            *[pltpu.VMEM(pair_shape, f32)] * 3,
         ],
     )
     back = [head_outs[0]] + [over_ep(head_outs[slot], slot) for slot in range(1, chips)]

time: 156 us -> 160 us (1.026)
  starting transfers between devices: 52.2 us -> 61.3 us
  waiting for transfers between devices: 61.6 us -> 55.7 us
  Pallas kernels: 36.8 us -> 38.7 us
    ppermute x24, starting transfers between devices: 30 us -> 34.8 us  [over_tp(): lax.ppermute(value, 'tp', [(i, i ^ offset) for i in range(tp_devices)])]
    ppermute x22, starting transfers between devices: 22.2 us -> 26.5 us  [over_ep(): return lax.ppermute(value, 'ep', pairs)]
    ppermute x24, waiting for transfers between devices: 17.5 us -> 13.5 us  [over_tp(): lax.ppermute(value, 'tp', [(i, i ^ offset) for i in range(tp_devices)])]
    pallas_call x14 -> x15, Pallas kernels: 33.6 us -> 35.5 us  [call(): pl.pallas_call(body, out_shape=out_shape if last else near_shapes(out_sha...]
    ppermute x22, waiting for transfers between devices: 44.1 us -> 42.2 us  [over_ep(): return lax.ppermute(value, 'ep', pairs)]
  transfers between devices with their start and end apart: 46 -> 46, of which waited for: 13 -> 12; matrix products, arithmetic and copies ran while one was open for 0% -> 0% of each run, Pallas kernels for 23% -> 24%
where the time goes in v2:
time: 160 us
  starting transfers between devices  61.3 us (38%)
  waiting for transfers between devices  55.7 us (35%)
  Pallas kernels  38.7 us (24%)
  local copies, waits for them, and re-layouts  2.31 us (1%)
    ppermute x22, waiting for transfers between devices, over_ep(): return lax.ppermute(value, 'ep', pairs)  42.2 us
    pallas_call x15, Pallas kernels, call(): pl.pallas_call(body, out_shape=out_shape if last else near_shapes(out_sha...  35.5 us
    ppermute x24, starting transfers between devices, over_tp(): lax.ppermute(value, 'tp', [(i, i ^ offset) for i in range(tp_devices)])  34.8 us
    ppermute x22, starting transfers between devices, over_ep(): return lax.ppermute(value, 'ep', pairs)  26.5 us
    ppermute x24, waiting for transfers between devices, over_tp(): lax.ppermute(value, 'tp', [(i, i ^ offset) for i in range(tp_devices)])  13.5 us
  transfers between devices with their start and end apart: 46, of which 12 were waited for; matrix products, arithmetic and copies ran while one was open for 0% of the time, Pallas kernels for 24%

profile of v2, /device:TPU:0, one launch (start us, length us, event | category | flops | bytes accessed | tf_op | source)
XLA Modules:
  0.0 160.0 jit_solution(5057944316194499184)
XLA Ops:
  0.6 1.0 shard_map.145.refs_0_
  1.6 4.1 %collective-permute-start.30 = (bf16[136,1024]{1,0:T(8,128)(2,1)S(1)}, bf16[136,1024]{1,0:T(8,128)(2,1)S(1)}, u32[]{:S(2)}, u32[]{:S(2)}) collective-permute-start(bf16[136,1024]{1,0:T(8,128)(2,1)S(1)} %shard_map.145.refs_0_), channel_id=1, source_target_pairs={{0,16},{4,20},{8,24},{12,28},{16,0},{20,4},{24,8},{28,12},{1,17},{... | collective-permute-start | bytes 835592 | tf_op jit(solution)/shard_map/ppermute | solution.py:463
  5.7 1.3 collective-permute-start.31
  7.3 2.2 %copy-done = bf16[1,4096,512]{2,1,0:T(8,128)(2,1)S(1)} copy-done((bf16[1,4096,512]{2,1,0:T(8,128)(2,1)S(1)}, bf16[1,4096,512]{2,1,0:T(8,128)(2,1)}, u32[]{:S(2)}) %copy-start) | copy-done | bytes 4194328
  9.6 2.2 %shard_map.141 = (bf16[384,384]{1,0:T(8,128)(2,1)S(1)}, bf16[384,384]{1,0:T(8,128)(2,1)S(1)}, bf16[384,384]{1,0:T(8,128)(2,1)S(1)}, bf16[384,384]{1,0:T(8,128)(2,1)S(1)}) custom-call(s32[3]{0:T(128)S(1)} %pad_add_fusion.where_ref, bf16[384,512]{1,0:T(8,128)(2,1)} %q_ref.1, bf16[384,512]{1,0:T(8,128)(2,1)} %k_ref.1, bf16[384,512]{1,0:T(8,128)(2,1)} %v_ref.1, ...), custom_call_target="tpu_custom_call" | custom-call | tf_op jit(solution)/shard_map/pallas_call | solution.py:518
  11.8 1.9 %collective-permute-start = (bf16[384,384]{1,0:T(8,128)(2,1)S(1)}, bf16[384,384]{1,0:T(8,128)(2,1)S(1)}, u32[]{:S(2)}, u32[]{:S(2)}) collective-permute-start(bf16[384,384]{1,0:T(8,128)(2,1)S(1)} %get-tuple-element.25), channel_id=1, source_target_pairs={{0,8},{4,12},{8,0},{12,4},{16,24},{20,28},{24,16},{28,20},{1,9},{5... | collective-permute-start | bytes 884744 | tf_op jit(solution)/shard_map/ppermute | solution.py:463
  13.7 11.6 %collective-permute-done.30.refs_0_ = bf16[136,1024]{1,0:T(8,128)(2,1)S(1)} collective-permute-done((bf16[136,1024]{1,0:T(8,128)(2,1)S(1)}, bf16[136,1024]{1,0:T(8,128)(2,1)S(1)}, u32[]{:S(2)}, u32[]{:S(2)}) %collective-permute-start.30) | collective-permute-done | bytes 278560 | tf_op jit(solution)/shard_map/ppermute | solution.py:463
  25.2 2.8 %collective-permute-start.2 = (bf16[384,384]{1,0:T(8,128)(2,1)S(1)}, bf16[384,384]{1,0:T(8,128)(2,1)S(1)}, u32[]{:S(2)}, u32[]{:S(2)}) collective-permute-start(bf16[384,384]{1,0:T(8,128)(2,1)S(1)} %get-tuple-element.27), channel_id=1, source_target_pairs={{0,24},{4,28},{8,16},{12,20},{16,8},{20,12},{24,0},{28,4},{1,25},{... | collective-permute-start | bytes 884744 | tf_op jit(solution)/shard_map/ppermute | solution.py:463
  28.0 0.5 collective-permute-start.32
  28.5 5.1 %collective-permute-done.refs_1_ = bf16[384,384]{1,0:T(8,128)(2,1)S(1)} collective-permute-done((bf16[384,384]{1,0:T(8,128)(2,1)S(1)}, bf16[384,384]{1,0:T(8,128)(2,1)S(1)}, u32[]{:S(2)}, u32[]{:S(2)}) %collective-permute-start) | collective-permute-done | bytes 294944 | tf_op jit(solution)/shard_map/ppermute | solution.py:463
  33.6 1.0 shard_map.146.refs_0_
  34.6 15.5 %collective-permute-done.1.refs_2_ = bf16[384,384]{1,0:T(8,128)(2,1)S(1)} collective-permute-done((bf16[384,384]{1,0:T(8,128)(2,1)S(1)}, bf16[384,384]{1,0:T(8,128)(2,1)S(1)}, u32[]{:S(2)}, u32[]{:S(2)}) %collective-permute-start.1) | collective-permute-done | bytes 294944 | tf_op jit(solution)/shard_map/ppermute | solution.py:463
  50.2 1.8 %collective-permute-start.18 = (bf16[128,1024]{1,0:T(8,128)(2,1)S(1)}, bf16[128,1024]{1,0:T(8,128)(2,1)S(1)}, u32[]{:S(2)}, u32[]{:S(2)}) collective-permute-start(bf16[128,1024]{1,0:T(8,128)(2,1)S(1)} %shard_map.146.refs_0_), channel_id=1, source_target_pairs={{0,1},{1,0},{2,3},{3,2},{4,5},{5,4},{6,7},{7,6},{8,9},{9,8},{10,11... | collective-permute-start | bytes 786440 | tf_op jit(solution)/shard_map/ppermute | solution.py:466
  52.0 1.5 collective-permute-start.19
  53.5 0.5 collective-permute-start.4
  54.0 1.0 shard_map.152.refs_0_
  55.0 0.6 collective-permute-start.33
  55.6 1.0 shard_map.153.refs_4_
  56.8 1.9 %collective-permute-start.38 = (bf16[128,1024]{1,0:T(8,128)(2,1)S(1)}, bf16[128,1024]{1,0:T(8,128)(2,1)S(1)}, u32[]{:S(2)}, u32[]{:S(2)}) collective-permute-start(bf16[128,1024]{1,0:T(8,128)(2,1)S(1)} %shard_map.153.refs_4_), channel_id=1, source_target_pairs={{0,2},{1,3},{2,0},{3,1},{4,6},{5,7},{6,4},{7,5},{8,10},{9,11},{10,... | collective-permute-start | bytes 786440 | tf_op jit(solution)/shard_map/ppermute | solution.py:466
  58.7 1.7 %collective-permute-start.34 = (bf16[128,1024]{1,0:T(8,128)(2,1)S(1)}, bf16[128,1024]{1,0:T(8,128)(2,1)S(1)}, u32[]{:S(2)}, u32[]{:S(2)}) collective-permute-start(bf16[128,1024]{1,0:T(8,128)(2,1)S(1)} %shard_map.152.refs_0_), channel_id=1, source_target_pairs={{0,2},{1,3},{2,0},{3,1},{4,6},{5,7},{6,4},{7,5},{8,10},{9,11},{10,... | collective-permute-start | bytes 786440 | tf_op jit(solution)/shard_map/ppermute | solution.py:466
  60.3 0.9 collective-permute-start.37
  61.2 1.0 shard_map.147.refs_4_
  62.3 2.0 %collective-permute-start.23 = (bf16[128,1024]{1,0:T(8,128)(2,1)S(1)}, bf16[128,1024]{1,0:T(8,128)(2,1)S(1)}, u32[]{:S(2)}, u32[]{:S(2)}) collective-permute-start(bf16[128,1024]{1,0:T(8,128)(2,1)S(1)} %shard_map.147.refs_4_), channel_id=1, source_target_pairs={{0,2},{1,3},{2,0},{3,1},{4,6},{5,7},{6,4},{7,5},{8,10},{9,11},{10,... | collective-permute-start | bytes 786440 | tf_op jit(solution)/shard_map/ppermute | solution.py:466
  64.3 0.5 collective-permute-start.35
  64.8 1.2 collective-permute-done.38.refs_6_
  66.0 2.4 %collective-permute-start.39 = (bf16[128,1024]{1,0:T(8,128)(2,1)S(1)}, bf16[128,1024]{1,0:T(8,128)(2,1)S(1)}, u32[]{:S(2)}, u32[]{:S(2)}) collective-permute-start(bf16[128,1024]{1,0:T(8,128)(2,1)S(1)} %collective-permute-done.38.refs_6_), channel_id=1, source_target_pairs={{0,1},{1,0},{2,3},{3,2},{4,5},{5,4},{6,7},{7,6},{8,9},{9,8},{10,11... | collective-permute-start | bytes 786440 | tf_op jit(solution)/shard_map/ppermute | solution.py:466
  68.3 3.3 %collective-permute-done.34.refs_2_ = bf16[128,1024]{1,0:T(8,128)(2,1)S(1)} collective-permute-done((bf16[128,1024]{1,0:T(8,128)(2,1)S(1)}, bf16[128,1024]{1,0:T(8,128)(2,1)S(1)}, u32[]{:S(2)}, u32[]{:S(2)}) %collective-permute-start.34) | collective-permute-done | bytes 262176 | tf_op jit(solution)/shard_map/ppermute | solution.py:466
  71.6 1.9 %collective-permute-start.20 = (bf16[128,1024]{1,0:T(8,128)(2,1)S(1)}, bf16[128,1024]{1,0:T(8,128)(2,1)S(1)}, u32[]{:S(2)}, u32[]{:S(2)}) collective-permute-start(bf16[128,1024]{1,0:T(8,128)(2,1)S(1)} %collective-permute-done.18.refs_1_), channel_id=1, source_target_pairs={{0,2},{1,3},{2,0},{3,1},{4,6},{5,7},{6,4},{7,5},{8,10},{9,11},{10,... | collective-permute-start | bytes 786440 | tf_op jit(solution)/shard_map/ppermute | solution.py:466
  73.5 2.5 %collective-permute-start.22 = (bf16[128,1024]{1,0:T(8,128)(2,1)S(1)}, bf16[128,1024]{1,0:T(8,128)(2,1)S(1)}, u32[]{:S(2)}, u32[]{:S(2)}) collective-permute-start(bf16[128,1024]{1,0:T(8,128)(2,1)S(1)} %shard_map.147.refs_4_), channel_id=1, source_target_pairs={{0,1},{1,0},{2,3},{3,2},{4,5},{5,4},{6,7},{7,6},{8,9},{9,8},{10,11... | collective-permute-start | bytes 786440 | tf_op jit(solution)/shard_map/ppermute | solution.py:466
  76.0 1.2 collective-permute-done.23.refs_6_
  77.2 2.4 %collective-permute-start.24 = (bf16[128,1024]{1,0:T(8,128)(2,1)S(1)}, bf16[128,1024]{1,0:T(8,128)(2,1)S(1)}, u32[]{:S(2)}, u32[]{:S(2)}) collective-permute-start(bf16[128,1024]{1,0:T(8,128)(2,1)S(1)} %collective-permute-done.23.refs_6_), channel_id=1, source_target_pairs={{0,1},{1,0},{2,3},{3,2},{4,5},{5,4},{6,7},{7,6},{8,9},{9,8},{10,11... | collective-permute-start | bytes 786440 | tf_op jit(solution)/shard_map/ppermute | solution.py:466
  79.6 3.3 %collective-permute-done.35.refs_3_ = bf16[128,1024]{1,0:T(8,128)(2,1)S(1)} collective-permute-done((bf16[128,1024]{1,0:T(8,128)(2,1)S(1)}, bf16[128,1024]{1,0:T(8,128)(2,1)S(1)}, u32[]{:S(2)}, u32[]{:S(2)}) %collective-permute-start.35) | collective-permute-done | bytes 262176 | tf_op jit(solution)/shard_map/ppermute | solution.py:466
  82.8 0.5 collective-permute-start.6
  83.3 3.7 %shard_map.154.refs_0_ = bf16[256,512]{1,0:T(8,128)(2,1)S(1)} custom-call(s32[3]{0:T(128)S(1)} %pad_add_fusion.where_ref, f32[4,1,1024]{2,1,0:T(1,128)S(1)} %bitcast.7, bf16[1,4096,512]{2,1,0:T(8,128)(2,1)S(1)} %copy-done.1, bf16[1,4096,512]{2,1,0:T(8,128)(2,1)S(1)} %copy-done.2, bf16[128,1024]{1,0:T(8,128)(2,1)S(1)} %shard_map.152.refs_0_, ...), custom_call_target="tpu_custom_call" | custom-call | tf_op jit(solution)/shard_map/pallas_call | solution.py:485
  87.2 2.3 %collective-permute-start.40 = (bf16[256,512]{1,0:T(8,128)(2,1)S(1)}, bf16[256,512]{1,0:T(8,128)(2,1)S(1)}, u32[]{:S(2)}, u32[]{:S(2)}) collective-permute-start(bf16[256,512]{1,0:T(8,128)(2,1)S(1)} %shard_map.154.refs_0_), channel_id=1, source_target_pairs={{0,1},{1,0},{2,3},{3,2},{4,5},{5,4},{6,7},{7,6},{8,9},{9,8},{10,11... | collective-permute-start | bytes 786440 | tf_op jit(solution)/shard_map/ppermute | solution.py:466
  89.5 1.2 collective-permute-start.41
  90.7 0.4 collective-permute-start.42
  91.0 3.7 %shard_map.149.refs_0_ = bf16[256,512]{1,0:T(8,128)(2,1)S(1)} custom-call(s32[3]{0:T(128)S(1)} %pad_add_fusion.where_ref, f32[4,1,1024]{2,1,0:T(1,128)S(1)} %bitcast.8, bf16[1,4096,512]{2,1,0:T(8,128)(2,1)S(1)} %copy-done.1, bf16[1,4096,512]{2,1,0:T(8,128)(2,1)S(1)} %copy-done.2, bf16[128,1024]{1,0:T(8,128)(2,1)S(1)} %shard_map.146.refs_0_, ...), custom_call_target="tpu_custom_call" | custom-call | tf_op jit(solution)/shard_map/pallas_call | solution.py:485
  94.8 2.0 %collective-permute-start.25 = (bf16[256,512]{1,0:T(8,128)(2,1)S(1)}, bf16[256,512]{1,0:T(8,128)(2,1)S(1)}, u32[]{:S(2)}, u32[]{:S(2)}) collective-permute-start(bf16[256,512]{1,0:T(8,128)(2,1)S(1)} %shard_map.149.refs_0_), channel_id=1, source_target_pairs={{0,1},{1,0},{2,3},{3,2},{4,5},{5,4},{6,7},{7,6},{8,9},{9,8},{10,11... | collective-permute-start | bytes 786440 | tf_op jit(solution)/shard_map/ppermute | solution.py:466
  96.8 1.2 collective-permute-start.26
  97.9 1.3 collective-permute-start.27
  99.3 4.3 %shard_map.142 = (f32[768,128]{1,0:T(8,128)S(1)}, f32[768,128]{1,0:T(8,128)S(1)}, f32[768,128]{1,0:T(8,128)S(1)}, f32[768,128]{1,0:T(8,128)S(1)}, f32[768,128]{1,0:T(8,128)S(1)}, /*index=5*/f32[768,128]{1,0:T(8,128)S(1)}) custom-call(s32[3]{0:T(128)S(1)} %pad_add_fusion.where_ref, bf16[384,384]{1,0:T(8,128)(2,1)S(1)} %get-tuple-element.24.refs_0_, ...), custom_call_target="tpu_custom_call" | custom-call | tf_op jit(solution)/shard_map/pallas_call | solution.py:485
  103.6 9.5 %shard_map.143 = (bf16[384,128]{1,0:T(8,128)(2,1)S(1)}, bf16[384,128]{1,0:T(8,128)(2,1)S(1)}, bf16[384,128]{1,0:T(8,128)(2,1)S(1)}, bf16[384,128]{1,0:T(8,128)(2,1)S(1)}) custom-call(s32[3]{0:T(128)S(1)} %pad_add_fusion.where_ref, f32[4]{0:T(128)S(1)} %copy-done.6, f32[1,128]{1,0:T(1,128)S(1)} %bitcast.9, bf16[384,384]{1,0:T(8,128)(2,1)S(1)} %get-tuple-element.24.refs_0_, ...), custom_call_target="tpu_custom_call" | custom-call | tf_op jit(solution)/shard_map/pallas_call | solution.py:485
  113.2 5.1 %collective-permute-start.7 = (bf16[384,128]{1,0:T(8,128)(2,1)S(1)}, bf16[384,128]{1,0:T(8,128)(2,1)S(1)}, u32[]{:S(2)}, u32[]{:S(2)}) collective-permute-start(bf16[384,128]{1,0:T(8,128)(2,1)S(1)} %get-tuple-element.35), channel_id=1, source_target_pairs={{0,8},{4,12},{8,0},{12,4},{16,24},{20,28},{24,16},{28,20},{1,9},{5... | collective-permute-start | bytes 294920 | tf_op jit(solution)/shard_map/ppermute | solution.py:463
  118.3 2.0 %collective-permute-start.11 = (bf16[384,128]{1,0:T(8,128)(2,1)S(1)}, bf16[384,128]{1,0:T(8,128)(2,1)S(1)}, u32[]{:S(2)}, u32[]{:S(2)}) collective-permute-start(bf16[384,128]{1,0:T(8,128)(2,1)S(1)} %get-tuple-element.36), channel_id=1, source_target_pairs={{0,16},{4,20},{8,24},{12,28},{16,0},{20,4},{24,8},{28,12},{1,17},{... | collective-permute-start | bytes 294920 | tf_op jit(solution)/shard_map/ppermute | solution.py:463
  120.3 1.9 %shard_map.155 = (bf16[128,1024]{1,0:T(8,128)(2,1)S(1)}, bf16[128,1024]{1,0:T(8,128)(2,1)S(1)}) custom-call(s32[3]{0:T(128)S(1)} %pad_add_fusion.where_ref, bf16[1,2048,1024]{2,1,0:T(8,128)(2,1)S(1)} %copy-done.3, bf16[256,512]{1,0:T(8,128)(2,1)S(1)} %shard_map.154.refs_0_, bf16[256,512]{1,0:T(8,128)(2,1)S(1)} %collective-permute-done.40.refs_1_, ...), custom_call_target="tpu_custom_call" | custom-call | tf_op jit(solution)/shard_map/pallas_call | solution.py:485
  122.3 2.9 %collective-permute-start.12 = (bf16[384,128]{1,0:T(8,128)(2,1)S(1)}, bf16[384,128]{1,0:T(8,128)(2,1)S(1)}, u32[]{:S(2)}, u32[]{:S(2)}) collective-permute-start(bf16[384,128]{1,0:T(8,128)(2,1)S(1)} %get-tuple-element.37), channel_id=1, source_target_pairs={{0,24},{4,28},{8,16},{12,20},{16,8},{20,12},{24,0},{28,4},{1,25},{... | collective-permute-start | bytes 294920 | tf_op jit(solution)/shard_map/ppermute | solution.py:463
  125.2 0.8 collective-permute-start.8
  126.0 1.5 collective-permute-start.9
  127.5 1.9 %shard_map.150 = (bf16[128,1024]{1,0:T(8,128)(2,1)S(1)}, bf16[128,1024]{1,0:T(8,128)(2,1)S(1)}) custom-call(s32[3]{0:T(128)S(1)} %pad_add_fusion.where_ref, bf16[1,2048,1024]{2,1,0:T(8,128)(2,1)S(1)} %copy-done.3, bf16[256,512]{1,0:T(8,128)(2,1)S(1)} %shard_map.149.refs_0_, bf16[256,512]{1,0:T(8,128)(2,1)S(1)} %collective-permute-done.25.refs_1_, ...), custom_call_target="tpu_custom_call" | custom-call | tf_op jit(solution)/shard_map/pallas_call | solution.py:485
  129.6 0.6 collective-permute-start.13
  130.2 1.5 collective-permute-start.14
  131.7 1.5 shard_map.156
  133.2 3.1 %collective-permute-start.45 = (bf16[128,1024]{1,0:T(8,128)(2,1)S(1)}, bf16[128,1024]{1,0:T(8,128)(2,1)S(1)}, u32[]{:S(2)}, u32[]{:S(2)}) collective-permute-start(bf16[128,1024]{1,0:T(8,128)(2,1)S(1)} %get-tuple-element.45), channel_id=1, source_target_pairs={{0,24},{4,28},{8,16},{12,20},{16,8},{20,12},{24,0},{28,4},{1,25},{... | collective-permute-start | bytes 786440 | tf_op jit(solution)/shard_map/ppermute | solution.py:463
  136.3 1.5 shard_map.151
  137.8 0.7 collective-permute-start.44
  138.5 0.7 collective-permute-start.29
  139.2 0.5 collective-permute-start.10
  139.7 1.4 collective-permute-start.15
  141.2 3.7 %collective-permute-done.10.refs_3_ = bf16[384,256]{1,0:T(8,128)(2,1)S(1)} collective-permute-done((bf16[384,256]{1,0:T(8,128)(2,1)S(1)}, bf16[384,256]{1,0:T(8,128)(2,1)S(1)}, u32[]{:S(2)}, u32[]{:S(2)}) %collective-permute-start.10) | collective-permute-done | bytes 196640 | tf_op jit(solution)/shard_map/ppermute | solution.py:466
  144.9 0.5 collective-permute-done.15.refs_7_
  145.4 3.7 %shard_map.144 = bf16[384,1024]{1,0:T(8,128)(2,1)} custom-call(s32[3]{0:T(128)S(1)} %pad_add_fusion.where_ref, bf16[2048,1024]{1,0:T(8,128)(2,1)S(1)} %copy-done.4, bf16[384,256]{1,0:T(8,128)(2,1)S(1)} %constant_dynamic-update-slice_fusion.refs_0_, bf16[384,256]{1,0:T(8,128)(2,1)S(1)} %collective-permute-done.8.refs_1_, ...), custom_call_target="tpu_custom_call" | custom-call | tf_op jit(solution)/shard_map/pallas_call | solution.py:485
  149.1 10.0 %collective-permute-done.44 = bf16[128,1024]{1,0:T(8,128)(2,1)S(1)} collective-permute-done((bf16[128,1024]{1,0:T(8,128)(2,1)S(1)}, bf16[128,1024]{1,0:T(8,128)(2,1)S(1)}, u32[]{:S(2)}, u32[]{:S(2)}) %collective-permute-start.44) | collective-permute-done | bytes 262176 | tf_op jit(solution)/shard_map/ppermute | solution.py:463
  159.1 0.9 add_convert_fusion
  (67 shorter events, 1.0 us)
Async XLA Ops:
  1.6 23.6 %collective-permute-start.30 = (bf16[136,1024]{1,0:T(8,128)(2,1)S(1)}, bf16[136,1024]{1,0:T(8,128)(2,1)S(1)}, u32[]{:S(2)}, u32[]{:S(2)}) collective-permute-start(bf16[136,1024]{1,0:T(8,128)(2,1)S(1)} %shard_map.145.refs_0_), channel_id=1, source_target_pairs={{0,16},{4,20},{8,24},{12,28},{16,0},{20,4},{24,8},{28,12},{1,17},{... | collective-permute-start | bytes 835592 | tf_op jit(solution)/shard_map/ppermute | solution.py:463
  5.7 19.5 %collective-permute-start.31 = (bf16[136,1024]{1,0:T(8,128)(2,1)S(1)}, bf16[136,1024]{1,0:T(8,128)(2,1)S(1)}, u32[]{:S(2)}, u32[]{:S(2)}) collective-permute-start(bf16[136,1024]{1,0:T(8,128)(2,1)S(1)} %shard_map.145.refs_0_), channel_id=1, source_target_pairs={{0,24},{4,28},{8,16},{12,20},{16,8},{20,12},{24,0},{28,4},{1,25},{... | collective-permute-start | bytes 835592 | tf_op jit(solution)/shard_map/ppermute | solution.py:463
  7.1 20.9 %collective-permute-start.16 = (bf16[136,1024]{1,0:T(8,128)(2,1)S(1)}, bf16[136,1024]{1,0:T(8,128)(2,1)S(1)}, u32[]{:S(2)}, u32[]{:S(2)}) collective-permute-start(bf16[136,1024]{1,0:T(8,128)(2,1)S(1)} %shard_map.145.refs_0_), channel_id=1, source_target_pairs={{0,8},{4,12},{8,0},{12,4},{16,24},{20,28},{24,16},{28,20},{1,9},{5... | collective-permute-start | bytes 835592 | tf_op jit(solution)/shard_map/ppermute | solution.py:463
  7.3 20.7 %collective-permute-start.17 = (bf16[136,1024]{1,0:T(8,128)(2,1)S(1)}, bf16[136,1024]{1,0:T(8,128)(2,1)S(1)}, u32[]{:S(2)}, u32[]{:S(2)}) collective-permute-start(bf16[136,1024]{1,0:T(8,128)(2,1)S(1)} %shard_map.145.refs_0_), channel_id=1, source_target_pairs={{0,4},{4,0},{8,12},{12,8},{16,20},{20,16},{24,28},{28,24},{1,5},{5... | collective-permute-start | bytes 835592 | tf_op jit(solution)/shard_map/ppermute | solution.py:463
  7.3 2.2 %copy-start = (bf16[1,4096,512]{2,1,0:T(8,128)(2,1)S(1)}, bf16[1,4096,512]{2,1,0:T(8,128)(2,1)}, u32[]{:S(2)}) copy-start(bf16[1,4096,512]{2,1,0:T(8,128)(2,1)} %gate_ref.3) | copy-start | bytes 12582916
  9.5 73.8 %copy-start.2 = (bf16[1,4096,512]{2,1,0:T(8,128)(2,1)S(1)}, bf16[1,4096,512]{2,1,0:T(8,128)(2,1)}, u32[]{:S(2)}) copy-start(bf16[1,4096,512]{2,1,0:T(8,128)(2,1)} %up_ref.3) | copy-start | bytes 12582916
  9.6 73.7 %copy-start.1 = (bf16[1,4096,512]{2,1,0:T(8,128)(2,1)S(1)}, bf16[1,4096,512]{2,1,0:T(8,128)(2,1)}, u32[]{:S(2)}) copy-start(bf16[1,4096,512]{2,1,0:T(8,128)(2,1)} %gate_ref.3) | copy-start | bytes 12582916
  9.6 73.7 %copy-start.5 = (f32[4096]{0:T(1024)S(1)}, f32[4096]{0:T(1024)}, u32[]{:S(2)}) copy-start(f32[4096]{0:T(1024)} %param.20) | copy-start | bytes 49156
  11.8 21.8 %collective-permute-start = (bf16[384,384]{1,0:T(8,128)(2,1)S(1)}, bf16[384,384]{1,0:T(8,128)(2,1)S(1)}, u32[]{:S(2)}, u32[]{:S(2)}) collective-permute-start(bf16[384,384]{1,0:T(8,128)(2,1)S(1)} %get-tuple-element.25), channel_id=1, source_target_pairs={{0,8},{4,12},{8,0},{12,4},{16,24},{20,28},{24,16},{28,20},{1,9},{5... | collective-permute-start | bytes 884744 | tf_op jit(solution)/shard_map/ppermute | solution.py:463
  25.2 24.9 %collective-permute-start.1 = (bf16[384,384]{1,0:T(8,128)(2,1)S(1)}, bf16[384,384]{1,0:T(8,128)(2,1)S(1)}, u32[]{:S(2)}, u32[]{:S(2)}) collective-permute-start(bf16[384,384]{1,0:T(8,128)(2,1)S(1)} %get-tuple-element.26), channel_id=1, source_target_pairs={{0,16},{4,20},{8,24},{12,28},{16,0},{20,4},{24,8},{28,12},{1,17},{... | collective-permute-start | bytes 884744 | tf_op jit(solution)/shard_map/ppermute | solution.py:463
  25.2 26.7 %collective-permute-start.2 = (bf16[384,384]{1,0:T(8,128)(2,1)S(1)}, bf16[384,384]{1,0:T(8,128)(2,1)S(1)}, u32[]{:S(2)}, u32[]{:S(2)}) collective-permute-start(bf16[384,384]{1,0:T(8,128)(2,1)S(1)} %get-tuple-element.27), channel_id=1, source_target_pairs={{0,24},{4,28},{8,16},{12,20},{16,8},{20,12},{24,0},{28,4},{1,25},{... | collective-permute-start | bytes 884744 | tf_op jit(solution)/shard_map/ppermute | solution.py:463
  28.0 25.5 %collective-permute-start.3 = (bf16[384,384]{1,0:T(8,128)(2,1)S(1)}, bf16[384,384]{1,0:T(8,128)(2,1)S(1)}, u32[]{:S(2)}, u32[]{:S(2)}) collective-permute-start(bf16[384,384]{1,0:T(8,128)(2,1)S(1)} %get-tuple-element.24.refs_0_), channel_id=1, source_target_pairs={{0,4},{4,0},{8,12},{12,8},{16,20},{20,16},{24,28},{28,24},{1,5},{5... | collective-permute-start | bytes 884744 | tf_op jit(solution)/shard_map/ppermute | solution.py:463
  28.0 25.5 %collective-permute-start.32 = (bf16[136,1024]{1,0:T(8,128)(2,1)S(1)}, bf16[136,1024]{1,0:T(8,128)(2,1)S(1)}, u32[]{:S(2)}, u32[]{:S(2)}) collective-permute-start(bf16[136,1024]{1,0:T(8,128)(2,1)S(1)} %collective-permute-done.30.refs_0_), channel_id=1, source_target_pairs={{0,4},{4,0},{8,12},{12,8},{16,20},{20,16},{24,28},{28,24},{1,5},{5... | collective-permute-start | bytes 835592 | tf_op jit(solution)/shard_map/ppermute | solution.py:463
  33.6 21.4 %collective-permute-start.36 = (bf16[136,1024]{1,0:T(8,128)(2,1)S(1)}, bf16[136,1024]{1,0:T(8,128)(2,1)S(1)}, u32[]{:S(2)}, u32[]{:S(2)}) collective-permute-start(bf16[136,1024]{1,0:T(8,128)(2,1)S(1)} %collective-permute-done.31.refs_0_.refs_1_), channel_id=1, source_target_pairs={{0,4},{4,0},{8,12},{12,8},{16,20},{20,16},{24,28},{28,24},{1,5},{5... | collective-permute-start | bytes 835592 | tf_op jit(solution)/shard_map/ppermute | solution.py:463
  50.2 6.6 %collective-permute-start.18 = (bf16[128,1024]{1,0:T(8,128)(2,1)S(1)}, bf16[128,1024]{1,0:T(8,128)(2,1)S(1)}, u32[]{:S(2)}, u32[]{:S(2)}) collective-permute-start(bf16[128,1024]{1,0:T(8,128)(2,1)S(1)} %shard_map.146.refs_0_), channel_id=1, source_target_pairs={{0,1},{1,0},{2,3},{3,2},{4,5},{5,4},{6,7},{7,6},{8,9},{9,8},{10,11... | collective-permute-start | bytes 786440 | tf_op jit(solution)/shard_map/ppermute | solution.py:466
  52.0 6.7 %collective-permute-start.19 = (bf16[128,1024]{1,0:T(8,128)(2,1)S(1)}, bf16[128,1024]{1,0:T(8,128)(2,1)S(1)}, u32[]{:S(2)}, u32[]{:S(2)}) collective-permute-start(bf16[128,1024]{1,0:T(8,128)(2,1)S(1)} %shard_map.146.refs_0_), channel_id=1, source_target_pairs={{0,2},{1,3},{2,0},{3,1},{4,6},{5,7},{6,4},{7,5},{8,10},{9,11},{10,... | collective-permute-start | bytes 786440 | tf_op jit(solution)/shard_map/ppermute | solution.py:466
  53.5 6.9 %collective-permute-start.21 = (bf16[136,1024]{1,0:T(8,128)(2,1)S(1)}, bf16[136,1024]{1,0:T(8,128)(2,1)S(1)}, u32[]{:S(2)}, u32[]{:S(2)}) collective-permute-start(bf16[136,1024]{1,0:T(8,128)(2,1)S(1)} %collective-permute-done.16.refs_0_.refs_1_), channel_id=1, source_target_pairs={{0,4},{4,0},{8,12},{12,8},{16,20},{20,16},{24,28},{28,24},{1,5},{5... | collective-permute-start | bytes 835592 | tf_op jit(solution)/shard_map/ppermute | solution.py:463
  53.5 8.8 %collective-permute-start.4 = (bf16[384,384]{1,0:T(8,128)(2,1)S(1)}, bf16[384,384]{1,0:T(8,128)(2,1)S(1)}, u32[]{:S(2)}, u32[]{:S(2)}) collective-permute-start(bf16[384,384]{1,0:T(8,128)(2,1)S(1)} %collective-permute-done.refs_1_), channel_id=1, source_target_pairs={{0,4},{4,0},{8,12},{12,8},{16,20},{20,16},{24,28},{28,24},{1,5},{5... | collective-permute-start | bytes 884744 | tf_op jit(solution)/shard_map/ppermute | solution.py:463
  55.0 9.3 %collective-permute-start.33 = (bf16[128,1024]{1,0:T(8,128)(2,1)S(1)}, bf16[128,1024]{1,0:T(8,128)(2,1)S(1)}, u32[]{:S(2)}, u32[]{:S(2)}) collective-permute-start(bf16[128,1024]{1,0:T(8,128)(2,1)S(1)} %shard_map.152.refs_0_), channel_id=1, source_target_pairs={{0,1},{1,0},{2,3},{3,2},{4,5},{5,4},{6,7},{7,6},{8,9},{9,8},{10,11... | collective-permute-start | bytes 786440 | tf_op jit(solution)/shard_map/ppermute | solution.py:466
  56.8 9.2 %collective-permute-start.38 = (bf16[128,1024]{1,0:T(8,128)(2,1)S(1)}, bf16[128,1024]{1,0:T(8,128)(2,1)S(1)}, u32[]{:S(2)}, u32[]{:S(2)}) collective-permute-start(bf16[128,1024]{1,0:T(8,128)(2,1)S(1)} %shard_map.153.refs_4_), channel_id=1, source_target_pairs={{0,2},{1,3},{2,0},{3,1},{4,6},{5,7},{6,4},{7,5},{8,10},{9,11},{10,... | collective-permute-start | bytes 786440 | tf_op jit(solution)/shard_map/ppermute | solution.py:466
  58.7 12.9 %collective-permute-start.34 = (bf16[128,1024]{1,0:T(8,128)(2,1)S(1)}, bf16[128,1024]{1,0:T(8,128)(2,1)S(1)}, u32[]{:S(2)}, u32[]{:S(2)}) collective-permute-start(bf16[128,1024]{1,0:T(8,128)(2,1)S(1)} %shard_map.152.refs_0_), channel_id=1, source_target_pairs={{0,2},{1,3},{2,0},{3,1},{4,6},{5,7},{6,4},{7,5},{8,10},{9,11},{10,... | collective-permute-start | bytes 786440 | tf_op jit(solution)/shard_map/ppermute | solution.py:466
  60.3 13.1 %collective-permute-start.37 = (bf16[128,1024]{1,0:T(8,128)(2,1)S(1)}, bf16[128,1024]{1,0:T(8,128)(2,1)S(1)}, u32[]{:S(2)}, u32[]{:S(2)}) collective-permute-start(bf16[128,1024]{1,0:T(8,128)(2,1)S(1)} %shard_map.153.refs_4_), channel_id=1, source_target_pairs={{0,1},{1,0},{2,3},{3,2},{4,5},{5,4},{6,7},{7,6},{8,9},{9,8},{10,11... | collective-permute-start | bytes 786440 | tf_op jit(solution)/shard_map/ppermute | solution.py:466
  62.3 14.9 %collective-permute-start.23 = (bf16[128,1024]{1,0:T(8,128)(2,1)S(1)}, bf16[128,1024]{1,0:T(8,128)(2,1)S(1)}, u32[]{:S(2)}, u32[]{:S(2)}) collective-permute-start(bf16[128,1024]{1,0:T(8,128)(2,1)S(1)} %shard_map.147.refs_4_), channel_id=1, source_target_pairs={{0,2},{1,3},{2,0},{3,1},{4,6},{5,7},{6,4},{7,5},{8,10},{9,11},{10,... | collective-permute-start | bytes 786440 | tf_op jit(solution)/shard_map/ppermute | solution.py:466
  64.3 18.5 %collective-permute-start.35 = (bf16[128,1024]{1,0:T(8,128)(2,1)S(1)}, bf16[128,1024]{1,0:T(8,128)(2,1)S(1)}, u32[]{:S(2)}, u32[]{:S(2)}) collective-permute-start(bf16[128,1024]{1,0:T(8,128)(2,1)S(1)} %collective-permute-done.33.refs_1_), channel_id=1, source_target_pairs={{0,2},{1,3},{2,0},{3,1},{4,6},{5,7},{6,4},{7,5},{8,10},{9,11},{10,... | collective-permute-start | bytes 786440 | tf_op jit(solution)/shard_map/ppermute | solution.py:466
  66.0 16.9 %collective-permute-start.39 = (bf16[128,1024]{1,0:T(8,128)(2,1)S(1)}, bf16[128,1024]{1,0:T(8,128)(2,1)S(1)}, u32[]{:S(2)}, u32[]{:S(2)}) collective-permute-start(bf16[128,1024]{1,0:T(8,128)(2,1)S(1)} %collective-permute-done.38.refs_6_), channel_id=1, source_target_pairs={{0,1},{1,0},{2,3},{3,2},{4,5},{5,4},{6,7},{7,6},{8,9},{9,8},{10,11... | collective-permute-start | bytes 786440 | tf_op jit(solution)/shard_map/ppermute | solution.py:466
  71.6 15.6 %collective-permute-start.20 = (bf16[128,1024]{1,0:T(8,128)(2,1)S(1)}, bf16[128,1024]{1,0:T(8,128)(2,1)S(1)}, u32[]{:S(2)}, u32[]{:S(2)}) collective-permute-start(bf16[128,1024]{1,0:T(8,128)(2,1)S(1)} %collective-permute-done.18.refs_1_), channel_id=1, source_target_pairs={{0,2},{1,3},{2,0},{3,1},{4,6},{5,7},{6,4},{7,5},{8,10},{9,11},{10,... | collective-permute-start | bytes 786440 | tf_op jit(solution)/shard_map/ppermute | solution.py:466
  73.5 16.0 %collective-permute-start.22 = (bf16[128,1024]{1,0:T(8,128)(2,1)S(1)}, bf16[128,1024]{1,0:T(8,128)(2,1)S(1)}, u32[]{:S(2)}, u32[]{:S(2)}) collective-permute-start(bf16[128,1024]{1,0:T(8,128)(2,1)S(1)} %shard_map.147.refs_4_), channel_id=1, source_target_pairs={{0,1},{1,0},{2,3},{3,2},{4,5},{5,4},{6,7},{7,6},{8,9},{9,8},{10,11... | collective-permute-start | bytes 786440 | tf_op jit(solution)/shard_map/ppermute | solution.py:466
  77.2 13.5 %collective-permute-start.24 = (bf16[128,1024]{1,0:T(8,128)(2,1)S(1)}, bf16[128,1024]{1,0:T(8,128)(2,1)S(1)}, u32[]{:S(2)}, u32[]{:S(2)}) collective-permute-start(bf16[128,1024]{1,0:T(8,128)(2,1)S(1)} %collective-permute-done.23.refs_6_), channel_id=1, source_target_pairs={{0,1},{1,0},{2,3},{3,2},{4,5},{5,4},{6,7},{7,6},{8,9},{9,8},{10,11... | collective-permute-start | bytes 786440 | tf_op jit(solution)/shard_map/ppermute | solution.py:466
  82.8 11.9 %collective-permute-start.5 = (bf16[384,384]{1,0:T(8,128)(2,1)S(1)}, bf16[384,384]{1,0:T(8,128)(2,1)S(1)}, u32[]{:S(2)}, u32[]{:S(2)}) collective-permute-start(bf16[384,384]{1,0:T(8,128)(2,1)S(1)} %collective-permute-done.1.refs_2_), channel_id=1, source_target_pairs={{0,4},{4,0},{8,12},{12,8},{16,20},{20,16},{24,28},{28,24},{1,5},{5... | collective-permute-start | bytes 884744 | tf_op jit(solution)/shard_map/ppermute | solution.py:463
  82.8 13.9 %collective-permute-start.6 = (bf16[384,384]{1,0:T(8,128)(2,1)S(1)}, bf16[384,384]{1,0:T(8,128)(2,1)S(1)}, u32[]{:S(2)}, u32[]{:S(2)}) collective-permute-start(bf16[384,384]{1,0:T(8,128)(2,1)S(1)} %collective-permute-done.2.refs_3_), channel_id=1, source_target_pairs={{0,4},{4,0},{8,12},{12,8},{16,20},{20,16},{24,28},{28,24},{1,5},{5... | collective-permute-start | bytes 884744 | tf_op jit(solution)/shard_map/ppermute | solution.py:463
  87.0 16.6 %copy-start.6 = (f32[4]{0:T(128)S(1)}, f32[4]{0:T(128)}, u32[]{:S(2)}) copy-start(f32[4]{0:T(128)} %scale_ref.1) | copy-start | bytes 52
  87.0 16.5 %copy-start.7 = (f32[128]{0:T(128)S(1)}, f32[128]{0:T(128)}, u32[]{:S(2)}) copy-start(f32[128]{0:T(128)} %param.17) | copy-start | bytes 1540
  87.2 10.8 %collective-permute-start.40 = (bf16[256,512]{1,0:T(8,128)(2,1)S(1)}, bf16[256,512]{1,0:T(8,128)(2,1)S(1)}, u32[]{:S(2)}, u32[]{:S(2)}) collective-permute-start(bf16[256,512]{1,0:T(8,128)(2,1)S(1)} %shard_map.154.refs_0_), channel_id=1, source_target_pairs={{0,1},{1,0},{2,3},{3,2},{4,5},{5,4},{6,7},{7,6},{8,9},{9,8},{10,11... | collective-permute-start | bytes 786440 | tf_op jit(solution)/shard_map/ppermute | solution.py:466
  89.5 23.7 %collective-permute-start.41 = (bf16[256,512]{1,0:T(8,128)(2,1)S(1)}, bf16[256,512]{1,0:T(8,128)(2,1)S(1)}, u32[]{:S(2)}, u32[]{:S(2)}) collective-permute-start(bf16[256,512]{1,0:T(8,128)(2,1)S(1)} %shard_map.154.refs_0_), channel_id=1, source_target_pairs={{0,2},{1,3},{2,0},{3,1},{4,6},{5,7},{6,4},{7,5},{8,10},{9,11},{10,... | collective-permute-start | bytes 786440 | tf_op jit(solution)/shard_map/ppermute | solution.py:466
  90.7 27.6 %collective-permute-start.42 = (bf16[256,512]{1,0:T(8,128)(2,1)S(1)}, bf16[256,512]{1,0:T(8,128)(2,1)S(1)}, u32[]{:S(2)}, u32[]{:S(2)}) collective-permute-start(bf16[256,512]{1,0:T(8,128)(2,1)S(1)} %shard_map.154.refs_0_), channel_id=1, source_target_pairs={{0,3},{1,2},{2,1},{3,0},{4,7},{5,6},{6,5},{7,4},{8,11},{9,10},{10,... | collective-permute-start | bytes 786440 | tf_op jit(solution)/shard_map/ppermute | solution.py:466
  94.7 25.6 %copy-start.3 = (bf16[1,2048,1024]{2,1,0:T(8,128)(2,1)S(1)}, bf16[1,2048,1024]{2,1,0:T(8,128)(2,1)}, u32[]{:S(2)}) copy-start(bf16[1,2048,1024]{2,1,0:T(8,128)(2,1)} %w_ref.5) | copy-start | bytes 12582916
  94.8 27.6 %collective-permute-start.25 = (bf16[256,512]{1,0:T(8,128)(2,1)S(1)}, bf16[256,512]{1,0:T(8,128)(2,1)S(1)}, u32[]{:S(2)}, u32[]{:S(2)}) collective-permute-start(bf16[256,512]{1,0:T(8,128)(2,1)S(1)} %shard_map.149.refs_0_), channel_id=1, source_target_pairs={{0,1},{1,0},{2,3},{3,2},{4,5},{5,4},{6,7},{7,6},{8,9},{9,8},{10,11... | collective-permute-start | bytes 786440 | tf_op jit(solution)/shard_map/ppermute | solution.py:466
  96.8 28.4 %collective-permute-start.26 = (bf16[256,512]{1,0:T(8,128)(2,1)S(1)}, bf16[256,512]{1,0:T(8,128)(2,1)S(1)}, u32[]{:S(2)}, u32[]{:S(2)}) collective-permute-start(bf16[256,512]{1,0:T(8,128)(2,1)S(1)} %shard_map.149.refs_0_), channel_id=1, source_target_pairs={{0,2},{1,3},{2,0},{3,1},{4,6},{5,7},{6,4},{7,5},{8,10},{9,11},{10,... | collective-permute-start | bytes 786440 | tf_op jit(solution)/shard_map/ppermute | solution.py:466
  97.9 28.1 %collective-permute-start.27 = (bf16[256,512]{1,0:T(8,128)(2,1)S(1)}, bf16[256,512]{1,0:T(8,128)(2,1)S(1)}, u32[]{:S(2)}, u32[]{:S(2)}) collective-permute-start(bf16[256,512]{1,0:T(8,128)(2,1)S(1)} %shard_map.149.refs_0_), channel_id=1, source_target_pairs={{0,3},{1,2},{2,1},{3,0},{4,7},{5,6},{6,5},{7,4},{8,11},{9,10},{10,... | collective-permute-start | bytes 786440 | tf_op jit(solution)/shard_map/ppermute | solution.py:466
  113.2 9.0 %collective-permute-start.7 = (bf16[384,128]{1,0:T(8,128)(2,1)S(1)}, bf16[384,128]{1,0:T(8,128)(2,1)S(1)}, u32[]{:S(2)}, u32[]{:S(2)}) collective-permute-start(bf16[384,128]{1,0:T(8,128)(2,1)S(1)} %get-tuple-element.35), channel_id=1, source_target_pairs={{0,8},{4,12},{8,0},{12,4},{16,24},{20,28},{24,16},{28,20},{1,9},{5... | collective-permute-start | bytes 294920 | tf_op jit(solution)/shard_map/ppermute | solution.py:463
  118.3 11.1 %collective-permute-start.11 = (bf16[384,128]{1,0:T(8,128)(2,1)S(1)}, bf16[384,128]{1,0:T(8,128)(2,1)S(1)}, u32[]{:S(2)}, u32[]{:S(2)}) collective-permute-start(bf16[384,128]{1,0:T(8,128)(2,1)S(1)} %get-tuple-element.36), channel_id=1, source_target_pairs={{0,16},{4,20},{8,24},{12,28},{16,0},{20,4},{24,8},{28,12},{1,17},{... | collective-permute-start | bytes 294920 | tf_op jit(solution)/shard_map/ppermute | solution.py:463
  122.2 23.2 %copy-start.4 = (bf16[2048,1024]{1,0:T(8,128)(2,1)S(1)}, bf16[2048,1024]{1,0:T(8,128)(2,1)}, u32[]{:S(2)}) copy-start(bf16[2048,1024]{1,0:T(8,128)(2,1)} %w_ref.3) | copy-start | bytes 12582916
  122.2 8.0 %collective-permute-start.43 = (bf16[128,1024]{1,0:T(8,128)(2,1)S(1)}, bf16[128,1024]{1,0:T(8,128)(2,1)S(1)}, u32[]{:S(2)}, u32[]{:S(2)}) collective-permute-start(bf16[128,1024]{1,0:T(8,128)(2,1)S(1)} %get-tuple-element.43), channel_id=1, source_target_pairs={{0,4},{4,0},{8,12},{12,8},{16,20},{20,16},{24,28},{28,24},{1,5},{5... | collective-permute-start | bytes 786440 | tf_op jit(solution)/shard_map/ppermute | solution.py:463
  122.3 7.2 %collective-permute-start.12 = (bf16[384,128]{1,0:T(8,128)(2,1)S(1)}, bf16[384,128]{1,0:T(8,128)(2,1)S(1)}, u32[]{:S(2)}, u32[]{:S(2)}) collective-permute-start(bf16[384,128]{1,0:T(8,128)(2,1)S(1)} %get-tuple-element.37), channel_id=1, source_target_pairs={{0,24},{4,28},{8,16},{12,20},{16,8},{20,12},{24,0},{28,4},{1,25},{... | collective-permute-start | bytes 294920 | tf_op jit(solution)/shard_map/ppermute | solution.py:463
  125.2 12.5 %collective-permute-start.8 = (bf16[384,256]{1,0:T(8,128)(2,1)S(1)}, bf16[384,256]{1,0:T(8,128)(2,1)S(1)}, u32[]{:S(2)}, u32[]{:S(2)}) collective-permute-start(bf16[384,256]{1,0:T(8,128)(2,1)S(1)} %constant_dynamic-update-slice_fusion.refs_0_), channel_id=1, source_target_pairs={{0,1},{1,0},{2,3},{3,2},{4,5},{5,4},{6,7},{7,6},{8,9},{9,8},{10,11... | collective-permute-start | bytes 589832 | tf_op jit(solution)/shard_map/ppermute | solution.py:466
  126.0 12.4 %collective-permute-start.9 = (bf16[384,256]{1,0:T(8,128)(2,1)S(1)}, bf16[384,256]{1,0:T(8,128)(2,1)S(1)}, u32[]{:S(2)}, u32[]{:S(2)}) collective-permute-start(bf16[384,256]{1,0:T(8,128)(2,1)S(1)} %constant_dynamic-update-slice_fusion.refs_0_), channel_id=1, source_target_pairs={{0,2},{1,3},{2,0},{3,1},{4,6},{5,7},{6,4},{7,5},{8,10},{9,11},{10,... | collective-permute-start | bytes 589832 | tf_op jit(solution)/shard_map/ppermute | solution.py:466
  129.4 3.8 %collective-permute-start.28 = (bf16[128,1024]{1,0:T(8,128)(2,1)S(1)}, bf16[128,1024]{1,0:T(8,128)(2,1)S(1)}, u32[]{:S(2)}, u32[]{:S(2)}) collective-permute-start(bf16[128,1024]{1,0:T(8,128)(2,1)S(1)} %get-tuple-element.39), channel_id=1, source_target_pairs={{0,4},{4,0},{8,12},{12,8},{16,20},{20,16},{24,28},{28,24},{1,5},{5... | collective-permute-start | bytes 786440 | tf_op jit(solution)/shard_map/ppermute | solution.py:463
  129.6 9.6 %collective-permute-start.13 = (bf16[384,256]{1,0:T(8,128)(2,1)S(1)}, bf16[384,256]{1,0:T(8,128)(2,1)S(1)}, u32[]{:S(2)}, u32[]{:S(2)}) collective-permute-start(bf16[384,256]{1,0:T(8,128)(2,1)S(1)} %constant_dynamic-update-slice_fusion.2.refs_4_), channel_id=1, source_target_pairs={{0,1},{1,0},{2,3},{3,2},{4,5},{5,4},{6,7},{7,6},{8,9},{9,8},{10,11... | collective-permute-start | bytes 589832 | tf_op jit(solution)/shard_map/ppermute | solution.py:466
  130.2 9.5 %collective-permute-start.14 = (bf16[384,256]{1,0:T(8,128)(2,1)S(1)}, bf16[384,256]{1,0:T(8,128)(2,1)S(1)}, u32[]{:S(2)}, u32[]{:S(2)}) collective-permute-start(bf16[384,256]{1,0:T(8,128)(2,1)S(1)} %constant_dynamic-update-slice_fusion.2.refs_4_), channel_id=1, source_target_pairs={{0,2},{1,3},{2,0},{3,1},{4,6},{5,7},{6,4},{7,5},{8,10},{9,11},{10,... | collective-permute-start | bytes 589832 | tf_op jit(solution)/shard_map/ppermute | solution.py:466
  133.2 15.9 %collective-permute-start.45 = (bf16[128,1024]{1,0:T(8,128)(2,1)S(1)}, bf16[128,1024]{1,0:T(8,128)(2,1)S(1)}, u32[]{:S(2)}, u32[]{:S(2)}) collective-permute-start(bf16[128,1024]{1,0:T(8,128)(2,1)S(1)} %get-tuple-element.45), channel_id=1, source_target_pairs={{0,24},{4,28},{8,16},{12,20},{16,8},{20,12},{24,0},{28,4},{1,25},{... | collective-permute-start | bytes 786440 | tf_op jit(solution)/shard_map/ppermute | solution.py:463
  137.8 21.3 %collective-permute-start.44 = (bf16[128,1024]{1,0:T(8,128)(2,1)S(1)}, bf16[128,1024]{1,0:T(8,128)(2,1)S(1)}, u32[]{:S(2)}, u32[]{:S(2)}) collective-permute-start(bf16[128,1024]{1,0:T(8,128)(2,1)S(1)} %get-tuple-element.44), channel_id=1, source_target_pairs={{0,16},{4,20},{8,24},{12,28},{16,0},{20,4},{24,8},{28,12},{1,17},{... | collective-permute-start | bytes 786440 | tf_op jit(solution)/shard_map/ppermute | solution.py:463
  138.5 20.6 %collective-permute-start.29 = (bf16[128,1024]{1,0:T(8,128)(2,1)S(1)}, bf16[128,1024]{1,0:T(8,128)(2,1)S(1)}, u32[]{:S(2)}, u32[]{:S(2)}) collective-permute-start(bf16[128,1024]{1,0:T(8,128)(2,1)S(1)} %get-tuple-element.41), channel_id=1, source_target_pairs={{0,8},{4,12},{8,0},{12,4},{16,24},{20,28},{24,16},{28,20},{1,9},{5... | collective-permute-start | bytes 786440 | tf_op jit(solution)/shard_map/ppermute | solution.py:463
  139.2 5.7 %collective-permute-start.10 = (bf16[384,256]{1,0:T(8,128)(2,1)S(1)}, bf16[384,256]{1,0:T(8,128)(2,1)S(1)}, u32[]{:S(2)}, u32[]{:S(2)}) collective-permute-start(bf16[384,256]{1,0:T(8,128)(2,1)S(1)} %collective-permute-done.8.refs_1_), channel_id=1, source_target_pairs={{0,2},{1,3},{2,0},{3,1},{4,6},{5,7},{6,4},{7,5},{8,10},{9,11},{10,... | collective-permute-start | bytes 589832 | tf_op jit(solution)/shard_map/ppermute | solution.py:466
  139.7 5.7 %collective-permute-start.15 = (bf16[384,256]{1,0:T(8,128)(2,1)S(1)}, bf16[384,256]{1,0:T(8,128)(2,1)S(1)}, u32[]{:S(2)}, u32[]{:S(2)}) collective-permute-start(bf16[384,256]{1,0:T(8,128)(2,1)S(1)} %collective-permute-done.14.refs_6_), channel_id=1, source_target_pairs={{0,1},{1,0},{2,3},{3,2},{4,5},{5,4},{6,7},{7,6},{8,9},{9,8},{10,11... | collective-permute-start | bytes 589832 | tf_op jit(solution)/shard_map/ppermute | solution.py:466

commit v3 on v2

--- a/solution.py
+++ b/solution.py
@@ -285,18 +285,32 @@
     out[...] = value_ref[0, 0:8, 0:128]
 
 
-def project_kernel(parts, groups, width, where_ref, w_ref, *refs):
-    pieces, (out, heads) = refs[: len(groups) * parts], refs[-2:]
+def fill_heads(parts, slots, width, pieces, heads):
+    for part in range(parts):
+        for i in range(len(slots)):
+            at = (part * len(slots) + i) * width
+            heads[:, at : at + width] = pieces[part][:, i * width : (i + 1) * width]
+
+
+def project_first_kernel(parts, groups, width, where_ref, w_ref, *refs):
+    pieces, (out, later, heads, rows) = refs[:parts], refs[parts:]
     chip, tp = where_ref[0], where_ref[2]
-    depth = heads.shape[1] // parts
-    for part in range(parts):
-        for number, slots in enumerate(groups):
+    depth = w_ref.shape[0] // parts
+    for slots, held in ((groups[0], rows), (groups[1], later)):
+        for part in range(parts):
             for i, slot in enumerate(slots):
-                at = pl.multiple_of((tp ^ part) * depth + (chip ^ slot) * width, width)
-                heads[:, pl.ds(at, width)] = pieces[number * parts + part][
-                    :, i * width : (i + 1) * width
-                ]
-    out[...] = jnp.dot(heads[...], w_ref[...], preferred_element_type=f32).astype(bf16)
+                source = pl.multiple_of((tp ^ part) * depth + (chip ^ slot) * width, width)
+                at = (part * len(slots) + i) * width
+                held[at : at + width] = w_ref[pl.ds(source, width)]
+    fill_heads(parts, groups[0], width, pieces, heads)
+    out[...] = jnp.dot(heads[...], rows[...], preferred_element_type=f32)
+
+
+def project_kernel(parts, slots, width, first_ref, w_ref, *refs):
+    pieces, (out, heads) = refs[:parts], refs[parts:]
+    fill_heads(parts, slots, width, pieces, heads)
+    product = jnp.dot(heads[...], w_ref[...], preferred_element_type=f32)
+    out[...] = (first_ref[...] + product).astype(bf16)
 
 
 def rows_kernel(count, rows_ref, ids_ref, share_ref, out, ids, share, sems):
@@ -621,14 +635,28 @@
     pieces = []
     for number, group in enumerate(head_groups):
         value = jnp.concatenate([back[slot] for slot in group], axis=1)
-        pieces += spread(value, 1 + number)
-    mixer_out = call(
-        functools.partial(project_kernel, tp_devices, head_groups, width),
-        sds(count_a, out_columns),
+        pieces.append(spread(value, 1 + number))
+    depth = tp_devices * len(head_groups[0]) * width
+    first, later = call(
+        functools.partial(project_first_kernel, tp_devices, head_groups, width),
+        [
+            jax.ShapeDtypeStruct((count_a, out_columns), f32),
+            sds(out_weight.shape[0] - depth, out_columns),
+        ],
         where,
         out_weight,
-        *pieces,
-        scratch=[pltpu.VMEM((count_a, out_weight.shape[0]), bf16)],
+        *pieces[0],
+        scratch=[pltpu.VMEM((count_a, depth), bf16), pltpu.VMEM((depth, out_columns), bf16)],
+        limit=12,
+    )
+    mixer_out = call(
+        functools.partial(project_kernel, tp_devices, head_groups[1], width),
+        sds(count_a, out_columns),
+        first,
+        later,
+        *pieces[1],
+        scalars=0,
+        scratch=[pltpu.VMEM((count_a, out_weight.shape[0] - depth), bf16)],
         limit=12,
         last=True,
     )

time: 160 us -> 163 us (1.019)
  waiting for transfers between devices: 55.7 us -> 63.5 us
  starting transfers between devices: 61.3 us -> 56.9 us
    ppermute x24, waiting for transfers between devices: 13.5 us -> 25.4 us  [over_tp(): lax.ppermute(value, 'tp', [(i, i ^ offset) for i in range(tp_devices)])]
    ppermute x24, starting transfers between devices: 34.8 us -> 29 us  [over_tp(): lax.ppermute(value, 'tp', [(i, i ^ offset) for i in range(tp_devices)])]
    ppermute x22, waiting for transfers between devices: 42.2 us -> 38.1 us  [over_ep(): return lax.ppermute(value, 'ep', pairs)]
    pallas_call x15 -> x16, Pallas kernels: 35.5 us -> 35.5 us  [call(): pl.pallas_call(body, out_shape=out_shape if last else near_shapes(out_sha...]
  transfers between devices with their start and end apart: 46 -> 46, of which waited for: 12 -> 15; matrix products, arithmetic and copies ran while one was open for 0% -> 0% of each run, Pallas kernels for 24% -> 23%
where the time goes in v3:
time: 163 us
  waiting for transfers between devices  63.5 us (39%)
  starting transfers between devices  56.9 us (35%)
  Pallas kernels  38.6 us (24%)
  local copies, waits for them, and re-layouts  2.31 us (1%)
    ppermute x22, waiting for transfers between devices, over_ep(): return lax.ppermute(value, 'ep', pairs)  38.1 us
    pallas_call x16, Pallas kernels, call(): pl.pallas_call(body, out_shape=out_shape if last else near_shapes(out_sha...  35.5 us
    ppermute x24, starting transfers between devices, over_tp(): lax.ppermute(value, 'tp', [(i, i ^ offset) for i in range(tp_devices)])  29 us
    ppermute x22, starting transfers between devices, over_ep(): return lax.ppermute(value, 'ep', pairs)  27.9 us
    ppermute x24, waiting for transfers between devices, over_tp(): lax.ppermute(value, 'tp', [(i, i ^ offset) for i in range(tp_devices)])  25.4 us
  transfers between devices with their start and end apart: 46, of which 15 were waited for; matrix products, arithmetic and copies ran while one was open for 0% of the time, Pallas kernels for 23%

profile of v3, /device:TPU:0, one launch (start us, length us, event | category | flops | bytes accessed | tf_op | source)
XLA Modules:
  0.0 163.3 jit_solution(6830693497403977779)
XLA Ops:
  0.6 1.0 shard_map.146.refs_0_
  1.6 4.1 %collective-permute-start.30 = (bf16[136,1024]{1,0:T(8,128)(2,1)S(1)}, bf16[136,1024]{1,0:T(8,128)(2,1)S(1)}, u32[]{:S(2)}, u32[]{:S(2)}) collective-permute-start(bf16[136,1024]{1,0:T(8,128)(2,1)S(1)} %shard_map.146.refs_0_), channel_id=1, source_target_pairs={{0,16},{4,20},{8,24},{12,28},{16,0},{20,4},{24,8},{28,12},{1,17},{... | collective-permute-start | bytes 835592 | tf_op jit(solution)/shard_map/ppermute | solution.py:477
  5.7 1.3 collective-permute-start.31
  7.3 2.2 %copy-done = bf16[1,4096,512]{2,1,0:T(8,128)(2,1)S(1)} copy-done((bf16[1,4096,512]{2,1,0:T(8,128)(2,1)S(1)}, bf16[1,4096,512]{2,1,0:T(8,128)(2,1)}, u32[]{:S(2)}) %copy-start) | copy-done | bytes 4194328
  9.6 2.2 %shard_map.141 = (bf16[384,384]{1,0:T(8,128)(2,1)S(1)}, bf16[384,384]{1,0:T(8,128)(2,1)S(1)}, bf16[384,384]{1,0:T(8,128)(2,1)S(1)}, bf16[384,384]{1,0:T(8,128)(2,1)S(1)}) custom-call(s32[3]{0:T(128)S(1)} %pad_add_fusion.where_ref, bf16[384,512]{1,0:T(8,128)(2,1)} %q_ref.1, bf16[384,512]{1,0:T(8,128)(2,1)} %k_ref.1, bf16[384,512]{1,0:T(8,128)(2,1)} %v_ref.1, ...), custom_call_target="tpu_custom_call" | custom-call | tf_op jit(solution)/shard_map/pallas_call | solution.py:532
  11.8 1.9 %collective-permute-start = (bf16[384,384]{1,0:T(8,128)(2,1)S(1)}, bf16[384,384]{1,0:T(8,128)(2,1)S(1)}, u32[]{:S(2)}, u32[]{:S(2)}) collective-permute-start(bf16[384,384]{1,0:T(8,128)(2,1)S(1)} %get-tuple-element.27), channel_id=1, source_target_pairs={{0,8},{4,12},{8,0},{12,4},{16,24},{20,28},{24,16},{28,20},{1,9},{5... | collective-permute-start | bytes 884744 | tf_op jit(solution)/shard_map/ppermute | solution.py:477
  13.7 11.6 %collective-permute-done.30.refs_0_ = bf16[136,1024]{1,0:T(8,128)(2,1)S(1)} collective-permute-done((bf16[136,1024]{1,0:T(8,128)(2,1)S(1)}, bf16[136,1024]{1,0:T(8,128)(2,1)S(1)}, u32[]{:S(2)}, u32[]{:S(2)}) %collective-permute-start.30) | collective-permute-done | bytes 278560 | tf_op jit(solution)/shard_map/ppermute | solution.py:477
  25.2 2.8 %collective-permute-start.2 = (bf16[384,384]{1,0:T(8,128)(2,1)S(1)}, bf16[384,384]{1,0:T(8,128)(2,1)S(1)}, u32[]{:S(2)}, u32[]{:S(2)}) collective-permute-start(bf16[384,384]{1,0:T(8,128)(2,1)S(1)} %get-tuple-element.29), channel_id=1, source_target_pairs={{0,24},{4,28},{8,16},{12,20},{16,8},{20,12},{24,0},{28,4},{1,25},{... | collective-permute-start | bytes 884744 | tf_op jit(solution)/shard_map/ppermute | solution.py:477
  28.0 0.5 collective-permute-start.32
  28.5 1.0 shard_map.147.refs_0_
  29.5 4.1 %collective-permute-done.refs_1_ = bf16[384,384]{1,0:T(8,128)(2,1)S(1)} collective-permute-done((bf16[384,384]{1,0:T(8,128)(2,1)S(1)}, bf16[384,384]{1,0:T(8,128)(2,1)S(1)}, u32[]{:S(2)}, u32[]{:S(2)}) %collective-permute-start) | collective-permute-done | bytes 294944 | tf_op jit(solution)/shard_map/ppermute | solution.py:477
  33.6 1.5 collective-permute-start.18
  35.1 15.1 %collective-permute-done.1.refs_2_ = bf16[384,384]{1,0:T(8,128)(2,1)S(1)} collective-permute-done((bf16[384,384]{1,0:T(8,128)(2,1)S(1)}, bf16[384,384]{1,0:T(8,128)(2,1)S(1)}, u32[]{:S(2)}, u32[]{:S(2)}) %collective-permute-start.1) | collective-permute-done | bytes 294944 | tf_op jit(solution)/shard_map/ppermute | solution.py:477
  50.2 1.8 %collective-permute-start.19 = (bf16[128,1024]{1,0:T(8,128)(2,1)S(1)}, bf16[128,1024]{1,0:T(8,128)(2,1)S(1)}, u32[]{:S(2)}, u32[]{:S(2)}) collective-permute-start(bf16[128,1024]{1,0:T(8,128)(2,1)S(1)} %shard_map.147.refs_0_), channel_id=1, source_target_pairs={{0,2},{1,3},{2,0},{3,1},{4,6},{5,7},{6,4},{7,5},{8,10},{9,11},{10,... | collective-permute-start | bytes 786440 | tf_op jit(solution)/shard_map/ppermute | solution.py:480
  52.5 1.0 shard_map.153.refs_0_
  53.5 1.6 collective-permute-start.33
  55.1 0.5 collective-permute-start.34
  55.6 1.0 shard_map.154.refs_4_
  56.6 2.7 %collective-permute-done.19.refs_2_ = bf16[128,1024]{1,0:T(8,128)(2,1)S(1)} collective-permute-done((bf16[128,1024]{1,0:T(8,128)(2,1)S(1)}, bf16[128,1024]{1,0:T(8,128)(2,1)S(1)}, u32[]{:S(2)}, u32[]{:S(2)}) %collective-permute-start.19) | collective-permute-done | bytes 262176 | tf_op jit(solution)/shard_map/ppermute | solution.py:480
  59.4 1.8 %collective-permute-start.38 = (bf16[128,1024]{1,0:T(8,128)(2,1)S(1)}, bf16[128,1024]{1,0:T(8,128)(2,1)S(1)}, u32[]{:S(2)}, u32[]{:S(2)}) collective-permute-start(bf16[128,1024]{1,0:T(8,128)(2,1)S(1)} %shard_map.154.refs_4_), channel_id=1, source_target_pairs={{0,2},{1,3},{2,0},{3,1},{4,6},{5,7},{6,4},{7,5},{8,10},{9,11},{10,... | collective-permute-start | bytes 786440 | tf_op jit(solution)/shard_map/ppermute | solution.py:480
  61.2 1.5 collective-permute-start.37
  62.7 1.0 shard_map.148.refs_4_
  63.7 0.6 collective-permute-start.23
  64.3 0.7 collective-permute-done.34.refs_2_
  65.0 1.8 %collective-permute-start.35 = (bf16[128,1024]{1,0:T(8,128)(2,1)S(1)}, bf16[128,1024]{1,0:T(8,128)(2,1)S(1)}, u32[]{:S(2)}, u32[]{:S(2)}) collective-permute-start(bf16[128,1024]{1,0:T(8,128)(2,1)S(1)} %collective-permute-done.33.refs_1_), channel_id=1, source_target_pairs={{0,2},{1,3},{2,0},{3,1},{4,6},{5,7},{6,4},{7,5},{8,10},{9,11},{10,... | collective-permute-start | bytes 786440 | tf_op jit(solution)/shard_map/ppermute | solution.py:480
  66.8 3.8 %collective-permute-done.38.refs_6_ = bf16[128,1024]{1,0:T(8,128)(2,1)S(1)} collective-permute-done((bf16[128,1024]{1,0:T(8,128)(2,1)S(1)}, bf16[128,1024]{1,0:T(8,128)(2,1)S(1)}, u32[]{:S(2)}, u32[]{:S(2)}) %collective-permute-start.38) | collective-permute-done | bytes 262176 | tf_op jit(solution)/shard_map/ppermute | solution.py:480
  70.6 1.8 %collective-permute-start.39 = (bf16[128,1024]{1,0:T(8,128)(2,1)S(1)}, bf16[128,1024]{1,0:T(8,128)(2,1)S(1)}, u32[]{:S(2)}, u32[]{:S(2)}) collective-permute-start(bf16[128,1024]{1,0:T(8,128)(2,1)S(1)} %collective-permute-done.38.refs_6_), channel_id=1, source_target_pairs={{0,1},{1,0},{2,3},{3,2},{4,5},{5,4},{6,7},{7,6},{8,9},{9,8},{10,11... | collective-permute-start | bytes 786440 | tf_op jit(solution)/shard_map/ppermute | solution.py:480
  72.4 3.8 %collective-permute-done.23.refs_6_ = bf16[128,1024]{1,0:T(8,128)(2,1)S(1)} collective-permute-done((bf16[128,1024]{1,0:T(8,128)(2,1)S(1)}, bf16[128,1024]{1,0:T(8,128)(2,1)S(1)}, u32[]{:S(2)}, u32[]{:S(2)}) %collective-permute-start.23) | collective-permute-done | bytes 262176 | tf_op jit(solution)/shard_map/ppermute | solution.py:480
  76.2 1.8 %collective-permute-start.20 = (bf16[128,1024]{1,0:T(8,128)(2,1)S(1)}, bf16[128,1024]{1,0:T(8,128)(2,1)S(1)}, u32[]{:S(2)}, u32[]{:S(2)}) collective-permute-start(bf16[128,1024]{1,0:T(8,128)(2,1)S(1)} %collective-permute-done.18.refs_1_), channel_id=1, source_target_pairs={{0,2},{1,3},{2,0},{3,1},{4,6},{5,7},{6,4},{7,5},{8,10},{9,11},{10,... | collective-permute-start | bytes 786440 | tf_op jit(solution)/shard_map/ppermute | solution.py:480
  78.0 3.8 %collective-permute-done.35.refs_3_ = bf16[128,1024]{1,0:T(8,128)(2,1)S(1)} collective-permute-done((bf16[128,1024]{1,0:T(8,128)(2,1)S(1)}, bf16[128,1024]{1,0:T(8,128)(2,1)S(1)}, u32[]{:S(2)}, u32[]{:S(2)}) %collective-permute-start.35) | collective-permute-done | bytes 262176 | tf_op jit(solution)/shard_map/ppermute | solution.py:480
  81.8 1.8 %collective-permute-start.22 = (bf16[128,1024]{1,0:T(8,128)(2,1)S(1)}, bf16[128,1024]{1,0:T(8,128)(2,1)S(1)}, u32[]{:S(2)}, u32[]{:S(2)}) collective-permute-start(bf16[128,1024]{1,0:T(8,128)(2,1)S(1)} %shard_map.148.refs_4_), channel_id=1, source_target_pairs={{0,1},{1,0},{2,3},{3,2},{4,5},{5,4},{6,7},{7,6},{8,9},{9,8},{10,11... | collective-permute-start | bytes 786440 | tf_op jit(solution)/shard_map/ppermute | solution.py:480
  83.9 3.8 %shard_map.155.refs_0_ = bf16[256,512]{1,0:T(8,128)(2,1)S(1)} custom-call(s32[3]{0:T(128)S(1)} %pad_add_fusion.where_ref, f32[4,1,1024]{2,1,0:T(1,128)S(1)} %bitcast.7, bf16[1,4096,512]{2,1,0:T(8,128)(2,1)S(1)} %copy-done.1, bf16[1,4096,512]{2,1,0:T(8,128)(2,1)S(1)} %copy-done.2, bf16[128,1024]{1,0:T(8,128)(2,1)S(1)} %shard_map.153.refs_0_, ...), custom_call_target="tpu_custom_call" | custom-call | tf_op jit(solution)/shard_map/pallas_call | solution.py:499
  87.8 1.9 %collective-permute-start.40 = (bf16[256,512]{1,0:T(8,128)(2,1)S(1)}, bf16[256,512]{1,0:T(8,128)(2,1)S(1)}, u32[]{:S(2)}, u32[]{:S(2)}) collective-permute-start(bf16[256,512]{1,0:T(8,128)(2,1)S(1)} %shard_map.155.refs_0_), channel_id=1, source_target_pairs={{0,1},{1,0},{2,3},{3,2},{4,5},{5,4},{6,7},{7,6},{8,9},{9,8},{10,11... | collective-permute-start | bytes 786440 | tf_op jit(solution)/shard_map/ppermute | solution.py:480
  89.6 1.5 collective-permute-start.41
  91.2 4.1 %shard_map.142 = (f32[768,128]{1,0:T(8,128)S(1)}, f32[768,128]{1,0:T(8,128)S(1)}, f32[768,128]{1,0:T(8,128)S(1)}, f32[768,128]{1,0:T(8,128)S(1)}, f32[768,128]{1,0:T(8,128)S(1)}, /*index=5*/f32[768,128]{1,0:T(8,128)S(1)}) custom-call(s32[3]{0:T(128)S(1)} %pad_add_fusion.where_ref, bf16[384,384]{1,0:T(8,128)(2,1)S(1)} %get-tuple-element.26.refs_0_, ...), custom_call_target="tpu_custom_call" | custom-call | tf_op jit(solution)/shard_map/pallas_call | solution.py:499
  95.3 9.5 %shard_map.143 = (bf16[384,128]{1,0:T(8,128)(2,1)S(1)}, bf16[384,128]{1,0:T(8,128)(2,1)S(1)}, bf16[384,128]{1,0:T(8,128)(2,1)S(1)}, bf16[384,128]{1,0:T(8,128)(2,1)S(1)}) custom-call(s32[3]{0:T(128)S(1)} %pad_add_fusion.where_ref, f32[4]{0:T(128)S(1)} %copy-done.6, f32[1,128]{1,0:T(1,128)S(1)} %bitcast.9, bf16[384,384]{1,0:T(8,128)(2,1)S(1)} %get-tuple-element.26.refs_0_, ...), custom_call_target="tpu_custom_call" | custom-call | tf_op jit(solution)/shard_map/pallas_call | solution.py:499
  104.9 5.9 %collective-permute-start.7 = (bf16[384,128]{1,0:T(8,128)(2,1)S(1)}, bf16[384,128]{1,0:T(8,128)(2,1)S(1)}, u32[]{:S(2)}, u32[]{:S(2)}) collective-permute-start(bf16[384,128]{1,0:T(8,128)(2,1)S(1)} %get-tuple-element.37), channel_id=1, source_target_pairs={{0,8},{4,12},{8,0},{12,4},{16,24},{20,28},{24,16},{28,20},{1,9},{5... | collective-permute-start | bytes 294920 | tf_op jit(solution)/shard_map/ppermute | solution.py:477
  110.8 0.5 collective-permute-start.42
  111.3 3.8 %shard_map.150.refs_0_ = bf16[256,512]{1,0:T(8,128)(2,1)S(1)} custom-call(s32[3]{0:T(128)S(1)} %pad_add_fusion.where_ref, f32[4,1,1024]{2,1,0:T(1,128)S(1)} %bitcast.8, bf16[1,4096,512]{2,1,0:T(8,128)(2,1)S(1)} %copy-done.1, bf16[1,4096,512]{2,1,0:T(8,128)(2,1)S(1)} %copy-done.2, bf16[128,1024]{1,0:T(8,128)(2,1)S(1)} %shard_map.147.refs_0_, ...), custom_call_target="tpu_custom_call" | custom-call | tf_op jit(solution)/shard_map/pallas_call | solution.py:499
  115.1 1.6 collective-permute-start.25
  116.6 1.5 collective-permute-start.26
  118.7 2.1 %collective-permute-start.11 = (bf16[384,128]{1,0:T(8,128)(2,1)S(1)}, bf16[384,128]{1,0:T(8,128)(2,1)S(1)}, u32[]{:S(2)}, u32[]{:S(2)}) collective-permute-start(bf16[384,128]{1,0:T(8,128)(2,1)S(1)} %get-tuple-element.40), channel_id=1, source_target_pairs={{0,16},{4,20},{8,24},{12,28},{16,0},{20,4},{24,8},{28,12},{1,17},{... | collective-permute-start | bytes 294920 | tf_op jit(solution)/shard_map/ppermute | solution.py:477
  121.0 3.4 %collective-permute-start.12 = (bf16[384,128]{1,0:T(8,128)(2,1)S(1)}, bf16[384,128]{1,0:T(8,128)(2,1)S(1)}, u32[]{:S(2)}, u32[]{:S(2)}) collective-permute-start(bf16[384,128]{1,0:T(8,128)(2,1)S(1)} %get-tuple-element.41), channel_id=1, source_target_pairs={{0,24},{4,28},{8,16},{12,20},{16,8},{20,12},{24,0},{28,4},{1,25},{... | collective-permute-start | bytes 294920 | tf_op jit(solution)/shard_map/ppermute | solution.py:477
  124.4 1.9 %shard_map.156 = (bf16[128,1024]{1,0:T(8,128)(2,1)S(1)}, bf16[128,1024]{1,0:T(8,128)(2,1)S(1)}) custom-call(s32[3]{0:T(128)S(1)} %pad_add_fusion.where_ref, bf16[1,2048,1024]{2,1,0:T(8,128)(2,1)S(1)} %copy-done.3, bf16[256,512]{1,0:T(8,128)(2,1)S(1)} %shard_map.155.refs_0_, bf16[256,512]{1,0:T(8,128)(2,1)S(1)} %collective-permute-done.40.refs_1_, ...), custom_call_target="tpu_custom_call" | custom-call | tf_op jit(solution)/shard_map/pallas_call | solution.py:499
  126.4 2.4 %collective-permute-done.26.refs_2_ = bf16[256,512]{1,0:T(8,128)(2,1)S(1)} collective-permute-done((bf16[256,512]{1,0:T(8,128)(2,1)S(1)}, bf16[256,512]{1,0:T(8,128)(2,1)S(1)}, u32[]{:S(2)}, u32[]{:S(2)}) %collective-permute-start.26) | collective-permute-done | bytes 262176 | tf_op jit(solution)/shard_map/ppermute | solution.py:480
  128.7 1.5 collective-permute-start.9
  130.2 1.1 collective-permute-done.27.refs_3_
  131.4 1.9 %shard_map.151 = (bf16[128,1024]{1,0:T(8,128)(2,1)S(1)}, bf16[128,1024]{1,0:T(8,128)(2,1)S(1)}) custom-call(s32[3]{0:T(128)S(1)} %pad_add_fusion.where_ref, bf16[1,2048,1024]{2,1,0:T(8,128)(2,1)S(1)} %copy-done.3, bf16[256,512]{1,0:T(8,128)(2,1)S(1)} %shard_map.150.refs_0_, bf16[256,512]{1,0:T(8,128)(2,1)S(1)} %collective-permute-done.25.refs_1_, ...), custom_call_target="tpu_custom_call" | custom-call | tf_op jit(solution)/shard_map/pallas_call | solution.py:499
  133.3 0.6 collective-permute-start.28
  133.9 0.6 collective-permute-start.14
  134.5 1.5 collective-permute-start.10
  136.0 1.5 shard_map.157
  137.5 3.5 %collective-permute-start.45 = (bf16[128,1024]{1,0:T(8,128)(2,1)S(1)}, bf16[128,1024]{1,0:T(8,128)(2,1)S(1)}, u32[]{:S(2)}, u32[]{:S(2)}) collective-permute-start(bf16[128,1024]{1,0:T(8,128)(2,1)S(1)} %get-tuple-element.49), channel_id=1, source_target_pairs={{0,24},{4,28},{8,16},{12,20},{16,8},{20,12},{24,0},{28,4},{1,25},{... | collective-permute-start | bytes 786440 | tf_op jit(solution)/shard_map/ppermute | solution.py:477
  141.0 1.5 shard_map.152
  142.4 1.0 collective-permute-start.29
  143.5 0.6 collective-permute-start.13
  144.0 1.0 collective-permute-done.10.refs_3_
  145.0 0.6 collective-permute-start.15
  145.6 1.6 shard_map.144
  147.2 3.8 %collective-permute-done.13.refs_1_ = bf16[384,256]{1,0:T(8,128)(2,1)S(1)} collective-permute-done((bf16[384,256]{1,0:T(8,128)(2,1)S(1)}, bf16[384,256]{1,0:T(8,128)(2,1)S(1)}, u32[]{:S(2)}, u32[]{:S(2)}) %collective-permute-start.13) | collective-permute-done | bytes 196640 | tf_op jit(solution)/shard_map/ppermute | solution.py:480
  151.0 2.1 %collective-permute-done.15.refs_3_ = bf16[384,256]{1,0:T(8,128)(2,1)S(1)} collective-permute-done((bf16[384,256]{1,0:T(8,128)(2,1)S(1)}, bf16[384,256]{1,0:T(8,128)(2,1)S(1)}, u32[]{:S(2)}, u32[]{:S(2)}) %collective-permute-start.15) | collective-permute-done | bytes 196640 | tf_op jit(solution)/shard_map/ppermute | solution.py:480
  153.1 1.9 %shard_map.145 = bf16[384,1024]{1,0:T(8,128)(2,1)} custom-call(f32[384,1024]{1,0:T(8,128)S(1)} %get-tuple-element.38.first_ref, bf16[1024,1024]{1,0:T(8,128)(2,1)S(1)} %get-tuple-element.39.w_ref, bf16[384,256]{1,0:T(8,128)(2,1)S(1)} %constant_dynamic-update-slice_fusion.2.refs_0_, bf16[384,256]{1,0:T(8,128)(2,1)S(1)} %collective-permute-done.13.refs_1_, ...), custom_call_target="tpu_custom_call" | custom-call | tf_op jit(solution)/shard_map/pallas_call | solution.py:499
  155.0 7.4 %collective-permute-done.44 = bf16[128,1024]{1,0:T(8,128)(2,1)S(1)} collective-permute-done((bf16[128,1024]{1,0:T(8,128)(2,1)S(1)}, bf16[128,1024]{1,0:T(8,128)(2,1)S(1)}, u32[]{:S(2)}, u32[]{:S(2)}) %collective-permute-start.44) | collective-permute-done | bytes 262176 | tf_op jit(solution)/shard_map/ppermute | solution.py:477
  162.4 0.9 add_convert_fusion
  (68 shorter events, 2.0 us)
Async XLA Ops:
  1.6 23.6 %collective-permute-start.30 = (bf16[136,1024]{1,0:T(8,128)(2,1)S(1)}, bf16[136,1024]{1,0:T(8,128)(2,1)S(1)}, u32[]{:S(2)}, u32[]{:S(2)}) collective-permute-start(bf16[136,1024]{1,0:T(8,128)(2,1)S(1)} %shard_map.146.refs_0_), channel_id=1, source_target_pairs={{0,16},{4,20},{8,24},{12,28},{16,0},{20,4},{24,8},{28,12},{1,17},{... | collective-permute-start | bytes 835592 | tf_op jit(solution)/shard_map/ppermute | solution.py:477
  5.7 19.5 %collective-permute-start.31 = (bf16[136,1024]{1,0:T(8,128)(2,1)S(1)}, bf16[136,1024]{1,0:T(8,128)(2,1)S(1)}, u32[]{:S(2)}, u32[]{:S(2)}) collective-permute-start(bf16[136,1024]{1,0:T(8,128)(2,1)S(1)} %shard_map.146.refs_0_), channel_id=1, source_target_pairs={{0,24},{4,28},{8,16},{12,20},{16,8},{20,12},{24,0},{28,4},{1,25},{... | collective-permute-start | bytes 835592 | tf_op jit(solution)/shard_map/ppermute | solution.py:477
  7.1 20.9 %collective-permute-start.16 = (bf16[136,1024]{1,0:T(8,128)(2,1)S(1)}, bf16[136,1024]{1,0:T(8,128)(2,1)S(1)}, u32[]{:S(2)}, u32[]{:S(2)}) collective-permute-start(bf16[136,1024]{1,0:T(8,128)(2,1)S(1)} %shard_map.146.refs_0_), channel_id=1, source_target_pairs={{0,8},{4,12},{8,0},{12,4},{16,24},{20,28},{24,16},{28,20},{1,9},{5... | collective-permute-start | bytes 835592 | tf_op jit(solution)/shard_map/ppermute | solution.py:477
  7.3 20.7 %collective-permute-start.17 = (bf16[136,1024]{1,0:T(8,128)(2,1)S(1)}, bf16[136,1024]{1,0:T(8,128)(2,1)S(1)}, u32[]{:S(2)}, u32[]{:S(2)}) collective-permute-start(bf16[136,1024]{1,0:T(8,128)(2,1)S(1)} %shard_map.146.refs_0_), channel_id=1, source_target_pairs={{0,4},{4,0},{8,12},{12,8},{16,20},{20,16},{24,28},{28,24},{1,5},{5... | collective-permute-start | bytes 835592 | tf_op jit(solution)/shard_map/ppermute | solution.py:477
  7.3 2.2 %copy-start = (bf16[1,4096,512]{2,1,0:T(8,128)(2,1)S(1)}, bf16[1,4096,512]{2,1,0:T(8,128)(2,1)}, u32[]{:S(2)}) copy-start(bf16[1,4096,512]{2,1,0:T(8,128)(2,1)} %gate_ref.3) | copy-start | bytes 12582916
  9.5 74.1 %copy-start.2 = (bf16[1,4096,512]{2,1,0:T(8,128)(2,1)S(1)}, bf16[1,4096,512]{2,1,0:T(8,128)(2,1)}, u32[]{:S(2)}) copy-start(bf16[1,4096,512]{2,1,0:T(8,128)(2,1)} %up_ref.3) | copy-start | bytes 12582916
  9.6 74.3 %copy-start.1 = (bf16[1,4096,512]{2,1,0:T(8,128)(2,1)S(1)}, bf16[1,4096,512]{2,1,0:T(8,128)(2,1)}, u32[]{:S(2)}) copy-start(bf16[1,4096,512]{2,1,0:T(8,128)(2,1)} %gate_ref.3) | copy-start | bytes 12582916
  9.6 74.3 %copy-start.5 = (f32[4096]{0:T(1024)S(1)}, f32[4096]{0:T(1024)}, u32[]{:S(2)}) copy-start(f32[4096]{0:T(1024)} %param.20) | copy-start | bytes 49156
  11.8 21.8 %collective-permute-start = (bf16[384,384]{1,0:T(8,128)(2,1)S(1)}, bf16[384,384]{1,0:T(8,128)(2,1)S(1)}, u32[]{:S(2)}, u32[]{:S(2)}) collective-permute-start(bf16[384,384]{1,0:T(8,128)(2,1)S(1)} %get-tuple-element.27), channel_id=1, source_target_pairs={{0,8},{4,12},{8,0},{12,4},{16,24},{20,28},{24,16},{28,20},{1,9},{5... | collective-permute-start | bytes 884744 | tf_op jit(solution)/shard_map/ppermute | solution.py:477
  25.2 24.9 %collective-permute-start.1 = (bf16[384,384]{1,0:T(8,128)(2,1)S(1)}, bf16[384,384]{1,0:T(8,128)(2,1)S(1)}, u32[]{:S(2)}, u32[]{:S(2)}) collective-permute-start(bf16[384,384]{1,0:T(8,128)(2,1)S(1)} %get-tuple-element.28), channel_id=1, source_target_pairs={{0,16},{4,20},{8,24},{12,28},{16,0},{20,4},{24,8},{28,12},{1,17},{... | collective-permute-start | bytes 884744 | tf_op jit(solution)/shard_map/ppermute | solution.py:477
  25.2 24.9 %collective-permute-start.2 = (bf16[384,384]{1,0:T(8,128)(2,1)S(1)}, bf16[384,384]{1,0:T(8,128)(2,1)S(1)}, u32[]{:S(2)}, u32[]{:S(2)}) collective-permute-start(bf16[384,384]{1,0:T(8,128)(2,1)S(1)} %get-tuple-element.29), channel_id=1, source_target_pairs={{0,24},{4,28},{8,16},{12,20},{16,8},{20,12},{24,0},{28,4},{1,25},{... | collective-permute-start | bytes 884744 | tf_op jit(solution)/shard_map/ppermute | solution.py:477
  28.0 24.0 %collective-permute-start.3 = (bf16[384,384]{1,0:T(8,128)(2,1)S(1)}, bf16[384,384]{1,0:T(8,128)(2,1)S(1)}, u32[]{:S(2)}, u32[]{:S(2)}) collective-permute-start(bf16[384,384]{1,0:T(8,128)(2,1)S(1)} %get-tuple-element.26.refs_0_), channel_id=1, source_target_pairs={{0,4},{4,0},{8,12},{12,8},{16,20},{20,16},{24,28},{28,24},{1,5},{5... | collective-permute-start | bytes 884744 | tf_op jit(solution)/shard_map/ppermute | solution.py:477
  28.0 24.2 %collective-permute-start.32 = (bf16[136,1024]{1,0:T(8,128)(2,1)S(1)}, bf16[136,1024]{1,0:T(8,128)(2,1)S(1)}, u32[]{:S(2)}, u32[]{:S(2)}) collective-permute-start(bf16[136,1024]{1,0:T(8,128)(2,1)S(1)} %collective-permute-done.30.refs_0_), channel_id=1, source_target_pairs={{0,4},{4,0},{8,12},{12,8},{16,20},{20,16},{24,28},{28,24},{1,5},{5... | collective-permute-start | bytes 835592 | tf_op jit(solution)/shard_map/ppermute | solution.py:477
  33.6 19.9 %collective-permute-start.18 = (bf16[128,1024]{1,0:T(8,128)(2,1)S(1)}, bf16[128,1024]{1,0:T(8,128)(2,1)S(1)}, u32[]{:S(2)}, u32[]{:S(2)}) collective-permute-start(bf16[128,1024]{1,0:T(8,128)(2,1)S(1)} %shard_map.147.refs_0_), channel_id=1, source_target_pairs={{0,1},{1,0},{2,3},{3,2},{4,5},{5,4},{6,7},{7,6},{8,9},{9,8},{10,11... | collective-permute-start | bytes 786440 | tf_op jit(solution)/shard_map/ppermute | solution.py:480
  50.2 4.9 %collective-permute-start.36 = (bf16[136,1024]{1,0:T(8,128)(2,1)S(1)}, bf16[136,1024]{1,0:T(8,128)(2,1)S(1)}, u32[]{:S(2)}, u32[]{:S(2)}) collective-permute-start(bf16[136,1024]{1,0:T(8,128)(2,1)S(1)} %collective-permute-done.31.refs_0_.refs_1_), channel_id=1, source_target_pairs={{0,4},{4,0},{8,12},{12,8},{16,20},{20,16},{24,28},{28,24},{1,5},{5... | collective-permute-start | bytes 835592 | tf_op jit(solution)/shard_map/ppermute | solution.py:477
  50.2 9.2 %collective-permute-start.19 = (bf16[128,1024]{1,0:T(8,128)(2,1)S(1)}, bf16[128,1024]{1,0:T(8,128)(2,1)S(1)}, u32[]{:S(2)}, u32[]{:S(2)}) collective-permute-start(bf16[128,1024]{1,0:T(8,128)(2,1)S(1)} %shard_map.147.refs_0_), channel_id=1, source_target_pairs={{0,2},{1,3},{2,0},{3,1},{4,6},{5,7},{6,4},{7,5},{8,10},{9,11},{10,... | collective-permute-start | bytes 786440 | tf_op jit(solution)/shard_map/ppermute | solution.py:480
  52.0 9.2 %collective-permute-start.21 = (bf16[136,1024]{1,0:T(8,128)(2,1)S(1)}, bf16[136,1024]{1,0:T(8,128)(2,1)S(1)}, u32[]{:S(2)}, u32[]{:S(2)}) collective-permute-start(bf16[136,1024]{1,0:T(8,128)(2,1)S(1)} %collective-permute-done.16.refs_0_.refs_1_), channel_id=1, source_target_pairs={{0,4},{4,0},{8,12},{12,8},{16,20},{20,16},{24,28},{28,24},{1,5},{5... | collective-permute-start | bytes 835592 | tf_op jit(solution)/shard_map/ppermute | solution.py:477
  52.2 11.4 %collective-permute-start.4 = (bf16[384,384]{1,0:T(8,128)(2,1)S(1)}, bf16[384,384]{1,0:T(8,128)(2,1)S(1)}, u32[]{:S(2)}, u32[]{:S(2)}) collective-permute-start(bf16[384,384]{1,0:T(8,128)(2,1)S(1)} %collective-permute-done.refs_1_), channel_id=1, source_target_pairs={{0,4},{4,0},{8,12},{12,8},{16,20},{20,16},{24,28},{28,24},{1,5},{5... | collective-permute-start | bytes 884744 | tf_op jit(solution)/shard_map/ppermute | solution.py:477
  53.5 10.7 %collective-permute-start.33 = (bf16[128,1024]{1,0:T(8,128)(2,1)S(1)}, bf16[128,1024]{1,0:T(8,128)(2,1)S(1)}, u32[]{:S(2)}, u32[]{:S(2)}) collective-permute-start(bf16[128,1024]{1,0:T(8,128)(2,1)S(1)} %shard_map.153.refs_0_), channel_id=1, source_target_pairs={{0,1},{1,0},{2,3},{3,2},{4,5},{5,4},{6,7},{7,6},{8,9},{9,8},{10,11... | collective-permute-start | bytes 786440 | tf_op jit(solution)/shard_map/ppermute | solution.py:480
  55.1 9.9 %collective-permute-start.34 = (bf16[128,1024]{1,0:T(8,128)(2,1)S(1)}, bf16[128,1024]{1,0:T(8,128)(2,1)S(1)}, u32[]{:S(2)}, u32[]{:S(2)}) collective-permute-start(bf16[128,1024]{1,0:T(8,128)(2,1)S(1)} %shard_map.153.refs_0_), channel_id=1, source_target_pairs={{0,2},{1,3},{2,0},{3,1},{4,6},{5,7},{6,4},{7,5},{8,10},{9,11},{10,... | collective-permute-start | bytes 786440 | tf_op jit(solution)/shard_map/ppermute | solution.py:480
  59.4 11.2 %collective-permute-start.38 = (bf16[128,1024]{1,0:T(8,128)(2,1)S(1)}, bf16[128,1024]{1,0:T(8,128)(2,1)S(1)}, u32[]{:S(2)}, u32[]{:S(2)}) collective-permute-start(bf16[128,1024]{1,0:T(8,128)(2,1)S(1)} %shard_map.154.refs_4_), channel_id=1, source_target_pairs={{0,2},{1,3},{2,0},{3,1},{4,6},{5,7},{6,4},{7,5},{8,10},{9,11},{10,... | collective-permute-start | bytes 786440 | tf_op jit(solution)/shard_map/ppermute | solution.py:480
  61.2 11.2 %collective-permute-start.37 = (bf16[128,1024]{1,0:T(8,128)(2,1)S(1)}, bf16[128,1024]{1,0:T(8,128)(2,1)S(1)}, u32[]{:S(2)}, u32[]{:S(2)}) collective-permute-start(bf16[128,1024]{1,0:T(8,128)(2,1)S(1)} %shard_map.154.refs_4_), channel_id=1, source_target_pairs={{0,1},{1,0},{2,3},{3,2},{4,5},{5,4},{6,7},{7,6},{8,9},{9,8},{10,11... | collective-permute-start | bytes 786440 | tf_op jit(solution)/shard_map/ppermute | solution.py:480
  63.7 12.5 %collective-permute-start.23 = (bf16[128,1024]{1,0:T(8,128)(2,1)S(1)}, bf16[128,1024]{1,0:T(8,128)(2,1)S(1)}, u32[]{:S(2)}, u32[]{:S(2)}) collective-permute-start(bf16[128,1024]{1,0:T(8,128)(2,1)S(1)} %shard_map.148.refs_4_), channel_id=1, source_target_pairs={{0,2},{1,3},{2,0},{3,1},{4,6},{5,7},{6,4},{7,5},{8,10},{9,11},{10,... | collective-permute-start | bytes 786440 | tf_op jit(solution)/shard_map/ppermute | solution.py:480
  64.3 23.5 %collective-permute-start.5 = (bf16[384,384]{1,0:T(8,128)(2,1)S(1)}, bf16[384,384]{1,0:T(8,128)(2,1)S(1)}, u32[]{:S(2)}, u32[]{:S(2)}) collective-permute-start(bf16[384,384]{1,0:T(8,128)(2,1)S(1)} %collective-permute-done.1.refs_2_), channel_id=1, source_target_pairs={{0,4},{4,0},{8,12},{12,8},{16,20},{20,16},{24,28},{28,24},{1,5},{5... | collective-permute-start | bytes 884744 | tf_op jit(solution)/shard_map/ppermute | solution.py:477
  65.0 16.9 %collective-permute-start.35 = (bf16[128,1024]{1,0:T(8,128)(2,1)S(1)}, bf16[128,1024]{1,0:T(8,128)(2,1)S(1)}, u32[]{:S(2)}, u32[]{:S(2)}) collective-permute-start(bf16[128,1024]{1,0:T(8,128)(2,1)S(1)} %collective-permute-done.33.refs_1_), channel_id=1, source_target_pairs={{0,2},{1,3},{2,0},{3,1},{4,6},{5,7},{6,4},{7,5},{8,10},{9,11},{10,... | collective-permute-start | bytes 786440 | tf_op jit(solution)/shard_map/ppermute | solution.py:480
  70.6 13.0 %collective-permute-start.39 = (bf16[128,1024]{1,0:T(8,128)(2,1)S(1)}, bf16[128,1024]{1,0:T(8,128)(2,1)S(1)}, u32[]{:S(2)}, u32[]{:S(2)}) collective-permute-start(bf16[128,1024]{1,0:T(8,128)(2,1)S(1)} %collective-permute-done.38.refs_6_), channel_id=1, source_target_pairs={{0,1},{1,0},{2,3},{3,2},{4,5},{5,4},{6,7},{7,6},{8,9},{9,8},{10,11... | collective-permute-start | bytes 786440 | tf_op jit(solution)/shard_map/ppermute | solution.py:480
  72.4 17.3 %collective-permute-start.6 = (bf16[384,384]{1,0:T(8,128)(2,1)S(1)}, bf16[384,384]{1,0:T(8,128)(2,1)S(1)}, u32[]{:S(2)}, u32[]{:S(2)}) collective-permute-start(bf16[384,384]{1,0:T(8,128)(2,1)S(1)} %collective-permute-done.2.refs_3_), channel_id=1, source_target_pairs={{0,4},{4,0},{8,12},{12,8},{16,20},{20,16},{24,28},{28,24},{1,5},{5... | collective-permute-start | bytes 884744 | tf_op jit(solution)/shard_map/ppermute | solution.py:477
  76.2 28.6 %collective-permute-start.20 = (bf16[128,1024]{1,0:T(8,128)(2,1)S(1)}, bf16[128,1024]{1,0:T(8,128)(2,1)S(1)}, u32[]{:S(2)}, u32[]{:S(2)}) collective-permute-start(bf16[128,1024]{1,0:T(8,128)(2,1)S(1)} %collective-permute-done.18.refs_1_), channel_id=1, source_target_pairs={{0,2},{1,3},{2,0},{3,1},{4,6},{5,7},{6,4},{7,5},{8,10},{9,11},{10,... | collective-permute-start | bytes 786440 | tf_op jit(solution)/shard_map/ppermute | solution.py:480
  81.8 28.9 %collective-permute-start.22 = (bf16[128,1024]{1,0:T(8,128)(2,1)S(1)}, bf16[128,1024]{1,0:T(8,128)(2,1)S(1)}, u32[]{:S(2)}, u32[]{:S(2)}) collective-permute-start(bf16[128,1024]{1,0:T(8,128)(2,1)S(1)} %shard_map.148.refs_4_), channel_id=1, source_target_pairs={{0,1},{1,0},{2,3},{3,2},{4,5},{5,4},{6,7},{7,6},{8,9},{9,8},{10,11... | collective-permute-start | bytes 786440 | tf_op jit(solution)/shard_map/ppermute | solution.py:480
  83.6 27.6 %collective-permute-start.24 = (bf16[128,1024]{1,0:T(8,128)(2,1)S(1)}, bf16[128,1024]{1,0:T(8,128)(2,1)S(1)}, u32[]{:S(2)}, u32[]{:S(2)}) collective-permute-start(bf16[128,1024]{1,0:T(8,128)(2,1)S(1)} %collective-permute-done.23.refs_6_), channel_id=1, source_target_pairs={{0,1},{1,0},{2,3},{3,2},{4,5},{5,4},{6,7},{7,6},{8,9},{9,8},{10,11... | collective-permute-start | bytes 786440 | tf_op jit(solution)/shard_map/ppermute | solution.py:480
  83.9 11.4 %copy-start.6 = (f32[4]{0:T(128)S(1)}, f32[4]{0:T(128)}, u32[]{:S(2)}) copy-start(f32[4]{0:T(128)} %scale_ref.1) | copy-start | bytes 52
  83.9 11.4 %copy-start.7 = (f32[128]{0:T(128)S(1)}, f32[128]{0:T(128)}, u32[]{:S(2)}) copy-start(f32[128]{0:T(128)} %param.17) | copy-start | bytes 1540
  87.8 30.4 %collective-permute-start.40 = (bf16[256,512]{1,0:T(8,128)(2,1)S(1)}, bf16[256,512]{1,0:T(8,128)(2,1)S(1)}, u32[]{:S(2)}, u32[]{:S(2)}) collective-permute-start(bf16[256,512]{1,0:T(8,128)(2,1)S(1)} %shard_map.155.refs_0_), channel_id=1, source_target_pairs={{0,1},{1,0},{2,3},{3,2},{4,5},{5,4},{6,7},{7,6},{8,9},{9,8},{10,11... | collective-permute-start | bytes 786440 | tf_op jit(solution)/shard_map/ppermute | solution.py:480
  89.6 29.0 %collective-permute-start.41 = (bf16[256,512]{1,0:T(8,128)(2,1)S(1)}, bf16[256,512]{1,0:T(8,128)(2,1)S(1)}, u32[]{:S(2)}, u32[]{:S(2)}) collective-permute-start(bf16[256,512]{1,0:T(8,128)(2,1)S(1)} %shard_map.155.refs_0_), channel_id=1, source_target_pairs={{0,2},{1,3},{2,0},{3,1},{4,6},{5,7},{6,4},{7,5},{8,10},{9,11},{10,... | collective-permute-start | bytes 786440 | tf_op jit(solution)/shard_map/ppermute | solution.py:480
  104.9 19.5 %copy-start.3 = (bf16[1,2048,1024]{2,1,0:T(8,128)(2,1)S(1)}, bf16[1,2048,1024]{2,1,0:T(8,128)(2,1)}, u32[]{:S(2)}) copy-start(bf16[1,2048,1024]{2,1,0:T(8,128)(2,1)} %w_ref.5) | copy-start | bytes 12582916
  104.9 11.8 %collective-permute-start.7 = (bf16[384,128]{1,0:T(8,128)(2,1)S(1)}, bf16[384,128]{1,0:T(8,128)(2,1)S(1)}, u32[]{:S(2)}, u32[]{:S(2)}) collective-permute-start(bf16[384,128]{1,0:T(8,128)(2,1)S(1)} %get-tuple-element.37), channel_id=1, source_target_pairs={{0,8},{4,12},{8,0},{12,4},{16,24},{20,28},{24,16},{28,20},{1,9},{5... | collective-permute-start | bytes 294920 | tf_op jit(solution)/shard_map/ppermute | solution.py:477
  110.8 10.2 %collective-permute-start.42 = (bf16[256,512]{1,0:T(8,128)(2,1)S(1)}, bf16[256,512]{1,0:T(8,128)(2,1)S(1)}, u32[]{:S(2)}, u32[]{:S(2)}) collective-permute-start(bf16[256,512]{1,0:T(8,128)(2,1)S(1)} %shard_map.155.refs_0_), channel_id=1, source_target_pairs={{0,3},{1,2},{2,1},{3,0},{4,7},{5,6},{6,5},{7,4},{8,11},{9,10},{10,... | collective-permute-start | bytes 786440 | tf_op jit(solution)/shard_map/ppermute | solution.py:480
  115.1 11.2 %collective-permute-start.25 = (bf16[256,512]{1,0:T(8,128)(2,1)S(1)}, bf16[256,512]{1,0:T(8,128)(2,1)S(1)}, u32[]{:S(2)}, u32[]{:S(2)}) collective-permute-start(bf16[256,512]{1,0:T(8,128)(2,1)S(1)} %shard_map.150.refs_0_), channel_id=1, source_target_pairs={{0,1},{1,0},{2,3},{3,2},{4,5},{5,4},{6,7},{7,6},{8,9},{9,8},{10,11... | collective-permute-start | bytes 786440 | tf_op jit(solution)/shard_map/ppermute | solution.py:480
  116.6 12.1 %collective-permute-start.26 = (bf16[256,512]{1,0:T(8,128)(2,1)S(1)}, bf16[256,512]{1,0:T(8,128)(2,1)S(1)}, u32[]{:S(2)}, u32[]{:S(2)}) collective-permute-start(bf16[256,512]{1,0:T(8,128)(2,1)S(1)} %shard_map.150.refs_0_), channel_id=1, source_target_pairs={{0,2},{1,3},{2,0},{3,1},{4,6},{5,7},{6,4},{7,5},{8,10},{9,11},{10,... | collective-permute-start | bytes 786440 | tf_op jit(solution)/shard_map/ppermute | solution.py:480
  118.2 13.2 %collective-permute-start.27 = (bf16[256,512]{1,0:T(8,128)(2,1)S(1)}, bf16[256,512]{1,0:T(8,128)(2,1)S(1)}, u32[]{:S(2)}, u32[]{:S(2)}) collective-permute-start(bf16[256,512]{1,0:T(8,128)(2,1)S(1)} %shard_map.150.refs_0_), channel_id=1, source_target_pairs={{0,3},{1,2},{2,1},{3,0},{4,7},{5,6},{6,5},{7,4},{8,11},{9,10},{10,... | collective-permute-start | bytes 786440 | tf_op jit(solution)/shard_map/ppermute | solution.py:480
  118.7 14.6 %collective-permute-start.11 = (bf16[384,128]{1,0:T(8,128)(2,1)S(1)}, bf16[384,128]{1,0:T(8,128)(2,1)S(1)}, u32[]{:S(2)}, u32[]{:S(2)}) collective-permute-start(bf16[384,128]{1,0:T(8,128)(2,1)S(1)} %get-tuple-element.40), channel_id=1, source_target_pairs={{0,16},{4,20},{8,24},{12,28},{16,0},{20,4},{24,8},{28,12},{1,17},{... | collective-permute-start | bytes 294920 | tf_op jit(solution)/shard_map/ppermute | solution.py:477
  121.0 12.9 %collective-permute-start.12 = (bf16[384,128]{1,0:T(8,128)(2,1)S(1)}, bf16[384,128]{1,0:T(8,128)(2,1)S(1)}, u32[]{:S(2)}, u32[]{:S(2)}) collective-permute-start(bf16[384,128]{1,0:T(8,128)(2,1)S(1)} %get-tuple-element.41), channel_id=1, source_target_pairs={{0,24},{4,28},{8,16},{12,20},{16,8},{20,12},{24,0},{28,4},{1,25},{... | collective-permute-start | bytes 294920 | tf_op jit(solution)/shard_map/ppermute | solution.py:477
  126.3 19.3 %copy-start.4 = (bf16[2048,1024]{1,0:T(8,128)(2,1)S(1)}, bf16[2048,1024]{1,0:T(8,128)(2,1)}, u32[]{:S(2)}) copy-start(bf16[2048,1024]{1,0:T(8,128)(2,1)} %w_ref.3) | copy-start | bytes 12582916
  126.3 8.2 %collective-permute-start.8 = (bf16[384,256]{1,0:T(8,128)(2,1)S(1)}, bf16[384,256]{1,0:T(8,128)(2,1)S(1)}, u32[]{:S(2)}, u32[]{:S(2)}) collective-permute-start(bf16[384,256]{1,0:T(8,128)(2,1)S(1)} %constant_dynamic-update-slice_fusion.refs_0_), channel_id=1, source_target_pairs={{0,1},{1,0},{2,3},{3,2},{4,5},{5,4},{6,7},{7,6},{8,9},{9,8},{10,11... | collective-permute-start | bytes 589832 | tf_op jit(solution)/shard_map/ppermute | solution.py:480
  128.7 13.7 %collective-permute-start.9 = (bf16[384,256]{1,0:T(8,128)(2,1)S(1)}, bf16[384,256]{1,0:T(8,128)(2,1)S(1)}, u32[]{:S(2)}, u32[]{:S(2)}) collective-permute-start(bf16[384,256]{1,0:T(8,128)(2,1)S(1)} %constant_dynamic-update-slice_fusion.refs_0_), channel_id=1, source_target_pairs={{0,2},{1,3},{2,0},{3,1},{4,6},{5,7},{6,4},{7,5},{8,10},{9,11},{10,... | collective-permute-start | bytes 589832 | tf_op jit(solution)/shard_map/ppermute | solution.py:480
  131.4 4.6 %collective-permute-start.43 = (bf16[128,1024]{1,0:T(8,128)(2,1)S(1)}, bf16[128,1024]{1,0:T(8,128)(2,1)S(1)}, u32[]{:S(2)}, u32[]{:S(2)}) collective-permute-start(bf16[128,1024]{1,0:T(8,128)(2,1)S(1)} %get-tuple-element.47), channel_id=1, source_target_pairs={{0,4},{4,0},{8,12},{12,8},{16,20},{20,16},{24,28},{28,24},{1,5},{5... | collective-permute-start | bytes 786440 | tf_op jit(solution)/shard_map/ppermute | solution.py:477
  133.3 7.7 %collective-permute-start.28 = (bf16[128,1024]{1,0:T(8,128)(2,1)S(1)}, bf16[128,1024]{1,0:T(8,128)(2,1)S(1)}, u32[]{:S(2)}, u32[]{:S(2)}) collective-permute-start(bf16[128,1024]{1,0:T(8,128)(2,1)S(1)} %get-tuple-element.43), channel_id=1, source_target_pairs={{0,4},{4,0},{8,12},{12,8},{16,20},{20,16},{24,28},{28,24},{1,5},{5... | collective-permute-start | bytes 786440 | tf_op jit(solution)/shard_map/ppermute | solution.py:477
  133.9 9.6 %collective-permute-start.14 = (bf16[384,256]{1,0:T(8,128)(2,1)S(1)}, bf16[384,256]{1,0:T(8,128)(2,1)S(1)}, u32[]{:S(2)}, u32[]{:S(2)}) collective-permute-start(bf16[384,256]{1,0:T(8,128)(2,1)S(1)} %constant_dynamic-update-slice_fusion.2.refs_0_), channel_id=1, source_target_pairs={{0,2},{1,3},{2,0},{3,1},{4,6},{5,7},{6,4},{7,5},{8,10},{9,11},{10,... | collective-permute-start | bytes 589832 | tf_op jit(solution)/shard_map/ppermute | solution.py:480
  134.5 10.5 %collective-permute-start.10 = (bf16[384,256]{1,0:T(8,128)(2,1)S(1)}, bf16[384,256]{1,0:T(8,128)(2,1)S(1)}, u32[]{:S(2)}, u32[]{:S(2)}) collective-permute-start(bf16[384,256]{1,0:T(8,128)(2,1)S(1)} %collective-permute-done.8.refs_1_), channel_id=1, source_target_pairs={{0,2},{1,3},{2,0},{3,1},{4,6},{5,7},{6,4},{7,5},{8,10},{9,11},{10,... | collective-permute-start | bytes 589832 | tf_op jit(solution)/shard_map/ppermute | solution.py:480
  137.5 17.5 %collective-permute-start.45 = (bf16[128,1024]{1,0:T(8,128)(2,1)S(1)}, bf16[128,1024]{1,0:T(8,128)(2,1)S(1)}, u32[]{:S(2)}, u32[]{:S(2)}) collective-permute-start(bf16[128,1024]{1,0:T(8,128)(2,1)S(1)} %get-tuple-element.49), channel_id=1, source_target_pairs={{0,24},{4,28},{8,16},{12,20},{16,8},{20,12},{24,0},{28,4},{1,25},{... | collective-permute-start | bytes 786440 | tf_op jit(solution)/shard_map/ppermute | solution.py:477
  140.9 21.4 %collective-permute-start.44 = (bf16[128,1024]{1,0:T(8,128)(2,1)S(1)}, bf16[128,1024]{1,0:T(8,128)(2,1)S(1)}, u32[]{:S(2)}, u32[]{:S(2)}) collective-permute-start(bf16[128,1024]{1,0:T(8,128)(2,1)S(1)} %get-tuple-element.48), channel_id=1, source_target_pairs={{0,16},{4,20},{8,24},{12,28},{16,0},{20,4},{24,8},{28,12},{1,17},{... | collective-permute-start | bytes 786440 | tf_op jit(solution)/shard_map/ppermute | solution.py:477
  142.4 19.9 %collective-permute-start.29 = (bf16[128,1024]{1,0:T(8,128)(2,1)S(1)}, bf16[128,1024]{1,0:T(8,128)(2,1)S(1)}, u32[]{:S(2)}, u32[]{:S(2)}) collective-permute-start(bf16[128,1024]{1,0:T(8,128)(2,1)S(1)} %get-tuple-element.45), channel_id=1, source_target_pairs={{0,8},{4,12},{8,0},{12,4},{16,24},{20,28},{24,16},{28,20},{1,9},{5... | collective-permute-start | bytes 786440 | tf_op jit(solution)/shard_map/ppermute | solution.py:477
  143.5 7.5 %collective-permute-start.13 = (bf16[384,256]{1,0:T(8,128)(2,1)S(1)}, bf16[384,256]{1,0:T(8,128)(2,1)S(1)}, u32[]{:S(2)}, u32[]{:S(2)}) collective-permute-start(bf16[384,256]{1,0:T(8,128)(2,1)S(1)} %constant_dynamic-update-slice_fusion.2.refs_0_), channel_id=1, source_target_pairs={{0,1},{1,0},{2,3},{3,2},{4,5},{5,4},{6,7},{7,6},{8,9},{9,8},{10,11... | collective-permute-start | bytes 589832 | tf_op jit(solution)/shard_map/ppermute | solution.py:480
  145.0 8.1 %collective-permute-start.15 = (bf16[384,256]{1,0:T(8,128)(2,1)S(1)}, bf16[384,256]{1,0:T(8,128)(2,1)S(1)}, u32[]{:S(2)}, u32[]{:S(2)}) collective-permute-start(bf16[384,256]{1,0:T(8,128)(2,1)S(1)} %collective-permute-done.14.refs_2_), channel_id=1, source_target_pairs={{0,1},{1,0},{2,3},{3,2},{4,5},{5,4},{6,7},{7,6},{8,9},{9,8},{10,11... | collective-permute-start | bytes 589832 | tf_op jit(solution)/shard_map/ppermute | solution.py:480
